TPU v7x, 256 devices: a whole 4x4x8 slice. The times are simulated.
256 devices in a mesh: sp: 64 (over z, y, core), tp: 4 (over x).
Axes of the slice: x: 4, y: 4, z: 8, core: 2. Of those that a mesh axis runs over, the one named last changes fastest.
Arguments:
- queries: bfloat16 [16384, 2048], P('sp', 'tp'), may hold values from -16 to 16
- key_value_pairs: bfloat16 [16384, 512], P('sp', 'tp'), may hold values from -16 to 16
- forget_gate_total: float32 [16384, 32], P('sp', 'tp'), may hold values from -16384 to 0, as said below
- residual_in: bfloat16 [16384, 2048], P(('sp', 'tp')), may hold values from -12 to 12
- out_weight: bfloat16 [2048, 2048], P('tp'), may hold values from -0.25 to 0.25
- norm_gain: float32 [2048], replicated, may hold values from 0.1 to 1.9
- routes: int32 [16384, 2], P(('sp', 'tp')), may hold values from 0 to 63, all different within a row; in each aligned block of 64 rows (0 to 63, 64 to 127, ...) at most 3 rows name the same one
- route_weight: float32 [16384, 2], P(('sp', 'tp')), may hold values from 0.2 to 1
- expert_gate: bfloat16 [64, 2048, 3072], P('sp', None, 'tp'), may hold values from -0.125 to 0.125
- expert_up: bfloat16 [64, 2048, 3072], P('sp', None, 'tp'), may hold values from -0.125 to 0.125
- expert_down: bfloat16 [64, 3072, 2048], P('sp', 'tp'), may hold values from -0.109375 to 0.109375
Outputs:
- layer_out: bfloat16 [16384, 2048], P(('sp', 'tp'))
Inputs may be any that keep to these rules, and one draw needn't show every extreme that they name: `routes`: each row names 2 different experts; among the rows of one device no expert is named more than 3 times, and in every draw some device names some expert exactly 3 times. `forget_gate_total`: along the positions, each head's values never rise.
All inputs are finite; a program needn't handle non-finite values.
Results may differ from a plain program's by a relative error of at most 0.011.
Values may be sent and summed in bfloat16 or wider, within the bound.
No kernel may reach another device: no remote copies, remote signals or barrier semaphores. Data moves between devices by JAX's collectives and lax.ppermute only.
A program may use at most 64 MiB of HBM per device.

v0:
```python
import math

import jax
import jax.numpy as jnp
from jax import lax
from jax.sharding import Mesh
from jax.sharding import PartitionSpec as P

HEAD_SIZE = 64
SP = ("sp_0", "sp_1", "sp_2")
SP_TP = ("sp_0", "sp_1", "sp_2", "tp")


NEG_FILL = -1e30
NORM_EPS = 1e-06


def copy_for_each(array, axis):
    copies = jnp.broadcast_to(array, (lax.axis_size(axis), *array.shape))
    return lax.all_to_all(copies, axis, split_axis=0, concat_axis=0, tiled=True)


def joined_along(tiles, dim):
    tiles = jnp.moveaxis(tiles, 0, dim)
    shape = tiles.shape
    return tiles.reshape(*shape[:dim], shape[dim] * shape[dim + 1], *shape[dim + 2 :])


def gathered_copies(array, axis, dim):
    tiles = copy_for_each(array, axis)
    return joined_along(tiles, dim)


def stacked_from(array, axes, order):
    tiles = array
    for k in order:
        tiles = lax.all_gather(tiles, axes[k])
    done = order[::-1]
    back = [done.index(k) for k in range(len(axes))]
    tiles = tiles.transpose(*back, *range(len(axes), tiles.ndim))
    return tiles.reshape(-1, *array.shape)


def gathered_by_axis(array, axes, order, dim):
    return joined_along(stacked_from(array, axes, order), dim)


def cut_along(array, dim, devices):
    shape = array.shape
    tiles = array.reshape(*shape[:dim], devices, shape[dim] // devices, *shape[dim + 1 :])
    return jnp.moveaxis(tiles, dim, 0)


def sum_at_owner(array, axis, dim):
    devices = lax.axis_size(axis)
    tiles = lax.all_to_all(cut_along(array, dim, devices), axis, 0, 0, tiled=True)
    return jnp.sum(tiles.astype(jnp.float32), axis=0)


def slot_ranks(chosen, experts):
    onehot = (chosen[..., None] == jnp.arange(experts, dtype=jnp.int32)).astype(jnp.int32)
    earlier = jnp.cumsum(onehot, axis=-2) - onehot
    return jnp.sum(earlier * onehot, axis=-1)


def fill_slots(source_rows, target, slot_total, per_row):
    owner_slot = (
        jnp.zeros((slot_total,), jnp.int32)
        .at[target]
        .set(jnp.arange(1, target.shape[0] + 1, dtype=jnp.int32))
    )
    picked = source_rows[jnp.maximum(owner_slot - 1, 0) // per_row]
    return jnp.where((owner_slot > 0)[:, None], picked, jnp.zeros_like(picked))


def local(
    queries,
    key_value_pairs,
    forget_gate_total,
    residual_in,
    out_weight,
    norm_gain,
    routes,
    route_weight,
    expert_gate,
    expert_up,
    expert_down,
):
    seq_devices = lax.axis_size(SP)
    head_devices = lax.axis_size("tp")
    tok_rows = queries.shape[0]
    local_heads = queries.shape[1] // HEAD_SIZE
    local_groups = key_value_pairs.shape[1] // (2 * HEAD_SIZE)
    queries_per_group = local_heads // local_groups
    score_scale = HEAD_SIZE ** (-0.5)
    seq_index = lax.axis_index(SP)
    own_start = seq_index * tok_rows
    all_gates = gathered_copies(forget_gate_total, SP, 0)

    def attend_block(carried, query_set, kv_block, key_start):
        grouped_queries, query_gate, query_pos = query_set
        run_max, run_total, run_acc = carried
        key_count = kv_block.shape[0]
        key_value_head_list = kv_block.reshape(key_count, local_groups, 2 * HEAD_SIZE)
        scores = (
            jnp.einsum(
                "tkgd,skd->ktgs",
                grouped_queries,
                key_value_head_list[:, :, :HEAD_SIZE],
                preferred_element_type=jnp.float32,
            )
            * score_scale
        )
        gate_block = lax.dynamic_slice_in_dim(all_gates, key_start, key_count, 0)
        key_gate = gate_block.reshape(key_count, local_groups, queries_per_group).transpose(1, 2, 0)
        scores = scores + query_gate[..., None] - key_gate[:, None, :, :]
        key_pos = key_start + jnp.arange(key_count, dtype=jnp.int32)
        scores = jnp.where(
            key_pos[None, None, None, :] <= query_pos[None, :, None, None], scores, NEG_FILL
        )
        new_max = jnp.maximum(run_max, jnp.max(scores, axis=3))
        weights = jnp.exp(scores - new_max[..., None])
        rescale = jnp.exp(run_max - new_max)
        run_total = run_total * rescale + jnp.sum(weights, axis=3)
        block_sum = jnp.einsum(
            "ktgs,skd->ktgd",
            weights.astype(jnp.bfloat16),
            key_value_head_list[:, :, HEAD_SIZE:],
            preferred_element_type=jnp.float32,
        )
        return (new_max, run_total, run_acc * rescale[..., None] + block_sum)

    def start_state(row_count):
        return (
            jnp.full((local_groups, row_count, queries_per_group), NEG_FILL, jnp.float32),
            jnp.zeros((local_groups, row_count, queries_per_group), jnp.float32),
            jnp.zeros((local_groups, row_count, queries_per_group, HEAD_SIZE), jnp.float32),
        )

    row_count = queries.shape[0]
    grouped_queries = queries.reshape(row_count, local_groups, queries_per_group, HEAD_SIZE)
    query_gate = lax.dynamic_slice_in_dim(all_gates, own_start, row_count, 0)
    query_gate = query_gate.reshape(row_count, local_groups, queries_per_group).transpose(1, 0, 2)
    query_pos = own_start + jnp.arange(row_count, dtype=jnp.int32)
    query_sets = ((grouped_queries, query_gate, query_pos),)
    initial = tuple((start_state(query_set[2].shape[0]) for query_set in query_sets))
    kv_piece = gathered_by_axis(key_value_pairs, SP, (1, 0, 2), 0)
    length = kv_piece.shape[0]
    key_block = math.gcd(length, 512)
    kv_blocks = kv_piece.reshape(length // key_block, key_block, kv_piece.shape[1])

    def one_block(block_index, inner_states):
        key_start = block_index * key_block
        updated = []
        for query_set, running in zip(query_sets, inner_states):
            last_pos = query_set[2][-1]
            updated.append(
                lax.cond(
                    key_start <= last_pos,
                    lambda state, chosen_set=query_set: attend_block(
                        state, chosen_set, kv_blocks[block_index], key_start
                    ),
                    lambda state: state,
                    running,
                )
            )
        return tuple(updated)

    states = lax.fori_loop(0, length // key_block, one_block, initial)
    run_max, run_total, run_acc = states[0]
    row_count = run_total.shape[1]
    attended = (
        (run_acc / run_total[..., None])
        .transpose(1, 0, 2, 3)
        .reshape(row_count, local_heads * HEAD_SIZE)
        .astype(jnp.bfloat16)
    )
    own_rows = tok_rows // head_devices
    row_block = attended
    mixed_rows = sum_at_owner(
        jnp.dot(row_block, out_weight, preferred_element_type=jnp.float32).astype(jnp.bfloat16),
        "tp",
        0,
    )
    hidden_state = residual_in.astype(jnp.float32) + mixed_rows
    normed = (
        hidden_state
        * lax.rsqrt(jnp.mean(hidden_state * hidden_state, axis=1, keepdims=True) + NORM_EPS)
        * norm_gain
    ).astype(jnp.bfloat16)
    top_count = routes.shape[1]
    capacity = max(2, 3 * own_rows * top_count // (2 * seq_devices))
    model_width = normed.shape[1]
    chosen = routes.reshape(-1)
    target = chosen * capacity + slot_ranks(chosen, seq_devices)
    outgoing = fill_slots(normed, target, seq_devices * capacity, top_count).reshape(
        seq_devices, capacity, model_width
    )
    incoming = lax.all_to_all(outgoing, SP, split_axis=0, concat_axis=0, tiled=True)
    arrived = lax.all_gather(incoming, "tp", axis=0, tiled=True)
    flat_in = arrived.reshape(-1, model_width)
    gate_value = jnp.dot(flat_in, expert_gate[0], preferred_element_type=jnp.float32)
    up_value = jnp.dot(flat_in, expert_up[0], preferred_element_type=jnp.float32)
    hidden_rows = (
        (jax.nn.silu(gate_value) * up_value)
        .astype(jnp.bfloat16)
        .reshape(arrived.shape[0], capacity, -1)
    )
    row_block = hidden_rows
    summed = lax.psum_scatter(
        jnp.einsum(
            "rcf,fd->rcd", row_block, expert_down[0], preferred_element_type=jnp.float32
        ).astype(jnp.bfloat16),
        "tp",
        scatter_dimension=0,
        tiled=True,
    )
    returned = lax.all_to_all(summed, SP, split_axis=0, concat_axis=0, tiled=True)
    picked = returned.reshape(-1, model_width)[target].reshape(own_rows, top_count, model_width)
    combined = jnp.sum(picked.astype(jnp.float32) * route_weight[..., None], axis=1)
    return (hidden_state + combined).astype(jnp.bfloat16)


def solution(mesh):
    finer = Mesh(mesh.devices.reshape(8, 4, 2, mesh.shape["tp"]), ("sp_0", "sp_1", "sp_2", "tp"))
    in_specs = (
        P(SP, "tp"),
        P(SP, "tp"),
        P(SP, "tp"),
        P(SP_TP, None),
        P("tp", None),
        P(),
        P(SP_TP, None),
        P(SP_TP, None),
        P(SP, None, "tp"),
        P(SP, None, "tp"),
        P(SP, "tp", None),
    )
    out_specs = P(SP_TP, None)
    return jax.shard_map(local, mesh=finer, in_specs=in_specs, out_specs=out_specs, check_vma=False)
```

profile of v0, /device:TPU:6, one launch (start us, length us, event | category | flops | bytes accessed | tf_op | source)
XLA Modules:
  0.0 572.0 jit_solution(312068319406776079)
XLA Ops:
  6.5 14.7 %all-gather = bf16[1024,128]{1,0:T(8,128)(2,1)} all-gather(bf16[256,128]{1,0:T(8,128)(2,1)} %param.16), channel_id=2, replica_groups=mesh['sp_0'=8,'sp_1'=4,'sp_2'=2,'tp'=4] {'sp_1'}, dimensions={0}, use_global_device_ids=true | all-gather | bytes 327680 | tf_op jit(solution)/shard_map/all_gather | solution.py:37
  21.3 42.3 %all-gather.9.cloned.1.call-done = bf16[32,256,128]{2,1,0:T(8,128)(2,1)} async-done(((bf16[4,256,128]{2,1,0:T(8,128)(2,1)}), bf16[32,256,128]{2,1,0:T(8,128)(2,1)}) %all-gather.9.cloned.1.call-update) | async-done | bytes 2097168 | tf_op jit(solution)/shard_map/all_gather | solution.py:37
  63.7 1.5 broadcast_in_dim.56
  65.2 8.0 %all-to-all-start = ((f32[64,256,8]{1,2,0:T(8,128)}), f32[64,256,8]{1,2,0:T(8,128)}, u32[]{:S(2)}, u32[]{:S(2)}) async-start(f32[64,256,8]{1,2,0:T(8,128)} %broadcast_in_dim.56), calls=%async_computation | async-start | bytes 1048576 | tf_op jit(solution)/shard_map/all_to_all | solution.py:20
  73.2 0.8 copy.36
  74.8 15.9 %all-to-all-done = f32[64,256,8]{1,2,0:T(8,128)} async-done(((f32[64,256,8]{1,2,0:T(8,128)}), f32[64,256,8]{1,2,0:T(8,128)}, u32[]{:S(2)}, u32[]{:S(2)}) %all-to-all-start) | async-done | bytes 524320 | tf_op jit(solution)/shard_map/all_to_all | solution.py:20
  90.7 0.7 constant_dynamic-slice_fusion
  91.4 4.7 copy.35
  96.0 6.5 %copy.37 = bf16[32,512,128]{1,2,0:T(8,128)(2,1)} copy(bf16[32,512,128]{2,1,0:T(8,128)(2,1)} %bitcast.86) | data formatting | bytes 8388608 | tf_op jit(solution)/shard_map/while | solution.py:169
  102.6 0.8 broadcast_in_dim.55
  103.4 42.3 %while.17 = (s32[]{:T(128)}, f32[1,256,8]{1,2,0:T(8,128)S(1)}, f32[1,256,8]{1,2,0:T(8,128)S(1)}, f32[1,256,8,64]{1,3,2,0:T(8,128)}, s32[256]{0:T(256)S(1)}, /*in...) while((s32[]{:T(128)}, f32[1,256,8]{1,2,0:T(8,128)S(1)}, ...), condition=%wide.region_5.6_spmd, body=%wide.region_0.5_spmd.sunk | while | flops 286661120 | bytes 19248544 | solution.py:169
  104.5 5.9 %conditional.2 = ((f32[1,256,8]{1,2,0:T(8,128)S(1)}, f32[1,256,8]{1,2,0:T(8,128)S(1)}, f32[1,256,8,64]{1,3,2,0:T(8,128)})) conditional(s32[]{:T(128)} %convert_element_type.84, (f32[1,256,8]{1,2,0:T(8,128)S(1)}, f32[1,256,8]{1,2,0:T(8,128)S(1)}, f32[1,256,8,64]{1,3,2,0:T(8,128)}) %tuple.41, (s32[]{:T(128)}, s32[256]{0:T(256)S(1)}, s32[]{:T(128)}, ...), branch_computations={%region_1.0_spmd, %region_2.4_spmd} | conditional | flops 286661120 | bytes 19248296 | solution.py:158
  104.5 0.7 dynamic-slice_bitcast_fusion.1
  105.3 0.9 dynamic-slice_bitcast_fusion
  106.3 1.1 fusion.3
  107.5 1.5 fusion.10
  109.0 1.4 fusion.2
  110.5 0.5 slice.26
  111.6 0.5 slice.26
  145.7 1.1 divide_convert_fusion
  146.8 3.4 convolution_convert_fusion.1
  150.2 4.8 all-to-all-start.1
  155.2 1.0 scatter_custom_fusion
  156.4 12.2 %all-to-all-done.1 = bf16[4,64,2048]{2,1,0:T(8,128)(2,1)} async-done(((bf16[4,64,2048]{2,1,0:T(8,128)(2,1)}), bf16[4,64,2048]{2,1,0:T(8,128)(2,1)}, u32[]{:S(2)}, u32[]{:S(2)}) %all-to-all-start.1) | async-done | bytes 1048608 | tf_op jit(solution)/shard_map/all_to_all | solution.py:56
  168.6 1.4 convert_reduce_fusion
  170.3 0.6 copy-done.1
  170.9 1.1 multiply_convert_fusion.1
  171.9 2.1 gather_fusion
  174.0 3.3 gather.9
  177.3 1.8 broadcast_select_fusion
  179.0 217.1 %all_to_all.20 = bf16[64,3,2048]{2,1,0:T(4,128)(2,1)S(1)} all-to-all(bf16[64,3,2048]{2,1,0:T(4,128)(2,1)S(1)} %broadcast_select_fusion), channel_id=1, replica_groups=mesh['sp_0'=8,'sp_1'=4,'sp_2'=2,'tp'=4] {'sp_0','sp_1','sp_2'}, dimensions={0} | all-to-all | bytes 1572864 | tf_op jit(solution)/shard_map/all_to_all | solution.py:199
  396.2 1.5 copy.40
  397.9 36.2 %all-gather.7.cloned.1.call-done = bf16[256,3,2048]{2,0,1:T(8,128)(2,1)} async-done(((bf16[64,3,2048]{2,0,1:T(8,128)(2,1)}), bf16[256,3,2048]{2,0,1:T(8,128)(2,1)}) %all-gather.7.cloned.1.call-update) | async-done | bytes 3145744 | tf_op jit(solution)/shard_map/all_gather | solution.py:200
  434.1 6.5 %copy.41 = bf16[256,3,2048]{2,1,0:T(4,128)(2,1)} copy(bf16[256,3,2048]{2,0,1:T(8,128)(2,1)} %all-gather.7.cloned.1.call-done) | data formatting | bytes 6291456 | tf_op jit(solution)/shard_map/all_gather | solution.py:200
  440.6 8.8 %reshape.151 = bf16[768,2048]{1,0:T(8,128)(2,1)} reshape(bf16[256,3,2048]{2,1,0:T(4,128)(2,1)} %copy.41) | data formatting | bytes 6291456 | tf_op jit(solution)/shard_map/reshape | solution.py:201
  449.4 5.6 fusion.19
  455.1 3.9 multiply_convert_fusion
  458.9 3.7 reshape.152
  462.6 5.4 convolution_convert_fusion
  468.1 41.2 %reduce-scatter.2.cloned.1.call-done = bf16[64,3,2048]{2,0,1:T(8,128)(2,1)} async-done(((bf16[256,3,2048]{2,0,1:T(8,128)(2,1)}), bf16[64,3,2048]{2,0,1:T(8,128)(2,1)}) %reduce-scatter.2.cloned.1.call-update) | async-done | bytes 786448 | tf_op jit(solution)/shard_map/reduce_scatter | solution.py:210
  509.3 2.8 copy.43
  512.1 11.0 %all-to-all-start.3 = ((bf16[64,3,2048]{2,1,0:T(4,128)(2,1)}), bf16[64,3,2048]{2,1,0:T(4,128)(2,1)}, u32[]{:S(2)}, u32[]{:S(2)}) async-start(bf16[64,3,2048]{2,1,0:T(4,128)(2,1)} %copy.43), calls=%async_computation.4 | async-start | bytes 2097152 | tf_op jit(solution)/shard_map/all_to_all | solution.py:218
  523.1 28.4 %all-to-all-done.3 = bf16[64,3,2048]{2,1,0:T(4,128)(2,1)} async-done(((bf16[64,3,2048]{2,1,0:T(4,128)(2,1)}), bf16[64,3,2048]{2,1,0:T(4,128)(2,1)}, u32[]{:S(2)}, u32[]{:S(2)}) %all-to-all-start.3) | async-done | bytes 786464 | tf_op jit(solution)/shard_map/all_to_all | solution.py:218
  551.5 3.2 reshape.153
  554.7 3.5 gather_fusion.1
  558.2 2.7 reshape.154
  560.9 2.8 multiply_reduce_fusion
  563.7 1.8 add_convert_fusion
  (121 shorter events, 18.7 us)
Async XLA Ops:
  6.5 456.1 %copy-start = (bf16[1,768,2048]{2,1,0:T(8,128)(2,1)S(1)}, bf16[1,768,2048]{2,1,0:T(8,128)(2,1)}, u32[]{:S(2)}) copy-start(bf16[1,768,2048]{2,1,0:T(8,128)(2,1)} %param.25) | copy-start | bytes 9437188
  6.5 66.7 %copy-start.7 = (bf16[256,512]{1,0:T(8,128)(2,1)S(1)}, bf16[256,512]{1,0:T(8,128)(2,1)}, u32[]{:S(2)}) copy-start(bf16[256,512]{1,0:T(8,128)(2,1)} %param.15) | copy-start | bytes 786436
  6.5 67.5 %copy-start.10 = (s32[64,2]{0,1:T(2,128)S(1)}, s32[64,2]{0,1:T(2,128)}, u32[]{:S(2)}) copy-start(s32[64,2]{0,1:T(2,128)} %param.21) | copy-start | bytes 1540
  6.5 57.1 %all-gather.9.cloned.1.call-start = ((), (), s32[]{:S(2)}) async-start(), calls=%async_computation.7 | async-start | bytes 2359296 | tf_op jit(solution)/shard_map/all_gather | solution.py:37
  21.3 70.1 %all-gather.11.cloned.1.call-start = ((), (), s32[]{:S(2)}) async-start(), calls=%async_computation.8 | async-start | bytes 6291456 | tf_op jit(solution)/shard_map/all_gather | solution.py:37
  65.2 25.5 %all-to-all-start = ((f32[64,256,8]{1,2,0:T(8,128)}), f32[64,256,8]{1,2,0:T(8,128)}, u32[]{:S(2)}, u32[]{:S(2)}) async-start(f32[64,256,8]{1,2,0:T(8,128)} %broadcast_in_dim.56), calls=%async_computation | async-start | bytes 1048576 | tf_op jit(solution)/shard_map/all_to_all | solution.py:20
  96.0 7.4 %copy-start.8 = (bf16[256,512]{0,1:T(8,128)(2,1)S(1)}, bf16[256,512]{0,1:T(8,128)(2,1)}, u32[]{:S(2)}) copy-start(bf16[256,512]{0,1:T(8,128)(2,1)} %copy.36) | copy-start | bytes 786436
  106.3 1.1 copy-start.5
  109.0 1.4 copy-start.6
  146.8 23.3 %copy-start.3 = (bf16[64,2048]{1,0:T(8,128)(2,1)S(1)}, bf16[64,2048]{1,0:T(8,128)(2,1)}, u32[]{:S(2)}) copy-start(bf16[64,2048]{1,0:T(8,128)(2,1)} %param.18) | copy-start | bytes 786436
  146.8 24.1 %copy-start.9 = (f32[2048]{0:T(1024)S(1)}, f32[2048]{0:T(1024)}, u32[]{:S(2)}) copy-start(f32[2048]{0:T(1024)} %param.20) | copy-start | bytes 24580
  150.2 18.5 %all-to-all-start.1 = ((bf16[4,64,2048]{2,1,0:T(8,128)(2,1)}), bf16[4,64,2048]{2,1,0:T(8,128)(2,1)}, u32[]{:S(2)}, u32[]{:S(2)}) async-start(bf16[4,64,2048]{2,1,0:T(8,128)(2,1)} %bitcast.88), calls=%async_computation.1 | async-start | bytes 2097152 | tf_op jit(solution)/shard_map/all_to_all | solution.py:56
  155.0 279.1 %all-gather.7.cloned.1.call-start = ((), (), s32[]{:S(2)}) async-start(), calls=%async_computation.5 | async-start | bytes 3932160 | tf_op jit(solution)/shard_map/all_gather | solution.py:200
  170.1 0.8 copy-start.1
  397.7 111.6 %reduce-scatter.2.cloned.1.call-start = ((), (), s32[]{:S(2)}) async-start(), calls=%async_computation.6 | async-start | bytes 3932160 | tf_op jit(solution)/shard_map/reduce_scatter | solution.py:210
  449.4 5.6 copy-start.2
  449.4 5.6 copy-start.12
  468.0 55.0 %copy-start.11 = (f32[64,2]{0,1:T(2,128)S(1)}, f32[64,2]{0,1:T(2,128)}, u32[]{:S(2)}) copy-start(f32[64,2]{0,1:T(2,128)} %param.22) | copy-start | bytes 1540
  512.1 39.4 %all-to-all-start.3 = ((bf16[64,3,2048]{2,1,0:T(4,128)(2,1)}), bf16[64,3,2048]{2,1,0:T(4,128)(2,1)}, u32[]{:S(2)}, u32[]{:S(2)}) async-start(bf16[64,3,2048]{2,1,0:T(4,128)(2,1)} %copy.43), calls=%async_computation.4 | async-start | bytes 2097152 | tf_op jit(solution)/shard_map/all_to_all | solution.py:218
  554.7 9.0 %copy-start.4 = (bf16[64,2048]{1,0:T(8,128)(2,1)S(1)}, bf16[64,2048]{1,0:T(8,128)(2,1)}, u32[]{:S(2)}) copy-start(bf16[64,2048]{1,0:T(8,128)(2,1)} %param.18) | copy-start | bytes 786436
Sparse Core Ops, SparseCore 0:
  21.4 42.2 all-gather.8
  65.4 17.5 all-gather.10
  397.8 36.2 all-gather.6
  468.2 41.0 reduce-scatter.1
where the time goes:
time: 578 us; the launch traced here: 572 us
  blocking collectives  232 us (40%)
  waiting for transfers between devices  176 us (30%)
  local copies, waits for them, and re-layouts  74.7 us (13%)
  starting transfers between devices  24 us (4%)
  matrix products  20.8 us (4%)
  loops' own time  18.9 us (3%)
  between operations  13.3 us (2%)
  other arithmetic  12.2 us (2%)
    all_to_all x1, blocking collectives, local(): lax.all_to_all(outgoing, SP, split_axis=0, concat_axis=0, tiled=True)  217 us
    all_gather x2, waiting for transfers between devices, stacked_from(): tiles = lax.all_gather(tiles, axes[k])  42.3 us
    reduce_scatter x1, waiting for transfers between devices, local(): lax.psum_scatter(jnp.einsum('rcf,fd->rcd', row_block, expert_down[0], pre...  41.2 us
    all_gather x1, waiting for transfers between devices, local(): arrived = lax.all_gather(incoming, 'tp', axis=0, tiled=True)  36.2 us
    all_to_all x1, waiting for transfers between devices, local(): lax.all_to_all(summed, SP, split_axis=0, concat_axis=0, tiled=True)  28.4 us
    another operation x1, loops' own time, local(): states = lax.fori_loop(0, length // key_block, one_block, initial)  18.4 us
    slice x32, local copies, waits for them, and re-layouts, one_block(): last_pos = query_set[2][-1]  17.6 us
    all_to_all x1, waiting for transfers between devices, copy_for_each(): return lax.all_to_all(copies, axis, split_axis=0, concat_axis=0, tiled=True)  15.9 us
  transfers between devices with their start and end apart: 7, of which 6 were waited for; matrix products, arithmetic and copies ran while one was open for 1% of the time, Pallas kernels for 0%

commit v1 on v0

v1 whole, which is shorter than its diff:
```python
import functools
import math

import jax
import jax.numpy as jnp
from jax import lax
from jax.experimental import pallas as pl
from jax.experimental.pallas import tpu as pltpu
from jax.sharding import Mesh
from jax.sharding import PartitionSpec as P

SP = ("sp_0", "sp_1", "sp_2")
SP_TP = ("sp_0", "sp_1", "sp_2", "tp")
NORM_EPS = 1e-06
HEAD_SIZE = 64
NEG_FILL = -1e30
LOG2E = math.log2(math.e)
BLOCK = 256
HALF = 128
KEY_ROWS = 96
VALUE_ROWS = 64


def prep_body(kv_ref, gate_ref, out_ref):
    kv = kv_ref[...].astype(jnp.float32).T
    gate = gate_ref[...]
    high = gate.astype(jnp.bfloat16).astype(jnp.float32)
    rest = gate - high
    middle = rest.astype(jnp.bfloat16).astype(jnp.float32)
    low = rest - middle
    gates = jnp.concatenate([high, middle, low, jnp.zeros_like(gate)], axis=0)
    out_ref[...] = jnp.concatenate(
        [kv[:HEAD_SIZE], gates, kv[HEAD_SIZE:]], axis=0
    ).astype(jnp.bfloat16)


def prepare_keys(kv, gate_t):
    return pl.pallas_call(
        prep_body,
        out_shape=jax.ShapeDtypeStruct((KEY_ROWS + VALUE_ROWS, kv.shape[0]), jnp.bfloat16),
        name="prepare_keys",
    )(kv, gate_t)


def attend_body(index_ref, qa_ref, qb_ref, own_ref, other_ref, outa_ref, outb_ref, qt_ref, max_ref, acc_ref, *, blocks, heads):
    columns = heads * HALF
    step = 256
    own_index = index_ref[0]
    core = own_index % 2
    row = lax.broadcasted_iota(jnp.int32, (KEY_ROWS - HEAD_SIZE, columns), 0)
    head = lax.broadcasted_iota(jnp.int32, (KEY_ROWS - HEAD_SIZE, columns), 1) // HALF
    picks = jnp.where((row % heads == head) & (row < 3 * heads), -1.0, 0.0)
    for which, q_ref in ((0, qa_ref), (1, qb_ref)):
        qt = (q_ref[...].astype(jnp.float32) * (HEAD_SIZE**-0.5)).T
        qt = jnp.concatenate(
            [qt[h * HEAD_SIZE : (h + 1) * HEAD_SIZE] for h in range(heads)], axis=1
        )
        qt_ref[which] = jnp.concatenate([qt, picks], axis=0).astype(jnp.bfloat16)
    max_ref[...] = jnp.full(max_ref.shape, NEG_FILL, jnp.float32)
    acc_ref[...] = jnp.zeros(acc_ref.shape, jnp.float32)

    def attend(which, pair, first_row):
        tile = jnp.concatenate([own_ref[pair], other_ref[pair]], axis=1)
        keys = tile[:KEY_ROWS].astype(jnp.float32).T.astype(jnp.bfloat16)
        values = jnp.concatenate(
            [tile[KEY_ROWS:], jnp.ones((16, 2 * BLOCK), jnp.bfloat16)], axis=0
        )
        for at in range(0, columns, step):
            cols = slice(at, at + step)
            scores = jnp.dot(keys, qt_ref[which, :, cols], preferred_element_type=jnp.float32)
            if first_row is not None:
                k = lax.broadcasted_iota(jnp.int32, scores.shape, 0)
                t = lax.broadcasted_iota(jnp.int32, scores.shape, 1) % HALF
                start = jnp.where(k < BLOCK, core * BLOCK, (1 - core) * BLOCK - BLOCK)
                seen = pair * (2 * BLOCK) + start + k <= first_row + t
                scores = jnp.where(seen, scores, NEG_FILL)
            before = max_ref[which, :, cols]
            now = jnp.maximum(before, jnp.max(scores, axis=0, keepdims=True))
            weights = jnp.exp2((scores - now) * LOG2E)
            rescale = jnp.exp2((before - now) * LOG2E)
            max_ref[which, :, cols] = now
            acc_ref[which, :, cols] = acc_ref[which, :, cols] * rescale + jnp.dot(
                values, weights.astype(jnp.bfloat16), preferred_element_type=jnp.float32
            )

    for which, index, first in (
        (0, own_index, own_index * BLOCK),
        (1, blocks - 1 - own_index, (blocks - 1 - own_index) * BLOCK + HALF),
    ):
        last_pair = index // 2

        def full(pair, carry, which=which):
            attend(which, pair, None)
            return carry

        lax.fori_loop(0, last_pair, full, 0)
        attend(which, last_pair, first)

    for which, out_ref in ((0, outa_ref), (1, outb_ref)):
        acc = acc_ref[which]
        out = acc[:VALUE_ROWS] / acc[VALUE_ROWS : VALUE_ROWS + 1]
        out = jnp.concatenate([out[:, h * HALF : (h + 1) * HALF] for h in range(heads)], axis=0)
        out_ref[...] = out.T.astype(out_ref.dtype)


def attend_rows(index, qa, qb, own, other):
    heads = qa.shape[1] // HEAD_SIZE
    blocks = 2 * own.shape[0]
    columns = heads * HALF
    out = jax.ShapeDtypeStruct(qa.shape, jnp.bfloat16)
    vmem = pl.BlockSpec(memory_space=pltpu.VMEM)
    return pl.pallas_call(
        functools.partial(attend_body, blocks=blocks, heads=heads),
        in_specs=[pl.BlockSpec(memory_space=pltpu.SMEM)] + [vmem] * 4,
        out_specs=[vmem] * 2,
        out_shape=[out, out],
        scratch_shapes=[
            pltpu.VMEM((2, KEY_ROWS, columns), jnp.bfloat16),
            pltpu.VMEM((2, 1, columns), jnp.float32),
            pltpu.VMEM((2, VALUE_ROWS + 16, columns), jnp.float32),
        ],
        compiler_params=pltpu.CompilerParams(vmem_limit_bytes=48 * 1024 * 1024),
        name="attend_rows",
    )(index, qa, qb, own, other)


def cut_along(array, dim, devices):
    shape = array.shape
    tiles = array.reshape(*shape[:dim], devices, shape[dim] // devices, *shape[dim + 1 :])
    return jnp.moveaxis(tiles, dim, 0)


def sum_at_owner(array, axis, dim):
    devices = lax.axis_size(axis)
    tiles = lax.all_to_all(cut_along(array, dim, devices), axis, 0, 0, tiled=True)
    return jnp.sum(tiles.astype(jnp.float32), axis=0)


def slot_ranks(chosen, experts):
    onehot = (chosen[..., None] == jnp.arange(experts, dtype=jnp.int32)).astype(jnp.int32)
    earlier = jnp.cumsum(onehot, axis=-2) - onehot
    return jnp.sum(earlier * onehot, axis=-1)


def fill_slots(source_rows, target, slot_total, per_row):
    owner_slot = (
        jnp.zeros((slot_total,), jnp.int32)
        .at[target]
        .set(jnp.arange(1, target.shape[0] + 1, dtype=jnp.int32))
    )
    picked = source_rows[jnp.maximum(owner_slot - 1, 0) // per_row]
    return jnp.where((owner_slot > 0)[:, None], picked, jnp.zeros_like(picked))


def local(
    queries,
    key_value_pairs,
    forget_gate_total,
    residual_in,
    out_weight,
    norm_gain,
    routes,
    route_weight,
    expert_gate,
    expert_up,
    expert_down,
):
    seq_devices = lax.axis_size(SP)
    head_devices = lax.axis_size("tp")
    tok_rows = queries.shape[0]
    index = lax.axis_index(SP).astype(jnp.int32)
    mirror = [(i, seq_devices - 1 - i) for i in range(seq_devices)]
    mirrored_queries = lax.ppermute(queries[HALF:], SP, mirror)
    block = prepare_keys(key_value_pairs, forget_gate_total.T)
    own = lax.all_gather(lax.all_gather(block, "sp_1"), "sp_0")
    own = own.reshape(-1, *block.shape)
    other = lax.ppermute(own, "sp_2", [(0, 1), (1, 0)])
    first, second = attend_rows(index.reshape(1), queries[:HALF], mirrored_queries, own, other)
    second = lax.ppermute(second, SP, mirror)
    attended = jnp.concatenate([first, second], axis=0)
    own_rows = tok_rows // head_devices
    row_block = attended
    mixed_rows = sum_at_owner(
        jnp.dot(row_block, out_weight, preferred_element_type=jnp.float32).astype(jnp.bfloat16),
        "tp",
        0,
    )
    hidden_state = residual_in.astype(jnp.float32) + mixed_rows
    normed = (
        hidden_state
        * lax.rsqrt(jnp.mean(hidden_state * hidden_state, axis=1, keepdims=True) + NORM_EPS)
        * norm_gain
    ).astype(jnp.bfloat16)
    top_count = routes.shape[1]
    capacity = max(2, 3 * own_rows * top_count // (2 * seq_devices))
    model_width = normed.shape[1]
    chosen = routes.reshape(-1)
    target = chosen * capacity + slot_ranks(chosen, seq_devices)
    outgoing = fill_slots(normed, target, seq_devices * capacity, top_count).reshape(
        seq_devices, capacity, model_width
    )
    incoming = lax.all_to_all(outgoing, SP, split_axis=0, concat_axis=0, tiled=True)
    arrived = lax.all_gather(incoming, "tp", axis=0, tiled=True)
    flat_in = arrived.reshape(-1, model_width)
    gate_value = jnp.dot(flat_in, expert_gate[0], preferred_element_type=jnp.float32)
    up_value = jnp.dot(flat_in, expert_up[0], preferred_element_type=jnp.float32)
    hidden_rows = (
        (jax.nn.silu(gate_value) * up_value)
        .astype(jnp.bfloat16)
        .reshape(arrived.shape[0], capacity, -1)
    )
    row_block = hidden_rows
    summed = lax.psum_scatter(
        jnp.einsum(
            "rcf,fd->rcd", row_block, expert_down[0], preferred_element_type=jnp.float32
        ).astype(jnp.bfloat16),
        "tp",
        scatter_dimension=0,
        tiled=True,
    )
    returned = lax.all_to_all(summed, SP, split_axis=0, concat_axis=0, tiled=True)
    picked = returned.reshape(-1, model_width)[target].reshape(own_rows, top_count, model_width)
    combined = jnp.sum(picked.astype(jnp.float32) * route_weight[..., None], axis=1)
    return (hidden_state + combined).astype(jnp.bfloat16)


def solution(mesh):
    finer = Mesh(mesh.devices.reshape(8, 4, 2, mesh.shape["tp"]), ("sp_0", "sp_1", "sp_2", "tp"))
    in_specs = (
        P(SP, "tp"),
        P(SP, "tp"),
        P(SP, "tp"),
        P(SP_TP, None),
        P("tp", None),
        P(),
        P(SP_TP, None),
        P(SP_TP, None),
        P(SP, None, "tp"),
        P(SP, None, "tp"),
        P(SP, "tp", None),
    )
    out_specs = P(SP_TP, None)
    return jax.shard_map(local, mesh=finer, in_specs=in_specs, out_specs=out_specs, check_vma=False)
```

time: 578 us -> 400 us (0.69)
  blocking collectives: 232 us -> 50.9 us
  Pallas kernels: 0 us -> 60.9 us
  local copies, waits for them, and re-layouts: 74.7 us -> 44.4 us
  loops' own time: 18.9 us -> 0 us
    all_to_all x1, blocking collectives: 217 us -> 36.3 us  [local(): lax.all_to_all(outgoing, SP, split_axis=0, concat_axis=0, tiled=True)]
    pallas_call x0 -> x2, Pallas kernels: none -> 60.9 us  [the longest x1 59.2 us: attend_rows(): pl.pallas_call(functools.partial(attend_body, blocks=blocks, heads=heads)...]
    another operation x33 -> x0, loops' own time: 18.9 us -> none  [the longest x1 18.4 us: local(): states = lax.fori_loop(0, length // key_block, one_block, initial)]
    slice x32 -> x1, local copies, waits for them, and re-layouts: 17.6 us -> 1.64 us  [local(): mirrored_queries = lax.ppermute(queries[HALF:], SP, mirror)]
    all_to_all x1 -> x0, waiting for transfers between devices: 15.9 us -> none  [copy_for_each(): return lax.all_to_all(copies, axis, split_axis=0, concat_axis=0, tiled=True)]
    ppermute x0 -> x3, waiting for transfers between devices: none -> 10.9 us  [the longest x1 5.54 us: local(): second = lax.ppermute(second, SP, mirror)]
    ppermute x0 -> x3, starting transfers between devices: none -> 9.15 us  [the longest x1 4.71 us: local(): second = lax.ppermute(second, SP, mirror)]
    all_to_all x1 -> x0, starting transfers between devices: 8 us -> none  [copy_for_each(): return lax.all_to_all(copies, axis, split_axis=0, concat_axis=0, tiled=True)]
  transfers between devices with their start and end apart: 7 -> 8, of which waited for: 6 -> 7; matrix products, arithmetic and copies ran while one was open for 1% -> 1% of each run, Pallas kernels for 0% -> 0%
where the time goes in v1:
time: 400 us; the launch traced here: 397 us
  waiting for transfers between devices  173 us (43%)
  Pallas kernels  60.9 us (15%)
  blocking collectives  50.9 us (13%)
  local copies, waits for them, and re-layouts  44.4 us (11%)
  starting transfers between devices  25.1 us (6%)
  matrix products  18.2 us (5%)
  between operations  13.3 us (3%)
  other arithmetic  11 us (3%)
    pallas_call x1, Pallas kernels, attend_rows(): pl.pallas_call(functools.partial(attend_body, blocks=blocks, heads=heads)...  59.2 us
    all_gather x1, waiting for transfers between devices, local(): own = lax.all_gather(lax.all_gather(block, 'sp_1'), 'sp_0')  43.7 us
    reduce_scatter x1, waiting for transfers between devices, local(): lax.psum_scatter(jnp.einsum('rcf,fd->rcd', row_block, expert_down[0], pre...  41.2 us
    all_gather x1, waiting for transfers between devices, local(): arrived = lax.all_gather(incoming, 'tp', axis=0, tiled=True)  36.4 us
    all_to_all x1, blocking collectives, local(): lax.all_to_all(outgoing, SP, split_axis=0, concat_axis=0, tiled=True)  36.3 us
    all_to_all x1, waiting for transfers between devices, local(): lax.all_to_all(summed, SP, split_axis=0, concat_axis=0, tiled=True)  28.4 us
    all_gather x1, blocking collectives, local(): own = lax.all_gather(lax.all_gather(block, 'sp_1'), 'sp_0')  14.6 us
    all_to_all x1, waiting for transfers between devices, sum_at_owner(): lax.all_to_all(cut_along(array, dim, devices), axis, 0, 0, tiled=True)  12.6 us
  transfers between devices with their start and end apart: 8, of which 7 were waited for; matrix products, arithmetic and copies ran while one was open for 1% of the time, Pallas kernels for 0%

profile of v1, /device:TPU:6, one launch (start us, length us, event | category | flops | bytes accessed | tf_op | source)
XLA Modules:
  0.0 397.0 jit_solution(7936559945799762332)
XLA Ops:
  6.5 1.7 prepare_keys.1
  8.3 14.6 %all-gather = bf16[640,256]{1,0:T(8,128)(2,1)} all-gather(bf16[160,256]{1,0:T(8,128)(2,1)} %prepare_keys.1), channel_id=2, replica_groups=mesh['sp_0'=8,'sp_1'=4,'sp_2'=2,'tp'=4] {'sp_1'}, dimensions={0}, use_global_device_ids=true | all-gather | bytes 409600 | tf_op jit(solution)/shard_map/all_gather | solution.py:175
  22.9 43.7 %all-gather.7.cloned.1.call-done.own_ref = bf16[32,160,256]{2,1,0:T(8,128)(2,1)} async-done(((bf16[4,160,256]{2,1,0:T(8,128)(2,1)}), bf16[32,160,256]{2,1,0:T(8,128)(2,1)}) %all-gather.7.cloned.1.call-update) | async-done | bytes 2621456 | tf_op jit(solution)/shard_map/all_gather | solution.py:175
  66.6 1.6 fusion.16
  68.3 4.4 %collective-permute-start = (bf16[128,512]{1,0:T(8,128)(2,1)}, bf16[128,512]{1,0:T(8,128)(2,1)S(1)}, u32[]{:S(2)}, u32[]{:S(2)}) collective-permute-start(bf16[128,512]{1,0:T(8,128)(2,1)} %get-tuple-element.9), channel_id=1, source_target_pairs={{0,252},{4,248},{8,244},{12,240},{16,236},{20,232},{24,228},{28,22... | collective-permute-start | bytes 393224 | tf_op jit(solution)/shard_map/ppermute | solution.py:173
  72.7 0.8 copy.22
  73.5 0.1 eq.15
  73.6 0.7 fusion.11
  74.3 5.4 %collective-permute-done.qb_ref = bf16[128,512]{1,0:T(8,128)(2,1)S(1)} collective-permute-done((bf16[128,512]{1,0:T(8,128)(2,1)}, bf16[128,512]{1,0:T(8,128)(2,1)S(1)}, u32[]{:S(2)}, u32[]{:S(2)}) %collective-permute-start) | collective-permute-done | bytes 131104 | tf_op jit(solution)/shard_map/ppermute | solution.py:173
  79.7 1.7 copy-done.1
  81.5 59.2 %attend_rows.1 = (bf16[128,512]{1,0:T(8,128)(2,1)S(1)}, bf16[128,512]{1,0:T(8,128)(2,1)}) custom-call(s32[1]{0:T(128)} %bitcast.index_ref, bf16[128,512]{1,0:T(8,128)(2,1)S(1)} %get-tuple-element.10.qa_ref, bf16[128,512]{1,0:T(8,128)(2,1)S(1)} %collective-permute-done.qb_ref, bf16[32,160,256]{2,1,0:T(8,128)(2,1)S(1)} %copy-done.1, ...), custom_call_target="tpu_custom_call" | custom-call | tf_op jit(solution)/shard_map/attend_rows/pallas_call | solution.py:112
  140.6 4.7 %collective-permute-start.2 = (bf16[128,512]{1,0:T(8,128)(2,1)}, bf16[128,512]{1,0:T(8,128)(2,1)S(1)}, u32[]{:S(2)}, u32[]{:S(2)}) collective-permute-start(bf16[128,512]{1,0:T(8,128)(2,1)} %get-tuple-element.8), channel_id=1, source_target_pairs={{0,252},{4,248},{8,244},{12,240},{16,236},{20,232},{24,228},{28,22... | collective-permute-start | bytes 393224 | tf_op jit(solution)/shard_map/ppermute | solution.py:179
  145.3 1.0 reduce_window_sum.11
  146.3 0.2 select_reduce_fusion
  146.5 5.5 %collective-permute-done.2 = bf16[128,512]{1,0:T(8,128)(2,1)S(1)} collective-permute-done((bf16[128,512]{1,0:T(8,128)(2,1)}, bf16[128,512]{1,0:T(8,128)(2,1)S(1)}, u32[]{:S(2)}, u32[]{:S(2)}) %collective-permute-start.2) | collective-permute-done | bytes 131104 | tf_op jit(solution)/shard_map/ppermute | solution.py:179
  152.1 3.3 convolution_convert_fusion.1
  155.4 4.9 %all-to-all-start = ((bf16[4,64,2048]{2,1,0:T(8,128)(2,1)}), bf16[4,64,2048]{2,1,0:T(8,128)(2,1)}, u32[]{:S(2)}, u32[]{:S(2)}) async-start(bf16[4,64,2048]{2,1,0:T(8,128)(2,1)} %bitcast.25), calls=%async_computation | async-start | bytes 2097152 | tf_op jit(solution)/shard_map/all_to_all | solution.py:135
  160.3 0.1 copy.21
  160.4 0.1 mul.63
  160.6 1.0 scatter_custom_fusion
  161.6 0.1 broadcast_in_dim.14
  161.8 12.6 %all-to-all-done = bf16[4,64,2048]{2,1,0:T(8,128)(2,1)} async-done(((bf16[4,64,2048]{2,1,0:T(8,128)(2,1)}), bf16[4,64,2048]{2,1,0:T(8,128)(2,1)}, u32[]{:S(2)}, u32[]{:S(2)}) %all-to-all-start) | async-done | bytes 1048608 | tf_op jit(solution)/shard_map/all_to_all | solution.py:135
  174.4 1.4 convert_reduce_fusion
  175.8 0.2 multiply_reduce_fusion.1
  176.0 0.6 copy-done.2
  176.6 1.1 multiply_convert_fusion.1
  177.7 2.1 gather_fusion
  179.8 3.3 gather.9
  183.0 1.8 broadcast_select_fusion
  184.8 36.3 %all_to_all.15 = bf16[64,3,2048]{2,1,0:T(4,128)(2,1)S(1)} all-to-all(bf16[64,3,2048]{2,1,0:T(4,128)(2,1)S(1)} %broadcast_select_fusion), channel_id=1, replica_groups=mesh['sp_0'=8,'sp_1'=4,'sp_2'=2,'tp'=4] {'sp_0','sp_1','sp_2'}, dimensions={0} | all-to-all | bytes 1572864 | tf_op jit(solution)/shard_map/all_to_all | solution.py:202
  221.1 1.5 copy.23
  222.6 36.4 %all-gather.5.cloned.1.call-done = bf16[256,3,2048]{2,0,1:T(8,128)(2,1)} async-done(((bf16[64,3,2048]{2,0,1:T(8,128)(2,1)}), bf16[256,3,2048]{2,0,1:T(8,128)(2,1)}) %all-gather.5.cloned.1.call-update) | async-done | bytes 3145744 | tf_op jit(solution)/shard_map/all_gather | solution.py:203
  259.0 6.5 %copy.24 = bf16[256,3,2048]{2,1,0:T(4,128)(2,1)} copy(bf16[256,3,2048]{2,0,1:T(8,128)(2,1)} %all-gather.5.cloned.1.call-done) | data formatting | bytes 6291456 | tf_op jit(solution)/shard_map/all_gather | solution.py:203
  265.5 8.8 %reshape.72 = bf16[768,2048]{1,0:T(8,128)(2,1)} reshape(bf16[256,3,2048]{2,1,0:T(4,128)(2,1)} %copy.24) | data formatting | bytes 6291456 | tf_op jit(solution)/shard_map/reshape | solution.py:204
  274.3 5.6 %fusion.1 = f32[768,768]{1,0:T(8,128)S(1)} fusion(bf16[768,2048]{1,0:T(8,128)(2,1)} %reshape.72, bf16[1,2048,768]{2,1,0:T(8,128)(2,1)} %param.20), kind=kOutput, calls=%fused_computation.5 | convolution fusion | flops 2415919104 | bytes 8650752 | tf_op jit(solution)/shard_map/dot_general | solution.py:206
  279.9 3.9 multiply_convert_fusion
  283.8 3.7 reshape.73
  287.6 5.4 %convolution_convert_fusion = bf16[256,3,2048]{2,0,1:T(8,128)(2,1)} fusion(bf16[1,768,2048]{2,1,0:T(8,128)(2,1)S(1)} %copy-done, bf16[256,3,768]{2,1,0:T(4,128)(2,1)} %reshape.73), kind=kOutput, calls=%fused_computation.3 | convolution fusion | flops 2417491968 | bytes 7471104 | tf_op jit(solution)/shard_map/rcf,fd->rcd/dot_general | solution.py:214
  293.0 41.2 %reduce-scatter.2.cloned.1.call-done = bf16[64,3,2048]{2,0,1:T(8,128)(2,1)} async-done(((bf16[256,3,2048]{2,0,1:T(8,128)(2,1)}), bf16[64,3,2048]{2,0,1:T(8,128)(2,1)}) %reduce-scatter.2.cloned.1.call-update) | async-done | bytes 786448 | tf_op jit(solution)/shard_map/reduce_scatter | solution.py:213
  334.1 2.8 copy.26
  337.0 11.0 %all-to-all-start.2 = ((bf16[64,3,2048]{2,1,0:T(4,128)(2,1)}), bf16[64,3,2048]{2,1,0:T(4,128)(2,1)}, u32[]{:S(2)}, u32[]{:S(2)}) async-start(bf16[64,3,2048]{2,1,0:T(4,128)(2,1)} %copy.26), calls=%async_computation.3 | async-start | bytes 2097152 | tf_op jit(solution)/shard_map/all_to_all | solution.py:221
  348.0 0.1 copy.27
  348.1 28.4 %all-to-all-done.2 = bf16[64,3,2048]{2,1,0:T(4,128)(2,1)} async-done(((bf16[64,3,2048]{2,1,0:T(4,128)(2,1)}), bf16[64,3,2048]{2,1,0:T(4,128)(2,1)}, u32[]{:S(2)}, u32[]{:S(2)}) %all-to-all-start.2) | async-done | bytes 786464 | tf_op jit(solution)/shard_map/all_to_all | solution.py:221
  376.4 3.2 reshape.74
  379.6 3.5 gather_fusion.1
  383.1 2.7 reshape.75
  385.8 2.8 multiply_reduce_fusion
  388.6 1.8 add_convert_fusion
  (34 shorter events, 0.2 us)
Async XLA Ops:
  6.5 281.0 %copy-start = (bf16[1,768,2048]{2,1,0:T(8,128)(2,1)S(1)}, bf16[1,768,2048]{2,1,0:T(8,128)(2,1)}, u32[]{:S(2)}) copy-start(bf16[1,768,2048]{2,1,0:T(8,128)(2,1)} %param.21) | copy-start | bytes 9437188
  6.5 60.1 %all-gather.7.cloned.1.call-start = ((), (), s32[]{:S(2)}) async-start(), calls=%async_computation.6 | async-start | bytes 2949120 | tf_op jit(solution)/shard_map/all_gather | solution.py:175
  66.6 13.1 %collective-permute-start.1 = (bf16[32,160,256]{2,1,0:T(8,128)(2,1)}, bf16[32,160,256]{2,1,0:T(8,128)(2,1)}, u32[]{:S(2)}, u32[]{:S(2)}) collective-permute-start(bf16[32,160,256]{2,1,0:T(8,128)(2,1)} %all-gather.7.cloned.1.call-done.own_ref), channel_id=1, source_target_pairs={{0,4},{4,0},{1,5},{5,1},{2,6},{6,2},{3,7},{7,3},{8,12},{12,8},{9,1... | collective-permute-start | bytes 7864328 | tf_op jit(solution)/shard_map/ppermute | solution.py:177
  68.3 11.4 %collective-permute-start = (bf16[128,512]{1,0:T(8,128)(2,1)}, bf16[128,512]{1,0:T(8,128)(2,1)S(1)}, u32[]{:S(2)}, u32[]{:S(2)}) collective-permute-start(bf16[128,512]{1,0:T(8,128)(2,1)} %get-tuple-element.9), channel_id=1, source_target_pairs={{0,252},{4,248},{8,244},{12,240},{16,236},{20,232},{24,228},{28,22... | collective-permute-start | bytes 393224 | tf_op jit(solution)/shard_map/ppermute | solution.py:173
  79.7 1.7 copy-start.1
  81.5 63.9 %copy-start.7 = (s32[64,2]{0,1:T(2,128)S(1)}, s32[64,2]{0,1:T(2,128)}, u32[]{:S(2)}) copy-start(s32[64,2]{0,1:T(2,128)} %param.17) | copy-start | bytes 1540
  140.6 11.4 %collective-permute-start.2 = (bf16[128,512]{1,0:T(8,128)(2,1)}, bf16[128,512]{1,0:T(8,128)(2,1)S(1)}, u32[]{:S(2)}, u32[]{:S(2)}) collective-permute-start(bf16[128,512]{1,0:T(8,128)(2,1)} %get-tuple-element.8), channel_id=1, source_target_pairs={{0,252},{4,248},{8,244},{12,240},{16,236},{20,232},{24,228},{28,22... | collective-permute-start | bytes 393224 | tf_op jit(solution)/shard_map/ppermute | solution.py:179
  155.4 20.4 %copy-start.4 = (bf16[64,2048]{1,0:T(8,128)(2,1)S(1)}, bf16[64,2048]{1,0:T(8,128)(2,1)}, u32[]{:S(2)}) copy-start(bf16[64,2048]{1,0:T(8,128)(2,1)} %param.14) | copy-start | bytes 786436
  155.4 21.2 %copy-start.6 = (f32[2048]{0:T(1024)S(1)}, f32[2048]{0:T(1024)}, u32[]{:S(2)}) copy-start(f32[2048]{0:T(1024)} %param.16) | copy-start | bytes 24580
  155.4 19.0 %all-to-all-start = ((bf16[4,64,2048]{2,1,0:T(8,128)(2,1)}), bf16[4,64,2048]{2,1,0:T(8,128)(2,1)}, u32[]{:S(2)}, u32[]{:S(2)}) async-start(bf16[4,64,2048]{2,1,0:T(8,128)(2,1)} %bitcast.25), calls=%async_computation | async-start | bytes 2097152 | tf_op jit(solution)/shard_map/all_to_all | solution.py:135
  160.3 98.7 %all-gather.5.cloned.1.call-start = ((), (), s32[]{:S(2)}) async-start(), calls=%async_computation.4 | async-start | bytes 3932160 | tf_op jit(solution)/shard_map/all_gather | solution.py:203
  175.8 0.8 copy-start.2
  222.5 111.6 %reduce-scatter.2.cloned.1.call-start = ((), (), s32[]{:S(2)}) async-start(), calls=%async_computation.5 | async-start | bytes 3932160 | tf_op jit(solution)/shard_map/reduce_scatter | solution.py:213
  274.3 5.6 %copy-start.3 = (bf16[768,2048]{1,0:T(8,128)(2,1)S(1)}, bf16[768,2048]{1,0:T(8,128)(2,1)}, u32[]{:S(2)}) copy-start(bf16[768,2048]{1,0:T(8,128)(2,1)} %reshape.72) | copy-start | bytes 9437188
  274.3 5.6 %copy-start.9 = (bf16[1,2048,768]{2,1,0:T(8,128)(2,1)S(1)}, bf16[1,2048,768]{2,1,0:T(8,128)(2,1)}, u32[]{:S(2)}) copy-start(bf16[1,2048,768]{2,1,0:T(8,128)(2,1)} %param.19) | copy-start | bytes 9437188
  293.0 55.0 %copy-start.8 = (f32[64,2]{0,1:T(2,128)S(1)}, f32[64,2]{0,1:T(2,128)}, u32[]{:S(2)}) copy-start(f32[64,2]{0,1:T(2,128)} %param.18) | copy-start | bytes 1540
  337.0 39.4 %all-to-all-start.2 = ((bf16[64,3,2048]{2,1,0:T(4,128)(2,1)}), bf16[64,3,2048]{2,1,0:T(4,128)(2,1)}, u32[]{:S(2)}, u32[]{:S(2)}) async-start(bf16[64,3,2048]{2,1,0:T(4,128)(2,1)} %copy.26), calls=%async_computation.3 | async-start | bytes 2097152 | tf_op jit(solution)/shard_map/all_to_all | solution.py:221
  383.1 5.5 %copy-start.5 = (bf16[64,2048]{1,0:T(8,128)(2,1)S(1)}, bf16[64,2048]{1,0:T(8,128)(2,1)}, u32[]{:S(2)}) copy-start(bf16[64,2048]{1,0:T(8,128)(2,1)} %param.14) | copy-start | bytes 786436
Sparse Core Ops, SparseCore 0:
  23.1 43.5 all-gather.6
  222.7 36.2 all-gather.4
  293.1 41.0 reduce-scatter.1

commit v2 on v1

--- a/solution.py
+++ b/solution.py
@@ -124,32 +124,69 @@
     )(index, qa, qb, own, other)
 
 
-def cut_along(array, dim, devices):
-    shape = array.shape
-    tiles = array.reshape(*shape[:dim], devices, shape[dim] // devices, *shape[dim + 1 :])
-    return jnp.moveaxis(tiles, dim, 0)
-
-
-def sum_at_owner(array, axis, dim):
-    devices = lax.axis_size(axis)
-    tiles = lax.all_to_all(cut_along(array, dim, devices), axis, 0, 0, tiled=True)
-    return jnp.sum(tiles.astype(jnp.float32), axis=0)
-
-
-def slot_ranks(chosen, experts):
-    onehot = (chosen[..., None] == jnp.arange(experts, dtype=jnp.int32)).astype(jnp.int32)
-    earlier = jnp.cumsum(onehot, axis=-2) - onehot
-    return jnp.sum(earlier * onehot, axis=-1)
-
-
-def fill_slots(source_rows, target, slot_total, per_row):
-    owner_slot = (
-        jnp.zeros((slot_total,), jnp.int32)
-        .at[target]
-        .set(jnp.arange(1, target.shape[0] + 1, dtype=jnp.int32))
-    )
-    picked = source_rows[jnp.maximum(owner_slot - 1, 0) // per_row]
-    return jnp.where((owner_slot > 0)[:, None], picked, jnp.zeros_like(picked))
+def routing(routes_ref, experts):
+    rows = routes_ref.shape[0]
+    lanes = lax.broadcasted_iota(jnp.int32, (rows, experts), 1)
+    first = (routes_ref[:, 0:1] == lanes).astype(jnp.float32)
+    second = (routes_ref[:, 1:2] == lanes).astype(jnp.float32)
+    named = first + second
+    above = lax.broadcasted_iota(jnp.int32, (rows, rows), 1) < lax.broadcasted_iota(
+        jnp.int32, (rows, rows), 0
+    )
+    earlier = jnp.dot(
+        above.astype(jnp.bfloat16), named.astype(jnp.bfloat16), preferred_element_type=jnp.float32
+    )
+    return first, second, named, earlier
+
+
+def dispatch_body(parts_ref, residual_ref, gain_ref, routes_ref, hidden_ref, slots_ref, *, capacity):
+    mixed = jnp.sum(parts_ref[...].astype(jnp.float32), axis=0)
+    hidden = residual_ref[...].astype(jnp.float32) + mixed
+    hidden_ref[...] = hidden
+    scale = lax.rsqrt(jnp.mean(hidden * hidden, axis=1, keepdims=True) + NORM_EPS)
+    normed = (hidden * scale * gain_ref[...]).astype(jnp.bfloat16)
+    experts = slots_ref.shape[1]
+    _, _, named, earlier = routing(routes_ref, experts)
+    for slot in range(capacity):
+        chosen = jnp.where(earlier == slot, named, 0.0).T.astype(jnp.bfloat16)
+        slots_ref[slot] = jnp.dot(chosen, normed, preferred_element_type=jnp.float32).astype(
+            jnp.bfloat16
+        )
+
+
+def dispatch(parts, residual, gain, routes, experts, capacity):
+    rows, width = residual.shape
+    return pl.pallas_call(
+        functools.partial(dispatch_body, capacity=capacity),
+        out_shape=[
+            jax.ShapeDtypeStruct((rows, width), jnp.float32),
+            jax.ShapeDtypeStruct((capacity, experts, width), jnp.bfloat16),
+        ],
+        name="dispatch",
+    )(parts, residual, gain.reshape(1, width), routes)
+
+
+def combine_body(returned_ref, hidden_ref, routes_ref, weight_ref, out_ref):
+    capacity, experts, _ = returned_ref.shape
+    first, second, _, earlier = routing(routes_ref, experts)
+    weight = first * weight_ref[:, 0:1] + second * weight_ref[:, 1:2]
+    total = hidden_ref[...]
+    for slot in range(capacity):
+        rest = jnp.where(earlier == slot, weight, 0.0)
+        rows = returned_ref[slot]
+        for _ in range(3):
+            piece = rest.astype(jnp.bfloat16)
+            rest = rest - piece.astype(jnp.float32)
+            total = total + jnp.dot(piece, rows, preferred_element_type=jnp.float32)
+    out_ref[...] = total.astype(jnp.bfloat16)
+
+
+def combine(returned, hidden, routes, route_weight):
+    return pl.pallas_call(
+        combine_body,
+        out_shape=jax.ShapeDtypeStruct(hidden.shape, jnp.bfloat16),
+        name="combine",
+    )(returned, hidden, routes, route_weight)
 
 
 def local(
@@ -167,61 +204,69 @@
 ):
     seq_devices = lax.axis_size(SP)
     head_devices = lax.axis_size("tp")
-    tok_rows = queries.shape[0]
     index = lax.axis_index(SP).astype(jnp.int32)
     mirror = [(i, seq_devices - 1 - i) for i in range(seq_devices)]
+    up = [(i, (i + 1) % head_devices) for i in range(head_devices)]
+    down = [(i, (i - 1) % head_devices) for i in range(head_devices)]
+
+    def neighbours(array):
+        return lax.ppermute(array, "tp", up), lax.ppermute(array, "tp", down)
+
+    def opposite(before, after):
+        half = before.shape[0] // 2
+        return jnp.concatenate(
+            [lax.ppermute(before[:half], "tp", up), lax.ppermute(after[half:], "tp", down)], axis=0
+        )
+
     mirrored_queries = lax.ppermute(queries[HALF:], SP, mirror)
     block = prepare_keys(key_value_pairs, forget_gate_total.T)
     own = lax.all_gather(lax.all_gather(block, "sp_1"), "sp_0")
     own = own.reshape(-1, *block.shape)
     other = lax.ppermute(own, "sp_2", [(0, 1), (1, 0)])
+    down_own = expert_down[0]
+    down_before, down_after = neighbours(down_own)
     first, second = attend_rows(index.reshape(1), queries[:HALF], mirrored_queries, own, other)
+    down_before, down_after, first, second = lax.optimization_barrier(
+        (down_before, down_after, first, second)
+    )
+    down_across = opposite(down_before, down_after)
     second = lax.ppermute(second, SP, mirror)
     attended = jnp.concatenate([first, second], axis=0)
-    own_rows = tok_rows // head_devices
-    row_block = attended
-    mixed_rows = sum_at_owner(
-        jnp.dot(row_block, out_weight, preferred_element_type=jnp.float32).astype(jnp.bfloat16),
-        "tp",
-        0,
-    )
-    hidden_state = residual_in.astype(jnp.float32) + mixed_rows
-    normed = (
-        hidden_state
-        * lax.rsqrt(jnp.mean(hidden_state * hidden_state, axis=1, keepdims=True) + NORM_EPS)
-        * norm_gain
-    ).astype(jnp.bfloat16)
-    top_count = routes.shape[1]
+    partial = jnp.dot(attended, out_weight, preferred_element_type=jnp.float32).astype(jnp.bfloat16)
+    parts = lax.all_to_all(
+        partial.reshape(head_devices, -1, partial.shape[1]), "tp", 0, 0, tiled=True
+    )
+    own_rows, top_count = routes.shape
     capacity = max(2, 3 * own_rows * top_count // (2 * seq_devices))
-    model_width = normed.shape[1]
-    chosen = routes.reshape(-1)
-    target = chosen * capacity + slot_ranks(chosen, seq_devices)
-    outgoing = fill_slots(normed, target, seq_devices * capacity, top_count).reshape(
-        seq_devices, capacity, model_width
-    )
-    incoming = lax.all_to_all(outgoing, SP, split_axis=0, concat_axis=0, tiled=True)
-    arrived = lax.all_gather(incoming, "tp", axis=0, tiled=True)
-    flat_in = arrived.reshape(-1, model_width)
-    gate_value = jnp.dot(flat_in, expert_gate[0], preferred_element_type=jnp.float32)
-    up_value = jnp.dot(flat_in, expert_up[0], preferred_element_type=jnp.float32)
-    hidden_rows = (
-        (jax.nn.silu(gate_value) * up_value)
-        .astype(jnp.bfloat16)
-        .reshape(arrived.shape[0], capacity, -1)
-    )
-    row_block = hidden_rows
-    summed = lax.psum_scatter(
-        jnp.einsum(
-            "rcf,fd->rcd", row_block, expert_down[0], preferred_element_type=jnp.float32
-        ).astype(jnp.bfloat16),
-        "tp",
-        scatter_dimension=0,
-        tiled=True,
-    )
-    returned = lax.all_to_all(summed, SP, split_axis=0, concat_axis=0, tiled=True)
-    picked = returned.reshape(-1, model_width)[target].reshape(own_rows, top_count, model_width)
-    combined = jnp.sum(picked.astype(jnp.float32) * route_weight[..., None], axis=1)
-    return (hidden_state + combined).astype(jnp.bfloat16)
+    hidden_state, slots = dispatch(
+        parts, residual_in, norm_gain, routes, seq_devices, capacity
+    )
+    width = slots.shape[2]
+    incoming = lax.all_to_all(slots.transpose(1, 0, 2), SP, 0, 0, tiled=True)
+    rows_own = incoming.transpose(1, 0, 2).reshape(-1, width)
+
+    def units(rows):
+        gate_value = jnp.dot(rows, expert_gate[0], preferred_element_type=jnp.float32)
+        up_value = jnp.dot(rows, expert_up[0], preferred_element_type=jnp.float32)
+        return (jax.nn.silu(gate_value) * up_value).astype(jnp.bfloat16)
+
+    rows_before, rows_after = neighbours(rows_own)
+    units_own = units(rows_own)
+    rows_across = opposite(rows_before, rows_after)
+    units_from_before = lax.ppermute(units(rows_after), "tp", up)
+    units_from_after = lax.ppermute(units(rows_before), "tp", down)
+    across = [(i, (i + 2) % head_devices) for i in range(head_devices)]
+    units_from_across = lax.ppermute(units(rows_across), "tp", across)
+    summed = jnp.dot(units_own, down_own, preferred_element_type=jnp.float32)
+    for got, weight in (
+        (units_from_before, down_before),
+        (units_from_after, down_after),
+        (units_from_across, down_across),
+    ):
+        summed = summed + jnp.dot(got, weight, preferred_element_type=jnp.float32)
+    leaving = summed.astype(jnp.bfloat16).reshape(capacity, seq_devices, width).transpose(1, 0, 2)
+    returned = lax.all_to_all(leaving, SP, 0, 0, tiled=True).transpose(1, 0, 2)
+    return combine(returned, hidden_state, routes, route_weight)
 
 
 def solution(mesh):

time: 400 us -> 343 us (0.86)
  blocking collectives: 50.9 us -> 14.6 us
  local copies, waits for them, and re-layouts: 44.4 us -> 21.7 us
  waiting for transfers between devices: 173 us -> 151 us
  starting transfers between devices: 25.1 us -> 45.6 us
  matrix products: 18.2 us -> 29.4 us
  other arithmetic: 11 us -> 0 us
  Pallas kernels: 60.9 us -> 66.3 us
    reduce_scatter x1 -> x0, waiting for transfers between devices: 41.2 us -> none  [local(): lax.psum_scatter(jnp.einsum('rcf,fd->rcd', row_block, expert_down[0], pre...]
    all_gather x1 -> x0, waiting for transfers between devices: 36.4 us -> none  [local(): arrived = lax.all_gather(incoming, 'tp', axis=0, tiled=True)]
    all_to_all x1 -> x0, blocking collectives: 36.3 us -> none  [local(): lax.all_to_all(outgoing, SP, split_axis=0, concat_axis=0, tiled=True)]
    ppermute x0 -> x11, waiting for transfers between devices: none -> 33.3 us  [the longest x4 18.5 us: neighbours(): return (lax.ppermute(array, 'tp', up), lax.ppermute(array, 'tp', down))]
    all_to_all x2 -> x3, waiting for transfers between devices: 41 us -> 62.5 us  [the longest x1 28 us: local(): returned = lax.all_to_all(leaving, SP, 0, 0, tiled=True).transpose(1, 0, 2)]
    reshape x3 -> x1, local copies, waits for them, and re-layouts: 15.7 us -> 1.65 us  [local(): summed.astype(jnp.bfloat16).reshape(capacity, seq_devices, width)]
    ppermute x0 -> x11, starting transfers between devices: none -> 12.9 us  [the longest x4 5.34 us: neighbours(): return (lax.ppermute(array, 'tp', up), lax.ppermute(array, 'tp', down))]
    dot_general x4 -> x12, matrix products: 18.2 us -> 29.4 us  [the longest x4 9.38 us: units(): jnp.dot(rows, expert_gate[0], preferred_element_type=jnp.float32)]
  transfers between devices with their start and end apart: 8 -> 18, of which waited for: 7 -> 9; matrix products, arithmetic and copies ran while one was open for 1% -> 11% of each run, Pallas kernels for 0% -> 17%
where the time goes in v2:
time: 343 us; the launch traced here: 342 us
  waiting for transfers between devices  151 us (44%)
  Pallas kernels  66.3 us (19%)
  starting transfers between devices  45.6 us (13%)
  matrix products  29.4 us (9%)
  local copies, waits for them, and re-layouts  21.7 us (6%)
  blocking collectives  14.6 us (4%)
  between operations  13.6 us (4%)
    pallas_call x1, Pallas kernels, attend_rows(): pl.pallas_call(functools.partial(attend_body, blocks=blocks, heads=heads)...  58.6 us
    all_gather x1, waiting for transfers between devices, local(): own = lax.all_gather(lax.all_gather(block, 'sp_1'), 'sp_0')  41.6 us
    all_to_all x1, waiting for transfers between devices, local(): returned = lax.all_to_all(leaving, SP, 0, 0, tiled=True).transpose(1, 0, 2)  28 us
    all_to_all x1, waiting for transfers between devices, local(): incoming = lax.all_to_all(slots.transpose(1, 0, 2), SP, 0, 0, tiled=True)  21.1 us
    ppermute x4, waiting for transfers between devices, neighbours(): return (lax.ppermute(array, 'tp', up), lax.ppermute(array, 'tp', down))  18.5 us
    all_gather x1, blocking collectives, local(): own = lax.all_gather(lax.all_gather(block, 'sp_1'), 'sp_0')  14.6 us
    all_to_all x1, waiting for transfers between devices, local(): lax.all_to_all(partial.reshape(head_devices, -1, partial.shape[1]), 'tp',...  13.4 us
    all_to_all x1, starting transfers between devices, local(): returned = lax.all_to_all(leaving, SP, 0, 0, tiled=True).transpose(1, 0, 2)  10.9 us
  transfers between devices with their start and end apart: 18, of which 9 were waited for; matrix products, arithmetic and copies ran while one was open for 11% of the time, Pallas kernels for 17%

profile of v2, /device:TPU:6, one launch (start us, length us, event | category | flops | bytes accessed | tf_op | source)
XLA Modules:
  0.0 342.1 jit_solution(15104915279528505728)
XLA Ops:
  6.5 1.7 prepare_keys.1
  8.3 14.6 %all-gather = bf16[640,256]{1,0:T(8,128)(2,1)} all-gather(bf16[160,256]{1,0:T(8,128)(2,1)} %prepare_keys.1), channel_id=2, replica_groups=mesh['sp_0'=8,'sp_1'=4,'sp_2'=2,'tp'=4] {'sp_1'}, dimensions={0}, use_global_device_ids=true | all-gather | bytes 409600 | tf_op jit(solution)/shard_map/all_gather | solution.py:223
  22.9 1.0 collective-permute-start
  23.9 1.1 collective-permute-start.1
  25.0 41.6 %all-gather.4.cloned.1.call-done.own_ref = bf16[32,160,256]{2,1,0:T(8,128)(2,1)} async-done(((bf16[4,160,256]{2,1,0:T(8,128)(2,1)}), bf16[32,160,256]{2,1,0:T(8,128)(2,1)}) %all-gather.4.cloned.1.call-update) | async-done | bytes 2621456 | tf_op jit(solution)/shard_map/all_gather | solution.py:223
  66.6 1.0 fusion.44
  67.6 4.5 %collective-permute-start.2 = (bf16[128,512]{1,0:T(8,128)(2,1)S(1)}, bf16[128,512]{1,0:T(8,128)(2,1)S(1)}, u32[]{:S(2)}, u32[]{:S(2)}) collective-permute-start(bf16[128,512]{1,0:T(8,128)(2,1)S(1)} %get-tuple-element.21), channel_id=1, source_target_pairs={{0,252},{4,248},{8,244},{12,240},{16,236},{20,232},{24,228},{28,22... | collective-permute-start | bytes 393224 | tf_op jit(solution)/shard_map/ppermute | solution.py:221
  72.1 6.8 %collective-permute-done.2.qb_ref = bf16[128,512]{1,0:T(8,128)(2,1)S(1)} collective-permute-done((bf16[128,512]{1,0:T(8,128)(2,1)S(1)}, bf16[128,512]{1,0:T(8,128)(2,1)S(1)}, u32[]{:S(2)}, u32[]{:S(2)}) %collective-permute-start.2) | collective-permute-done | bytes 131104 | tf_op jit(solution)/shard_map/ppermute | solution.py:221
  78.9 1.7 copy-done.1
  80.7 58.6 %attend_rows.1 = (bf16[128,512]{1,0:T(8,128)(2,1)S(1)}, bf16[128,512]{1,0:T(8,128)(2,1)S(1)}) custom-call(s32[1]{0:T(128)} %bitcast.1.index_ref, bf16[128,512]{1,0:T(8,128)(2,1)S(1)} %get-tuple-element.22.qa_ref, bf16[128,512]{1,0:T(8,128)(2,1)S(1)} %collective-permute-done.2.qb_ref, bf16[32,160,256]{2,1,0:T(8,128)(2,1)S(1)} %copy-done.1, ...), custom_call_target="tpu_custom_call" | custom-call | tf_op jit(solution)/shard_map/attend_rows/pallas_call | solution.py:112
  139.4 4.5 %collective-permute-start.4 = (bf16[128,512]{1,0:T(8,128)(2,1)S(1)}, bf16[128,512]{1,0:T(8,128)(2,1)S(1)}, u32[]{:S(2)}, u32[]{:S(2)}) collective-permute-start(bf16[128,512]{1,0:T(8,128)(2,1)S(1)} %get-tuple-element.16), channel_id=1, source_target_pairs={{0,252},{4,248},{8,244},{12,240},{16,236},{20,232},{24,228},{28,22... | collective-permute-start | bytes 393224 | tf_op jit(solution)/shard_map/ppermute | solution.py:233
  143.9 6.8 %collective-permute-done.4 = bf16[128,512]{1,0:T(8,128)(2,1)S(1)} collective-permute-done((bf16[128,512]{1,0:T(8,128)(2,1)S(1)}, bf16[128,512]{1,0:T(8,128)(2,1)S(1)}, u32[]{:S(2)}, u32[]{:S(2)}) %collective-permute-start.4) | collective-permute-done | bytes 131104 | tf_op jit(solution)/shard_map/ppermute | solution.py:233
  150.7 1.8 convolution_convert_fusion
  152.5 4.8 %all-to-all-start = ((bf16[4,64,2048]{2,1,0:T(8,128)(2,1)}), bf16[4,64,2048]{2,1,0:T(8,128)(2,1)}, u32[]{:S(2)}, u32[]{:S(2)}) async-start(bf16[4,64,2048]{2,1,0:T(8,128)(2,1)} %bitcast.64), calls=%async_computation | async-start | bytes 2097152 | tf_op jit(solution)/shard_map/all_to_all | solution.py:236
  157.3 0.7 copy.21.routes_ref
  158.0 13.4 %all-to-all-done.parts_ref = bf16[4,64,2048]{2,1,0:T(8,128)(2,1)} async-done(((bf16[4,64,2048]{2,1,0:T(8,128)(2,1)}), bf16[4,64,2048]{2,1,0:T(8,128)(2,1)}, u32[]{:S(2)}, u32[]{:S(2)}) %all-to-all-start) | async-done | bytes 1048608 | tf_op jit(solution)/shard_map/all_to_all | solution.py:236
  171.4 3.0 dispatch.1
  174.3 2.8 copy.22
  177.1 7.9 %all-to-all-start.1 = ((bf16[64,3,2048]{2,1,0:T(4,128)(2,1)}), bf16[64,3,2048]{2,1,0:T(4,128)(2,1)}, u32[]{:S(2)}, u32[]{:S(2)}) async-start(bf16[64,3,2048]{2,1,0:T(4,128)(2,1)} %copy.22), calls=%async_computation.1 | async-start | bytes 2097152 | tf_op jit(solution)/shard_map/all_to_all | solution.py:245
  185.0 2.8 slice.22
  187.8 2.1 collective-permute-start.12
  189.9 2.8 slice.23
  192.6 21.1 %all-to-all-done.1 = bf16[64,3,2048]{2,1,0:T(4,128)(2,1)} async-done(((bf16[64,3,2048]{2,1,0:T(4,128)(2,1)}), bf16[64,3,2048]{2,1,0:T(4,128)(2,1)}, u32[]{:S(2)}, u32[]{:S(2)}) %all-to-all-start.1) | async-done | bytes 786464 | tf_op jit(solution)/shard_map/all_to_all | solution.py:245
  213.7 2.7 copy.23
  216.4 3.2 collective-permute-start.7
  219.7 3.7 %fusion.18 = f32[192,768]{1,0:T(8,128)} fusion(bf16[192,2048]{1,0:T(8,128)(2,1)} %bitcast.8, bf16[1,2048,768]{2,1,0:T(8,128)(2,1)} %param.19), kind=kOutput, calls=%fused_computation.18 | convolution fusion | flops 603979776 | bytes 4521984 | tf_op jit(solution)/shard_map/dot_general | solution.py:249
  223.4 5.1 %fusion.29 = f32[192,2048]{1,0:T(8,128)} fusion(bf16[192,2048]{1,0:T(8,128)(2,1)} %bitcast.8, bf16[1,2048,768]{2,1,0:T(8,128)(2,1)S(1)} %copy-done, f32[192,768]{1,0:T(8,128)} %fusion.18, bf16[1,768,2048]{2,1,0:T(8,128)(2,1)} %param.21), kind=kOutput, calls=%fused_computation.28 | convolution fusion | flops 1208844288 | bytes 9240576 | tf_op jit(solution)/shard_map/dot_general | solution.py:260
  228.6 18.5 %collective-permute-done.5 = bf16[192,2048]{1,0:T(8,128)(2,1)} collective-permute-done((bf16[192,2048]{1,0:T(8,128)(2,1)}, bf16[192,2048]{1,0:T(8,128)(2,1)}, u32[]{:S(2)}, u32[]{:S(2)}) %collective-permute-start.5) | collective-permute-done | bytes 786464 | tf_op jit(solution)/shard_map/ppermute | solution.py:213
  247.0 2.9 fusion.16
  249.9 2.1 multiply_convert_fusion.2
  252.1 1.0 slice.24
  253.2 1.0 slice.25
  254.3 2.1 collective-permute-start.10
  256.4 1.9 fusion.14
  258.3 1.9 multiply_convert_fusion.1
  260.2 8.1 %collective-permute-done.9 = bf16[96,2048]{1,0:T(8,128)(2,1)S(1)} collective-permute-done((bf16[96,2048]{1,0:T(8,128)(2,1)S(1)}, bf16[96,2048]{1,0:T(8,128)(2,1)S(1)}, u32[]{:S(2)}, u32[]{:S(2)}) %collective-permute-start.9) | collective-permute-done | bytes 393248 | tf_op jit(solution)/shard_map/ppermute | solution.py:218
  268.4 0.8 fusion.12
  269.2 0.8 multiply_convert_fusion
  270.0 3.3 collective-permute-start.11
  273.2 2.7 convolution_add_fusion.1
  276.0 6.7 %collective-permute-done.11 = bf16[192,768]{1,0:T(8,128)(2,1)S(1)} collective-permute-done((bf16[192,768]{1,0:T(8,128)(2,1)S(1)}, bf16[192,768]{1,0:T(8,128)(2,1)S(1)}, u32[]{:S(2)}, u32[]{:S(2)}) %collective-permute-start.11) | collective-permute-done | bytes 294944 | tf_op jit(solution)/shard_map/ppermute | solution.py:259
  282.7 2.7 fusion
  285.4 2.8 fusion.21
  288.3 1.7 copy.30
  289.9 10.9 %all-to-all-start.2 = ((bf16[64,3,2048]{2,1,0:T(4,128)(2,1)}), bf16[64,3,2048]{2,1,0:T(4,128)(2,1)}, u32[]{:S(2)}, u32[]{:S(2)}) async-start(bf16[64,3,2048]{2,1,0:T(4,128)(2,1)} %bitcast.63), calls=%async_computation.2 | async-start | bytes 2097152 | tf_op jit(solution)/shard_map/all_to_all | solution.py:268
  301.5 28.0 %all-to-all-done.2 = bf16[64,3,2048]{2,1,0:T(4,128)(2,1)} async-done(((bf16[64,3,2048]{2,1,0:T(4,128)(2,1)}), bf16[64,3,2048]{2,1,0:T(4,128)(2,1)}, u32[]{:S(2)}, u32[]{:S(2)}) %all-to-all-start.2) | async-done | bytes 786464 | tf_op jit(solution)/shard_map/all_to_all | solution.py:268
  329.5 2.7 copy.31
  332.2 3.0 combine.1
  (33 shorter events, 1.0 us)
Async XLA Ops:
  6.5 216.9 %copy-start = (bf16[1,2048,768]{2,1,0:T(8,128)(2,1)S(1)}, bf16[1,2048,768]{2,1,0:T(8,128)(2,1)}, u32[]{:S(2)}) copy-start(bf16[1,2048,768]{2,1,0:T(8,128)(2,1)} %param.20) | copy-start | bytes 9437188
  6.5 60.1 %all-gather.4.cloned.1.call-start = ((), (), s32[]{:S(2)}) async-start(), calls=%async_computation.3 | async-start | bytes 2949120 | tf_op jit(solution)/shard_map/all_gather | solution.py:223
  22.9 116.4 %collective-permute-start = (bf16[768,2048]{1,0:T(8,128)(2,1)}, bf16[768,2048]{1,0:T(8,128)(2,1)}, u32[]{:S(2)}, u32[]{:S(2)}) collective-permute-start(bf16[768,2048]{1,0:T(8,128)(2,1)} %bitcast.71), channel_id=1, source_target_pairs={{0,1},{1,2},{2,3},{3,0},{4,5},{5,6},{6,7},{7,4},{8,9},{9,10},{10,1... | collective-permute-start | bytes 9437192 | tf_op jit(solution)/shard_map/ppermute | solution.py:213
  23.9 115.4 %collective-permute-start.1 = (bf16[768,2048]{1,0:T(8,128)(2,1)}, bf16[768,2048]{1,0:T(8,128)(2,1)}, u32[]{:S(2)}, u32[]{:S(2)}) collective-permute-start(bf16[768,2048]{1,0:T(8,128)(2,1)} %bitcast.72), channel_id=1, source_target_pairs={{0,3},{1,0},{2,1},{3,2},{4,7},{5,4},{6,5},{7,6},{8,11},{9,8},{10,9... | collective-permute-start | bytes 9437192 | tf_op jit(solution)/shard_map/ppermute | solution.py:213
  66.6 12.3 %collective-permute-start.3 = (bf16[32,160,256]{2,1,0:T(8,128)(2,1)}, bf16[32,160,256]{2,1,0:T(8,128)(2,1)}, u32[]{:S(2)}, u32[]{:S(2)}) collective-permute-start(bf16[32,160,256]{2,1,0:T(8,128)(2,1)} %all-gather.4.cloned.1.call-done.own_ref), channel_id=1, source_target_pairs={{0,4},{4,0},{1,5},{5,1},{2,6},{6,2},{3,7},{7,3},{8,12},{12,8},{9,1... | collective-permute-start | bytes 7864328 | tf_op jit(solution)/shard_map/ppermute | solution.py:225
  67.6 11.3 %collective-permute-start.2 = (bf16[128,512]{1,0:T(8,128)(2,1)S(1)}, bf16[128,512]{1,0:T(8,128)(2,1)S(1)}, u32[]{:S(2)}, u32[]{:S(2)}) collective-permute-start(bf16[128,512]{1,0:T(8,128)(2,1)S(1)} %get-tuple-element.21), channel_id=1, source_target_pairs={{0,252},{4,248},{8,244},{12,240},{16,236},{20,232},{24,228},{28,22... | collective-permute-start | bytes 393224 | tf_op jit(solution)/shard_map/ppermute | solution.py:221
  78.9 1.7 copy-start.1
  80.7 70.0 %copy-start.3 = (bf16[512,2048]{1,0:T(8,128)(2,1)S(1)}, bf16[512,2048]{1,0:T(8,128)(2,1)}, u32[]{:S(2)}) copy-start(bf16[512,2048]{1,0:T(8,128)(2,1)} %param.15) | copy-start | bytes 6291460
  139.3 18.0 %copy-start.5 = (s32[64,2]{0,1:T(2,128)S(1)}, s32[64,2]{0,1:T(2,128)}, u32[]{:S(2)}) copy-start(s32[64,2]{0,1:T(2,128)} %param.17) | copy-start | bytes 1540
  139.4 11.3 %collective-permute-start.4 = (bf16[128,512]{1,0:T(8,128)(2,1)S(1)}, bf16[128,512]{1,0:T(8,128)(2,1)S(1)}, u32[]{:S(2)}, u32[]{:S(2)}) collective-permute-start(bf16[128,512]{1,0:T(8,128)(2,1)S(1)} %get-tuple-element.16), channel_id=1, source_target_pairs={{0,252},{4,248},{8,244},{12,240},{16,236},{20,232},{24,228},{28,22... | collective-permute-start | bytes 393224 | tf_op jit(solution)/shard_map/ppermute | solution.py:233
  152.5 18.9 %all-to-all-start = ((bf16[4,64,2048]{2,1,0:T(8,128)(2,1)}), bf16[4,64,2048]{2,1,0:T(8,128)(2,1)}, u32[]{:S(2)}, u32[]{:S(2)}) async-start(bf16[4,64,2048]{2,1,0:T(8,128)(2,1)} %bitcast.64), calls=%async_computation | async-start | bytes 2097152 | tf_op jit(solution)/shard_map/all_to_all | solution.py:236
  177.1 36.6 %all-to-all-start.1 = ((bf16[64,3,2048]{2,1,0:T(4,128)(2,1)}), bf16[64,3,2048]{2,1,0:T(4,128)(2,1)}, u32[]{:S(2)}, u32[]{:S(2)}) async-start(bf16[64,3,2048]{2,1,0:T(4,128)(2,1)} %copy.22), calls=%async_computation.1 | async-start | bytes 2097152 | tf_op jit(solution)/shard_map/all_to_all | solution.py:245
  187.8 88.2 %collective-permute-start.12 = (bf16[384,2048]{1,0:T(8,128)(2,1)}, bf16[384,2048]{1,0:T(8,128)(2,1)}, u32[]{:S(2)}, u32[]{:S(2)}) collective-permute-start(bf16[384,2048]{1,0:T(8,128)(2,1)} %slice.22), channel_id=1, source_target_pairs={{0,1},{1,2},{2,3},{3,0},{4,5},{5,6},{6,7},{7,4},{8,9},{9,10},{10,1... | collective-permute-start | bytes 4718600 | tf_op jit(solution)/shard_map/ppermute | solution.py:218
  192.6 83.4 %collective-permute-start.13 = (bf16[384,2048]{1,0:T(8,128)(2,1)}, bf16[384,2048]{1,0:T(8,128)(2,1)}, u32[]{:S(2)}, u32[]{:S(2)}) collective-permute-start(bf16[384,2048]{1,0:T(8,128)(2,1)} %slice.23), channel_id=1, source_target_pairs={{0,3},{1,0},{2,1},{3,2},{4,7},{5,4},{6,5},{7,6},{8,11},{9,8},{10,9... | collective-permute-start | bytes 4718600 | tf_op jit(solution)/shard_map/ppermute | solution.py:218
  216.4 30.6 %collective-permute-start.5 = (bf16[192,2048]{1,0:T(8,128)(2,1)}, bf16[192,2048]{1,0:T(8,128)(2,1)}, u32[]{:S(2)}, u32[]{:S(2)}) collective-permute-start(bf16[192,2048]{1,0:T(8,128)(2,1)} %bitcast.8), channel_id=1, source_target_pairs={{0,3},{1,0},{2,1},{3,2},{4,7},{5,4},{6,5},{7,6},{8,11},{9,8},{10,9... | collective-permute-start | bytes 2359304 | tf_op jit(solution)/shard_map/ppermute | solution.py:213
  216.4 35.7 %collective-permute-start.7 = (bf16[192,2048]{1,0:T(8,128)(2,1)}, bf16[192,2048]{1,0:T(8,128)(2,1)}, u32[]{:S(2)}, u32[]{:S(2)}) collective-permute-start(bf16[192,2048]{1,0:T(8,128)(2,1)} %bitcast.8), channel_id=1, source_target_pairs={{0,1},{1,2},{2,3},{3,0},{4,5},{5,6},{6,7},{7,4},{8,9},{9,10},{10,1... | collective-permute-start | bytes 2359304 | tf_op jit(solution)/shard_map/ppermute | solution.py:213
  249.9 6.4 %copy-start.2 = (bf16[1,2048,768]{2,1,0:T(8,128)(2,1)S(1)}, bf16[1,2048,768]{2,1,0:T(8,128)(2,1)}, u32[]{:S(2)}) copy-start(bf16[1,2048,768]{2,1,0:T(8,128)(2,1)} %param.19) | copy-start | bytes 9437188
  252.0 21.2 %collective-permute-start.6 = (bf16[192,768]{1,0:T(8,128)(2,1)S(1)}, bf16[192,768]{1,0:T(8,128)(2,1)S(1)}, u32[]{:S(2)}, u32[]{:S(2)}) collective-permute-start(bf16[192,768]{1,0:T(8,128)(2,1)S(1)} %multiply_convert_fusion.2), channel_id=1, source_target_pairs={{0,1},{1,2},{2,3},{3,0},{4,5},{5,6},{6,7},{7,4},{8,9},{9,10},{10,1... | collective-permute-start | bytes 884744 | tf_op jit(solution)/shard_map/ppermute | solution.py:256
  253.1 15.1 %collective-permute-start.9 = (bf16[96,2048]{1,0:T(8,128)(2,1)S(1)}, bf16[96,2048]{1,0:T(8,128)(2,1)S(1)}, u32[]{:S(2)}, u32[]{:S(2)}) collective-permute-start(bf16[96,2048]{1,0:T(8,128)(2,1)S(1)} %slice.24), channel_id=1, source_target_pairs={{0,1},{1,2},{2,3},{3,0},{4,5},{5,6},{6,7},{7,4},{8,9},{9,10},{10,1... | collective-permute-start | bytes 1179656 | tf_op jit(solution)/shard_map/ppermute | solution.py:218
  254.3 14.1 %collective-permute-start.10 = (bf16[96,2048]{1,0:T(8,128)(2,1)S(1)}, bf16[96,2048]{1,0:T(8,128)(2,1)S(1)}, u32[]{:S(2)}, u32[]{:S(2)}) collective-permute-start(bf16[96,2048]{1,0:T(8,128)(2,1)S(1)} %slice.25), channel_id=1, source_target_pairs={{0,3},{1,0},{2,1},{3,2},{4,7},{5,4},{6,5},{7,6},{8,11},{9,8},{10,9... | collective-permute-start | bytes 1179656 | tf_op jit(solution)/shard_map/ppermute | solution.py:218
  268.3 17.2 %collective-permute-start.8 = (bf16[192,768]{1,0:T(8,128)(2,1)S(1)}, bf16[192,768]{1,0:T(8,128)(2,1)S(1)}, u32[]{:S(2)}, u32[]{:S(2)}) collective-permute-start(bf16[192,768]{1,0:T(8,128)(2,1)S(1)} %multiply_convert_fusion.1), channel_id=1, source_target_pairs={{0,3},{1,0},{2,1},{3,2},{4,7},{5,4},{6,5},{7,6},{8,11},{9,8},{10,9... | collective-permute-start | bytes 884744 | tf_op jit(solution)/shard_map/ppermute | solution.py:257
  269.2 4.1 %copy-start.4 = (f32[192,2048]{1,0:T(8,128)S(1)}, f32[192,2048]{1,0:T(8,128)}, u32[]{:S(2)}) copy-start(f32[192,2048]{1,0:T(8,128)} %fusion.29) | copy-start | bytes 4718596
  270.0 12.7 %collective-permute-start.11 = (bf16[192,768]{1,0:T(8,128)(2,1)S(1)}, bf16[192,768]{1,0:T(8,128)(2,1)S(1)}, u32[]{:S(2)}, u32[]{:S(2)}) collective-permute-start(bf16[192,768]{1,0:T(8,128)(2,1)S(1)} %multiply_convert_fusion), channel_id=1, source_target_pairs={{0,2},{1,3},{2,0},{3,1},{4,6},{5,7},{6,4},{7,5},{8,10},{9,11},{10,... | collective-permute-start | bytes 884744 | tf_op jit(solution)/shard_map/ppermute | solution.py:259
  288.3 12.6 %copy-start.6 = (f32[64,2]{0,1:T(2,128)S(1)}, f32[64,2]{0,1:T(2,128)}, u32[]{:S(2)}) copy-start(f32[64,2]{0,1:T(2,128)} %param.18) | copy-start | bytes 1540
  289.9 39.6 %all-to-all-start.2 = ((bf16[64,3,2048]{2,1,0:T(4,128)(2,1)}), bf16[64,3,2048]{2,1,0:T(4,128)(2,1)}, u32[]{:S(2)}, u32[]{:S(2)}) async-start(bf16[64,3,2048]{2,1,0:T(4,128)(2,1)} %bitcast.63), calls=%async_computation.2 | async-start | bytes 2097152 | tf_op jit(solution)/shard_map/all_to_all | solution.py:268
Sparse Core Ops, SparseCore 0:
  23.1 43.5 all-gather.3

commit v3 on v2

--- a/solution.py
+++ b/solution.py
@@ -21,16 +21,25 @@
 VALUE_ROWS = 64
 
 
+SAFE_SCORE = 60.0
+
+
+def bf16_pieces(values):
+    high = values.astype(jnp.bfloat16).astype(jnp.float32)
+    rest = values - high
+    middle = rest.astype(jnp.bfloat16).astype(jnp.float32)
+    return [high, middle, rest - middle]
+
+
 def prep_body(kv_ref, gate_ref, out_ref):
     kv = kv_ref[...].astype(jnp.float32).T
-    gate = gate_ref[...]
-    high = gate.astype(jnp.bfloat16).astype(jnp.float32)
-    rest = gate - high
-    middle = rest.astype(jnp.bfloat16).astype(jnp.float32)
-    low = rest - middle
-    gates = jnp.concatenate([high, middle, low, jnp.zeros_like(gate)], axis=0)
+    keys = kv[:HEAD_SIZE]
+    square = jnp.sum(keys * keys, axis=0, keepdims=True) * 1.02
+    ones = jnp.ones_like(square)
+    zeros = jnp.zeros_like(square)
     out_ref[...] = jnp.concatenate(
-        [kv[:HEAD_SIZE], gates, kv[HEAD_SIZE:]], axis=0
+        [keys, *bf16_pieces(gate_ref[...])] + [ones] * 3 + [square] + [zeros] * 4 + [kv[HEAD_SIZE:]],
+        axis=0,
     ).astype(jnp.bfloat16)
 
 
@@ -42,38 +51,80 @@
     )(kv, gate_t)
 
 
-def attend_body(index_ref, qa_ref, qb_ref, own_ref, other_ref, outa_ref, outb_ref, qt_ref, max_ref, acc_ref, *, blocks, heads):
+def attend_body(index_ref, qa_ref, qb_ref, own_ref, other_ref, out_ref, qt_ref, max_ref, acc_ref, *, blocks, heads):
     columns = heads * HALF
     step = 256
     own_index = index_ref[0]
     core = own_index % 2
-    row = lax.broadcasted_iota(jnp.int32, (KEY_ROWS - HEAD_SIZE, columns), 0)
-    head = lax.broadcasted_iota(jnp.int32, (KEY_ROWS - HEAD_SIZE, columns), 1) // HALF
-    picks = jnp.where((row % heads == head) & (row < 3 * heads), -1.0, 0.0)
-    for which, q_ref in ((0, qa_ref), (1, qb_ref)):
+    picked = 3 * heads
+    row = lax.broadcasted_iota(jnp.int32, (picked, columns), 0)
+    head = lax.broadcasted_iota(jnp.int32, (picked, columns), 1) // HALF
+    picks = jnp.where(row % heads == head, -1.0, 0.0)
+    largest_query = jnp.float32(0.0)
+    mirror = blocks - 1 - own_index
+    gates_at = slice(HEAD_SIZE, HEAD_SIZE + picked)
+    gates_a = own_ref[own_index // 2, gates_at, :HALF].astype(jnp.float32)
+    gates_b = other_ref[mirror // 2, gates_at, HALF:].astype(jnp.float32)
+    for which, q_ref, gates in ((0, qa_ref, gates_a), (1, qb_ref, gates_b)):
         qt = (q_ref[...].astype(jnp.float32) * (HEAD_SIZE**-0.5)).T
         qt = jnp.concatenate(
             [qt[h * HEAD_SIZE : (h + 1) * HEAD_SIZE] for h in range(heads)], axis=1
         )
-        qt_ref[which] = jnp.concatenate([qt, picks], axis=0).astype(jnp.bfloat16)
-    max_ref[...] = jnp.full(max_ref.shape, NEG_FILL, jnp.float32)
+        largest_query = jnp.maximum(
+            largest_query, jnp.max(jnp.sum(qt * qt, axis=0, keepdims=True))
+        )
+        pieces = [
+            jnp.concatenate([gates[p + h : p + h + 1] for h in range(heads)], axis=1)
+            for p in range(0, picked, heads)
+        ]
+        qt_ref[which] = jnp.concatenate(
+            [qt, picks, *pieces, jnp.zeros((5, columns), jnp.float32)], axis=0
+        ).astype(jnp.bfloat16)
+    tail = slice(KEY_ROWS - 16, KEY_ROWS)
+    squares = jnp.maximum(
+        jnp.max(own_ref[:, tail].astype(jnp.float32), axis=0),
+        jnp.max(other_ref[:, tail].astype(jnp.float32), axis=0),
+    )
+    largest_key = jnp.max(squares[11:12])
+    bounded = largest_query * largest_key <= SAFE_SCORE**2
     acc_ref[...] = jnp.zeros(acc_ref.shape, jnp.float32)
 
-    def attend(which, pair, first_row):
+    def operands(pair):
         tile = jnp.concatenate([own_ref[pair], other_ref[pair]], axis=1)
         keys = tile[:KEY_ROWS].astype(jnp.float32).T.astype(jnp.bfloat16)
         values = jnp.concatenate(
             [tile[KEY_ROWS:], jnp.ones((16, 2 * BLOCK), jnp.bfloat16)], axis=0
         )
+        return keys, values
+
+    def masked(scores, pair, first_row):
+        k = lax.broadcasted_iota(jnp.int32, scores.shape, 0)
+        t = lax.broadcasted_iota(jnp.int32, scores.shape, 1) % HALF
+        start = jnp.where(k < BLOCK, core * BLOCK, (1 - core) * BLOCK - BLOCK)
+        seen = pair * (2 * BLOCK) + start + k <= first_row + t
+        return jnp.where(seen, scores, NEG_FILL)
+
+    def plan(which):
+        index = jnp.where(which == 0, own_index, blocks - 1 - own_index)
+        return index // 2, index * BLOCK + which * HALF
+
+    def plain(which, pair, first_row):
+        keys, values = operands(pair)
         for at in range(0, columns, step):
             cols = slice(at, at + step)
             scores = jnp.dot(keys, qt_ref[which, :, cols], preferred_element_type=jnp.float32)
             if first_row is not None:
-                k = lax.broadcasted_iota(jnp.int32, scores.shape, 0)
-                t = lax.broadcasted_iota(jnp.int32, scores.shape, 1) % HALF
-                start = jnp.where(k < BLOCK, core * BLOCK, (1 - core) * BLOCK - BLOCK)
-                seen = pair * (2 * BLOCK) + start + k <= first_row + t
-                scores = jnp.where(seen, scores, NEG_FILL)
+                scores = masked(scores, pair, first_row)
+            weights = jnp.exp2(scores * LOG2E).astype(jnp.bfloat16)
+            acc_ref[which, :, cols] += jnp.dot(values, weights, preferred_element_type=jnp.float32)
+
+    def shifted(which, pair, first_row):
+        keys, values = operands(pair)
+
+        def chunk(c, carry):
+            cols = pl.ds(pl.multiple_of(c * step, step), step)
+            scores = jnp.dot(keys, qt_ref[which, :, cols], preferred_element_type=jnp.float32)
+            scores = masked(scores, pair, first_row)
             before = max_ref[which, :, cols]
             now = jnp.maximum(before, jnp.max(scores, axis=0, keepdims=True))
             weights = jnp.exp2((scores - now) * LOG2E)
@@ -82,38 +133,58 @@
             acc_ref[which, :, cols] = acc_ref[which, :, cols] * rescale + jnp.dot(
                 values, weights.astype(jnp.bfloat16), preferred_element_type=jnp.float32
             )
-
-    for which, index, first in (
-        (0, own_index, own_index * BLOCK),
-        (1, blocks - 1 - own_index, (blocks - 1 - own_index) * BLOCK + HALF),
-    ):
-        last_pair = index // 2
-
-        def full(pair, carry, which=which):
-            attend(which, pair, None)
             return carry
 
-        lax.fori_loop(0, last_pair, full, 0)
-        attend(which, last_pair, first)
-
-    for which, out_ref in ((0, outa_ref), (1, outb_ref)):
+        lax.fori_loop(0, columns // step, chunk, 0)
+
+    @pl.when(bounded)
+    def _():
+        def one(which, carry):
+            last_pair, first_row = plan(which)
+
+            def full(pair, inner):
+                plain(which, pair, None)
+                return inner
+
+            lax.fori_loop(0, last_pair, full, 0)
+            plain(which, last_pair, first_row)
+            return carry
+
+        lax.fori_loop(0, 2, one, 0)
+
+    @pl.when(jnp.logical_not(bounded))
+    def _():
+        max_ref[...] = jnp.full(max_ref.shape, NEG_FILL, jnp.float32)
+
+        def one(which, carry):
+            last_pair, first_row = plan(which)
+
+            def any_pair(pair, inner):
+                shifted(which, pair, first_row)
+                return inner
+
+            lax.fori_loop(0, last_pair + 1, any_pair, 0)
+            return carry
+
+        lax.fori_loop(0, 2, one, 0)
+
+    for which in range(2):
         acc = acc_ref[which]
         out = acc[:VALUE_ROWS] / acc[VALUE_ROWS : VALUE_ROWS + 1]
         out = jnp.concatenate([out[:, h * HALF : (h + 1) * HALF] for h in range(heads)], axis=0)
-        out_ref[...] = out.T.astype(out_ref.dtype)
+        out_ref[which] = out.T.astype(out_ref.dtype)
 
 
 def attend_rows(index, qa, qb, own, other):
     heads = qa.shape[1] // HEAD_SIZE
     blocks = 2 * own.shape[0]
     columns = heads * HALF
-    out = jax.ShapeDtypeStruct(qa.shape, jnp.bfloat16)
     vmem = pl.BlockSpec(memory_space=pltpu.VMEM)
     return pl.pallas_call(
         functools.partial(attend_body, blocks=blocks, heads=heads),
         in_specs=[pl.BlockSpec(memory_space=pltpu.SMEM)] + [vmem] * 4,
-        out_specs=[vmem] * 2,
-        out_shape=[out, out],
+        out_specs=vmem,
+        out_shape=jax.ShapeDtypeStruct((2, *qa.shape), jnp.bfloat16),
         scratch_shapes=[
             pltpu.VMEM((2, KEY_ROWS, columns), jnp.bfloat16),
             pltpu.VMEM((2, 1, columns), jnp.float32),
@@ -218,31 +289,48 @@
             [lax.ppermute(before[:half], "tp", up), lax.ppermute(after[half:], "tp", down)], axis=0
         )
 
+    whole = [
+        (i * head_devices + t, (i if 2 * t < head_devices else seq_devices - 1 - i) * head_devices + t)
+        for i in range(seq_devices)
+        for t in range(head_devices)
+    ]
+    flipped = 2 * lax.axis_index("tp") >= head_devices
+    block = prepare_keys(key_value_pairs, forget_gate_total.T)
     mirrored_queries = lax.ppermute(queries[HALF:], SP, mirror)
-    block = prepare_keys(key_value_pairs, forget_gate_total.T)
-    own = lax.all_gather(lax.all_gather(block, "sp_1"), "sp_0")
-    own = own.reshape(-1, *block.shape)
-    other = lax.ppermute(own, "sp_2", [(0, 1), (1, 0)])
+    near = lax.all_gather(block, "sp_1")
+    near, mirrored_queries = lax.optimization_barrier((near, mirrored_queries))
+    own = lax.all_gather(near, "sp_0").reshape(-1, *block.shape)
     down_own = expert_down[0]
     down_before, down_after = neighbours(down_own)
-    first, second = attend_rows(index.reshape(1), queries[:HALF], mirrored_queries, own, other)
-    down_before, down_after, first, second = lax.optimization_barrier(
-        (down_before, down_after, first, second)
+    held_residual = lax.ppermute(residual_in, SP_TP, whole)
+    held_routes = lax.ppermute(routes, SP_TP, whole)
+    other = lax.ppermute(own, "sp_2", [(0, 1), (1, 0)])
+    attended = attend_rows(index.reshape(1), queries[:HALF], mirrored_queries, own, other)
+    down_before, down_after, attended = lax.optimization_barrier(
+        (down_before, down_after, attended)
     )
     down_across = opposite(down_before, down_after)
-    second = lax.ppermute(second, SP, mirror)
-    attended = jnp.concatenate([first, second], axis=0)
-    partial = jnp.dot(attended, out_weight, preferred_element_type=jnp.float32).astype(jnp.bfloat16)
+    partial = jnp.dot(
+        attended.reshape(-1, attended.shape[2]), out_weight, preferred_element_type=jnp.float32
+    ).astype(jnp.bfloat16)
     parts = lax.all_to_all(
         partial.reshape(head_devices, -1, partial.shape[1]), "tp", 0, 0, tiled=True
     )
     own_rows, top_count = routes.shape
     capacity = max(2, 3 * own_rows * top_count // (2 * seq_devices))
-    hidden_state, slots = dispatch(
-        parts, residual_in, norm_gain, routes, seq_devices, capacity
-    )
+    ranked_routes = jnp.where(flipped, seq_devices - 1 - held_routes, held_routes)
+    held_hidden, slots = dispatch(
+        parts, held_residual, norm_gain, ranked_routes, seq_devices, capacity
+    )
+    hidden_state = lax.ppermute(held_hidden, SP_TP, whole)
     width = slots.shape[2]
-    incoming = lax.all_to_all(slots.transpose(1, 0, 2), SP, 0, 0, tiled=True)
+    ranks = [
+        [(i if 2 * t < head_devices else seq_devices - 1 - i) * head_devices + t for i in range(seq_devices)]
+        for t in range(head_devices)
+    ]
+    incoming = lax.all_to_all(
+        slots.transpose(1, 0, 2), SP_TP, 0, 0, axis_index_groups=ranks, tiled=True
+    )
     rows_own = incoming.transpose(1, 0, 2).reshape(-1, width)
 
     def units(rows):

time: 343 us -> 358 us (1.044)
  starting transfers between devices: 45.6 us -> 82.6 us
  Pallas kernels: 66.3 us -> 53.7 us
  waiting for transfers between devices: 151 us -> 142 us
    all_to_all x1, starting transfers between devices: 7.9 us -> 34.6 us  [local(): lax.all_to_all(slots.transpose(1, 0, 2), SP_TP, 0, 0, axis_index_groups=r...]
    ppermute x1 -> x3, waiting for transfers between devices: 6.79 us -> 24.3 us  [the longest x1 19 us: local(): hidden_state = lax.ppermute(held_hidden, SP_TP, whole)]
    all_to_all x1, waiting for transfers between devices: 13.4 us -> 0.01 us  [local(): lax.all_to_all(partial.reshape(head_devices, -1, partial.shape[1]), 'tp',...]
    pallas_call x1, Pallas kernels: 58.6 us -> 46.2 us  [attend_rows(): pl.pallas_call(functools.partial(attend_body, blocks=blocks, heads=heads)...]
    ppermute x1 -> x3, starting transfers between devices: 4.53 us -> 15.6 us  [the longest x1 6.76 us: local(): hidden_state = lax.ppermute(held_hidden, SP_TP, whole)]
    all_to_all x1, waiting for transfers between devices: 28 us -> 21.1 us  [local(): returned = lax.all_to_all(leaving, SP, 0, 0, tiled=True).transpose(1, 0, 2)]
    ppermute x1, waiting for transfers between devices: 6.8 us -> 0.01 us  [local(): mirrored_queries = lax.ppermute(queries[HALF:], SP, mirror)]
    ppermute x1, waiting for transfers between devices: 0.01 us -> 5.25 us  [local(): other = lax.ppermute(own, 'sp_2', [(0, 1), (1, 0)])]
  transfers between devices with their start and end apart: 18 -> 20, of which waited for: 9 -> 9; matrix products, arithmetic and copies ran while one was open for 11% -> 11% of each run, Pallas kernels for 17% -> 13%
where the time goes in v3:
time: 358 us; the launch traced here: 357 us
  waiting for transfers between devices  142 us (40%)
  starting transfers between devices  82.6 us (23%)
  Pallas kernels  53.7 us (15%)
  matrix products  29.4 us (8%)
  local copies, waits for them, and re-layouts  21.8 us (6%)
  between operations  13.7 us (4%)
  blocking collectives  13.5 us (4%)
    pallas_call x1, Pallas kernels, attend_rows(): pl.pallas_call(functools.partial(attend_body, blocks=blocks, heads=heads)...  46.2 us
    all_gather x1, waiting for transfers between devices, local(): own = lax.all_gather(near, 'sp_0').reshape(-1, *block.shape)  38.3 us
    all_to_all x1, starting transfers between devices, local(): lax.all_to_all(slots.transpose(1, 0, 2), SP_TP, 0, 0, axis_index_groups=r...  34.6 us
    all_to_all x1, waiting for transfers between devices, local(): returned = lax.all_to_all(leaving, SP, 0, 0, tiled=True).transpose(1, 0, 2)  21.1 us
    ppermute x4, waiting for transfers between devices, neighbours(): return (lax.ppermute(array, 'tp', up), lax.ppermute(array, 'tp', down))  20.7 us
    ppermute x1, waiting for transfers between devices, local(): hidden_state = lax.ppermute(held_hidden, SP_TP, whole)  19 us
    all_to_all x1, waiting for transfers between devices, local(): lax.all_to_all(slots.transpose(1, 0, 2), SP_TP, 0, 0, axis_index_groups=r...  17.3 us
    all_gather x1, blocking collectives, local(): near = lax.all_gather(block, 'sp_1')  13.5 us
  transfers between devices with their start and end apart: 20, of which 9 were waited for; matrix products, arithmetic and copies ran while one was open for 11% of the time, Pallas kernels for 13%

profile of v3, /device:TPU:6, one launch (start us, length us, event | category | flops | bytes accessed | tf_op | source)
XLA Modules:
  0.0 357.4 jit_solution(15684009506874239503)
XLA Ops:
  6.5 1.1 fusion.40
  7.7 7.8 %collective-permute-start.2 = (bf16[128,512]{1,0:T(8,128)(2,1)S(1)}, bf16[128,512]{1,0:T(8,128)(2,1)S(1)}, u32[]{:S(2)}, u32[]{:S(2)}) collective-permute-start(bf16[128,512]{1,0:T(8,128)(2,1)S(1)} %get-tuple-element.19), channel_id=1, source_target_pairs={{0,252},{4,248},{8,244},{12,240},{16,236},{20,232},{24,228},{28,22... | collective-permute-start | bytes 393224 | tf_op jit(solution)/shard_map/ppermute | solution.py:299
  15.5 1.6 prepare_keys.1
  17.1 13.5 %all-gather = bf16[640,256]{1,0:T(8,128)(2,1)} all-gather(bf16[160,256]{1,0:T(8,128)(2,1)} %prepare_keys.1), channel_id=2, replica_groups=mesh['sp_0'=8,'sp_1'=4,'sp_2'=2,'tp'=4] {'sp_1'}, dimensions={0}, use_global_device_ids=true | all-gather | bytes 409600 | tf_op jit(solution)/shard_map/all_gather | solution.py:300
  31.1 1.5 collective-permute-start.1
  32.7 38.3 %all-gather.4.cloned.1.call-done.own_ref = bf16[32,160,256]{2,1,0:T(8,128)(2,1)} async-done(((bf16[4,160,256]{2,1,0:T(8,128)(2,1)}), bf16[32,160,256]{2,1,0:T(8,128)(2,1)}) %all-gather.4.cloned.1.call-update) | async-done | bytes 2621456 | tf_op jit(solution)/shard_map/all_gather | solution.py:302
  71.0 5.2 %collective-permute-done.3.other_ref = bf16[32,160,256]{2,1,0:T(8,128)(2,1)} collective-permute-done((bf16[32,160,256]{2,1,0:T(8,128)(2,1)}, bf16[32,160,256]{2,1,0:T(8,128)(2,1)}, u32[]{:S(2)}, u32[]{:S(2)}) %collective-permute-start.3) | collective-permute-done | bytes 2621472 | tf_op jit(solution)/shard_map/ppermute | solution.py:307
  76.2 1.7 copy-done.1
  78.0 46.2 %attend_rows.1 = bf16[2,128,512]{2,1,0:T(8,128)(2,1)S(1)} custom-call(s32[1]{0:T(128)} %bitcast.1.index_ref, bf16[128,512]{1,0:T(8,128)(2,1)S(1)} %get-tuple-element.20.qa_ref, bf16[128,512]{1,0:T(8,128)(2,1)S(1)} %collective-permute-done.2.qb_ref, bf16[32,160,256]{2,1,0:T(8,128)(2,1)S(1)} %copy-done.1, bf16[32,160,256]{2,1,0:T(8,128)(2,1)} %collective-permute-done.3.other_ref), custom_call_target="tpu_custom_call" | custom-call | tf_op jit(solution)/shard_map/attend_rows/pallas_call | solution.py:183
  124.3 1.8 convolution_convert_fusion
  126.1 4.8 %all-to-all-start = ((bf16[4,64,2048]{2,1,0:T(8,128)(2,1)}), bf16[4,64,2048]{2,1,0:T(8,128)(2,1)}, u32[]{:S(2)}, u32[]{:S(2)}) async-start(bf16[4,64,2048]{2,1,0:T(8,128)(2,1)} %bitcast.67), calls=%async_computation | async-start | bytes 2097152 | tf_op jit(solution)/shard_map/all_to_all | solution.py:316
  130.9 5.6 %collective-permute-start.4 = (bf16[64,2048]{1,0:T(8,128)(2,1)}, bf16[64,2048]{1,0:T(8,128)(2,1)S(1)}, u32[]{:S(2)}, u32[]{:S(2)}) collective-permute-start(bf16[64,2048]{1,0:T(8,128)(2,1)} %param.14), channel_id=1, source_target_pairs={{0,0},{1,1},{2,254},{3,255},{4,4},{5,5},{6,250},{7,251},{8,8},{9,9... | collective-permute-start | bytes 786440 | tf_op jit(solution)/shard_map/ppermute | solution.py:305
  136.6 3.2 collective-permute-start.5
  139.9 5.4 %collective-permute-done.5 = s32[64,2]{1,0:T(8,128)S(1)} collective-permute-done((s32[64,2]{1,0:T(8,128)S(1)}, s32[64,2]{1,0:T(8,128)S(1)}, u32[]{:S(2)}, u32[]{:S(2)}) %collective-permute-start.5) | collective-permute-done | bytes 544 | tf_op jit(solution)/shard_map/ppermute | solution.py:306
  146.6 3.0 dispatch.1
  149.5 2.8 copy.22
  152.3 34.6 %all-to-all-start.1 = ((bf16[64,3,2048]{2,1,0:T(4,128)(2,1)}), bf16[64,3,2048]{2,1,0:T(4,128)(2,1)}, u32[]{:S(2)}, u32[]{:S(2)}) async-start(bf16[64,3,2048]{2,1,0:T(4,128)(2,1)} %copy.22), calls=%async_computation.1 | async-start | bytes 2097152 | tf_op jit(solution)/shard_map/all_to_all | solution.py:331
  187.0 2.7 slice.22
  189.7 2.8 slice.23
  192.5 2.0 collective-permute-start.14
  194.5 17.3 %all-to-all-done.1 = bf16[64,3,2048]{2,1,0:T(4,128)(2,1)} async-done(((bf16[64,3,2048]{2,1,0:T(4,128)(2,1)}), bf16[64,3,2048]{2,1,0:T(4,128)(2,1)}, u32[]{:S(2)}, u32[]{:S(2)}) %all-to-all-start.1) | async-done | bytes 786464 | tf_op jit(solution)/shard_map/all_to_all | solution.py:331
  211.8 2.7 copy.23
  214.5 0.9 collective-permute-start.6
  215.3 2.4 collective-permute-start.8
  217.7 3.7 %fusion.18 = f32[192,768]{1,0:T(8,128)} fusion(bf16[192,2048]{1,0:T(8,128)(2,1)} %bitcast.9, bf16[1,2048,768]{2,1,0:T(8,128)(2,1)} %param.19), kind=kOutput, calls=%fused_computation.18 | convolution fusion | flops 603979776 | bytes 4521984 | tf_op jit(solution)/shard_map/dot_general | solution.py:337
  221.4 5.1 %fusion.29 = f32[192,2048]{1,0:T(8,128)} fusion(bf16[192,2048]{1,0:T(8,128)(2,1)} %bitcast.9, bf16[1,2048,768]{2,1,0:T(8,128)(2,1)S(1)} %copy-done, f32[192,768]{1,0:T(8,128)} %fusion.18, bf16[1,768,2048]{2,1,0:T(8,128)(2,1)} %param.21), kind=kOutput, calls=%fused_computation.28 | convolution fusion | flops 1208844288 | bytes 9240576 | tf_op jit(solution)/shard_map/dot_general | solution.py:348
  226.6 20.7 %collective-permute-done.6 = bf16[192,2048]{1,0:T(8,128)(2,1)} collective-permute-done((bf16[192,2048]{1,0:T(8,128)(2,1)}, bf16[192,2048]{1,0:T(8,128)(2,1)}, u32[]{:S(2)}, u32[]{:S(2)}) %collective-permute-start.6) | collective-permute-done | bytes 786464 | tf_op jit(solution)/shard_map/ppermute | solution.py:284
  247.3 2.9 fusion.16
  250.2 2.1 multiply_convert_fusion.2
  252.6 1.0 slice.24
  253.6 1.8 collective-permute-start.10
  255.5 1.0 slice.25
  256.9 1.9 fusion.14
  258.8 1.9 multiply_convert_fusion.1
  260.7 8.2 %collective-permute-done.10 = bf16[96,2048]{1,0:T(8,128)(2,1)S(1)} collective-permute-done((bf16[96,2048]{1,0:T(8,128)(2,1)S(1)}, bf16[96,2048]{1,0:T(8,128)(2,1)S(1)}, u32[]{:S(2)}, u32[]{:S(2)}) %collective-permute-start.10) | collective-permute-done | bytes 393248 | tf_op jit(solution)/shard_map/ppermute | solution.py:289
  270.1 0.8 multiply_convert_fusion
  270.9 3.0 collective-permute-start.12
  273.9 2.7 convolution_add_fusion.1
  276.7 7.0 %collective-permute-done.12 = bf16[192,768]{1,0:T(8,128)(2,1)S(1)} collective-permute-done((bf16[192,768]{1,0:T(8,128)(2,1)S(1)}, bf16[192,768]{1,0:T(8,128)(2,1)S(1)}, u32[]{:S(2)}, u32[]{:S(2)}) %collective-permute-start.12) | collective-permute-done | bytes 294944 | tf_op jit(solution)/shard_map/ppermute | solution.py:347
  283.6 2.7 fusion
  286.4 2.8 fusion.21
  289.2 1.6 copy.30
  290.8 6.5 %all-to-all-start.2 = ((bf16[64,3,2048]{2,1,0:T(4,128)(2,1)}), bf16[64,3,2048]{2,1,0:T(4,128)(2,1)}, u32[]{:S(2)}, u32[]{:S(2)}) async-start(bf16[64,3,2048]{2,1,0:T(4,128)(2,1)} %bitcast.66), calls=%async_computation.2 | async-start | bytes 2097152 | tf_op jit(solution)/shard_map/all_to_all | solution.py:356
  297.4 6.8 %collective-permute-start.15 = (f32[64,2048]{1,0:T(8,128)}, f32[64,2048]{1,0:T(8,128)}, u32[]{:S(2)}, u32[]{:S(2)}) collective-permute-start(f32[64,2048]{1,0:T(8,128)} %get-tuple-element.18), channel_id=1, source_target_pairs={{0,0},{1,1},{2,254},{3,255},{4,4},{5,5},{6,250},{7,251},{8,8},{9,9... | collective-permute-start | bytes 1572872 | tf_op jit(solution)/shard_map/ppermute | solution.py:325
  304.8 21.1 %all-to-all-done.2 = bf16[64,3,2048]{2,1,0:T(4,128)(2,1)} async-done(((bf16[64,3,2048]{2,1,0:T(4,128)(2,1)}), bf16[64,3,2048]{2,1,0:T(4,128)(2,1)}, u32[]{:S(2)}, u32[]{:S(2)}) %all-to-all-start.2) | async-done | bytes 786464 | tf_op jit(solution)/shard_map/all_to_all | solution.py:356
  325.9 2.7 copy.31
  328.6 19.0 %collective-permute-done.15.hidden_ref = f32[64,2048]{1,0:T(8,128)} collective-permute-done((f32[64,2048]{1,0:T(8,128)}, f32[64,2048]{1,0:T(8,128)}, u32[]{:S(2)}, u32[]{:S(2)}) %collective-permute-start.15) | collective-permute-done | bytes 524320 | tf_op jit(solution)/shard_map/ppermute | solution.py:325
  347.6 3.0 combine.1
  (42 shorter events, 4.5 us)
Async XLA Ops:
  6.5 214.9 %copy-start = (bf16[1,2048,768]{2,1,0:T(8,128)(2,1)S(1)}, bf16[1,2048,768]{2,1,0:T(8,128)(2,1)}, u32[]{:S(2)}) copy-start(bf16[1,2048,768]{2,1,0:T(8,128)(2,1)} %param.20) | copy-start | bytes 9437188
  6.5 64.5 %all-gather.4.cloned.1.call-start = ((), (), s32[]{:S(2)}) async-start(), calls=%async_computation.3 | async-start | bytes 2949120 | tf_op jit(solution)/shard_map/all_gather | solution.py:302
  7.7 22.9 %collective-permute-start.2 = (bf16[128,512]{1,0:T(8,128)(2,1)S(1)}, bf16[128,512]{1,0:T(8,128)(2,1)S(1)}, u32[]{:S(2)}, u32[]{:S(2)}) collective-permute-start(bf16[128,512]{1,0:T(8,128)(2,1)S(1)} %get-tuple-element.19), channel_id=1, source_target_pairs={{0,252},{4,248},{8,244},{12,240},{16,236},{20,232},{24,228},{28,22... | collective-permute-start | bytes 393224 | tf_op jit(solution)/shard_map/ppermute | solution.py:299
  30.6 93.6 %collective-permute-start = (bf16[768,2048]{1,0:T(8,128)(2,1)}, bf16[768,2048]{1,0:T(8,128)(2,1)}, u32[]{:S(2)}, u32[]{:S(2)}) collective-permute-start(bf16[768,2048]{1,0:T(8,128)(2,1)} %bitcast.74), channel_id=1, source_target_pairs={{0,1},{1,2},{2,3},{3,0},{4,5},{5,6},{6,7},{7,4},{8,9},{9,10},{10,1... | collective-permute-start | bytes 9437192 | tf_op jit(solution)/shard_map/ppermute | solution.py:284
  31.1 93.1 %collective-permute-start.1 = (bf16[768,2048]{1,0:T(8,128)(2,1)}, bf16[768,2048]{1,0:T(8,128)(2,1)}, u32[]{:S(2)}, u32[]{:S(2)}) collective-permute-start(bf16[768,2048]{1,0:T(8,128)(2,1)} %bitcast.75), channel_id=1, source_target_pairs={{0,3},{1,0},{2,1},{3,2},{4,7},{5,4},{6,5},{7,6},{8,11},{9,8},{10,9... | collective-permute-start | bytes 9437192 | tf_op jit(solution)/shard_map/ppermute | solution.py:284
  71.0 5.3 %collective-permute-start.3 = (bf16[32,160,256]{2,1,0:T(8,128)(2,1)}, bf16[32,160,256]{2,1,0:T(8,128)(2,1)}, u32[]{:S(2)}, u32[]{:S(2)}) collective-permute-start(bf16[32,160,256]{2,1,0:T(8,128)(2,1)} %all-gather.4.cloned.1.call-done.own_ref), channel_id=1, source_target_pairs={{0,4},{4,0},{1,5},{5,1},{2,6},{6,2},{3,7},{7,3},{8,12},{12,8},{9,1... | collective-permute-start | bytes 7864328 | tf_op jit(solution)/shard_map/ppermute | solution.py:307
  76.2 1.7 copy-start.1
  78.0 46.3 %copy-start.3 = (bf16[512,2048]{1,0:T(8,128)(2,1)S(1)}, bf16[512,2048]{1,0:T(8,128)(2,1)}, u32[]{:S(2)}) copy-start(bf16[512,2048]{1,0:T(8,128)(2,1)} %param.15) | copy-start | bytes 6291460
  124.2 12.3 %copy-start.7 = (s32[64,2]{0,1:T(2,128)S(1)}, s32[64,2]{0,1:T(2,128)}, u32[]{:S(2)}) copy-start(s32[64,2]{0,1:T(2,128)} %param.17) | copy-start | bytes 1540
  126.1 19.8 %all-to-all-start = ((bf16[4,64,2048]{2,1,0:T(8,128)(2,1)}), bf16[4,64,2048]{2,1,0:T(8,128)(2,1)}, u32[]{:S(2)}, u32[]{:S(2)}) async-start(bf16[4,64,2048]{2,1,0:T(8,128)(2,1)} %bitcast.67), calls=%async_computation | async-start | bytes 2097152 | tf_op jit(solution)/shard_map/all_to_all | solution.py:316
  130.9 15.0 %collective-permute-start.4 = (bf16[64,2048]{1,0:T(8,128)(2,1)}, bf16[64,2048]{1,0:T(8,128)(2,1)S(1)}, u32[]{:S(2)}, u32[]{:S(2)}) collective-permute-start(bf16[64,2048]{1,0:T(8,128)(2,1)} %param.14), channel_id=1, source_target_pairs={{0,0},{1,1},{2,254},{3,255},{4,4},{5,5},{6,250},{7,251},{8,8},{9,9... | collective-permute-start | bytes 786440 | tf_op jit(solution)/shard_map/ppermute | solution.py:305
  136.6 53.1 %copy-start.6 = (s32[64,2]{1,0:T(8,128)}, s32[64,2]{1,0:T(8,128)S(1)}, u32[]{:S(2)}) copy-start(s32[64,2]{1,0:T(8,128)S(1)} %copy.21.routes_ref) | copy-start | bytes 1540
  136.6 8.6 %collective-permute-start.5 = (s32[64,2]{1,0:T(8,128)S(1)}, s32[64,2]{1,0:T(8,128)S(1)}, u32[]{:S(2)}, u32[]{:S(2)}) collective-permute-start(s32[64,2]{1,0:T(8,128)S(1)} %copy.21.routes_ref), channel_id=1, source_target_pairs={{0,0},{1,1},{2,254},{3,255},{4,4},{5,5},{6,250},{7,251},{8,8},{9,9... | collective-permute-start | bytes 1544 | tf_op jit(solution)/shard_map/ppermute | solution.py:306
  145.9 0.7 copy-start.5
  152.3 59.5 %all-to-all-start.1 = ((bf16[64,3,2048]{2,1,0:T(4,128)(2,1)}), bf16[64,3,2048]{2,1,0:T(4,128)(2,1)}, u32[]{:S(2)}, u32[]{:S(2)}) async-start(bf16[64,3,2048]{2,1,0:T(4,128)(2,1)} %copy.22), calls=%async_computation.1 | async-start | bytes 2097152 | tf_op jit(solution)/shard_map/all_to_all | solution.py:331
  189.7 86.9 %collective-permute-start.13 = (bf16[384,2048]{1,0:T(8,128)(2,1)}, bf16[384,2048]{1,0:T(8,128)(2,1)}, u32[]{:S(2)}, u32[]{:S(2)}) collective-permute-start(bf16[384,2048]{1,0:T(8,128)(2,1)} %slice.22), channel_id=1, source_target_pairs={{0,1},{1,2},{2,3},{3,0},{4,5},{5,6},{6,7},{7,4},{8,9},{9,10},{10,1... | collective-permute-start | bytes 4718600 | tf_op jit(solution)/shard_map/ppermute | solution.py:289
  192.5 84.2 %collective-permute-start.14 = (bf16[384,2048]{1,0:T(8,128)(2,1)}, bf16[384,2048]{1,0:T(8,128)(2,1)}, u32[]{:S(2)}, u32[]{:S(2)}) collective-permute-start(bf16[384,2048]{1,0:T(8,128)(2,1)} %slice.23), channel_id=1, source_target_pairs={{0,3},{1,0},{2,1},{3,2},{4,7},{5,4},{6,5},{7,6},{8,11},{9,8},{10,9... | collective-permute-start | bytes 4718600 | tf_op jit(solution)/shard_map/ppermute | solution.py:289
  214.5 32.8 %collective-permute-start.6 = (bf16[192,2048]{1,0:T(8,128)(2,1)}, bf16[192,2048]{1,0:T(8,128)(2,1)}, u32[]{:S(2)}, u32[]{:S(2)}) collective-permute-start(bf16[192,2048]{1,0:T(8,128)(2,1)} %bitcast.9), channel_id=1, source_target_pairs={{0,3},{1,0},{2,1},{3,2},{4,7},{5,4},{6,5},{7,6},{8,11},{9,8},{10,9... | collective-permute-start | bytes 2359304 | tf_op jit(solution)/shard_map/ppermute | solution.py:284
  215.3 37.3 %collective-permute-start.8 = (bf16[192,2048]{1,0:T(8,128)(2,1)}, bf16[192,2048]{1,0:T(8,128)(2,1)}, u32[]{:S(2)}, u32[]{:S(2)}) collective-permute-start(bf16[192,2048]{1,0:T(8,128)(2,1)} %bitcast.9), channel_id=1, source_target_pairs={{0,1},{1,2},{2,3},{3,0},{4,5},{5,6},{6,7},{7,4},{8,9},{9,10},{10,1... | collective-permute-start | bytes 2359304 | tf_op jit(solution)/shard_map/ppermute | solution.py:284
  250.2 6.7 %copy-start.2 = (bf16[1,2048,768]{2,1,0:T(8,128)(2,1)S(1)}, bf16[1,2048,768]{2,1,0:T(8,128)(2,1)}, u32[]{:S(2)}) copy-start(bf16[1,2048,768]{2,1,0:T(8,128)(2,1)} %param.19) | copy-start | bytes 9437188
  252.3 21.6 %collective-permute-start.7 = (bf16[192,768]{1,0:T(8,128)(2,1)S(1)}, bf16[192,768]{1,0:T(8,128)(2,1)S(1)}, u32[]{:S(2)}, u32[]{:S(2)}) collective-permute-start(bf16[192,768]{1,0:T(8,128)(2,1)S(1)} %multiply_convert_fusion.2), channel_id=1, source_target_pairs={{0,1},{1,2},{2,3},{3,0},{4,5},{5,6},{6,7},{7,4},{8,9},{9,10},{10,1... | collective-permute-start | bytes 884744 | tf_op jit(solution)/shard_map/ppermute | solution.py:344
  253.6 15.3 %collective-permute-start.10 = (bf16[96,2048]{1,0:T(8,128)(2,1)S(1)}, bf16[96,2048]{1,0:T(8,128)(2,1)S(1)}, u32[]{:S(2)}, u32[]{:S(2)}) collective-permute-start(bf16[96,2048]{1,0:T(8,128)(2,1)S(1)} %slice.24), channel_id=1, source_target_pairs={{0,1},{1,2},{2,3},{3,0},{4,5},{5,6},{6,7},{7,4},{8,9},{9,10},{10,1... | collective-permute-start | bytes 1179656 | tf_op jit(solution)/shard_map/ppermute | solution.py:289
  256.5 12.7 %collective-permute-start.11 = (bf16[96,2048]{1,0:T(8,128)(2,1)S(1)}, bf16[96,2048]{1,0:T(8,128)(2,1)S(1)}, u32[]{:S(2)}, u32[]{:S(2)}) collective-permute-start(bf16[96,2048]{1,0:T(8,128)(2,1)S(1)} %slice.25), channel_id=1, source_target_pairs={{0,3},{1,0},{2,1},{3,2},{4,7},{5,4},{6,5},{7,6},{8,11},{9,8},{10,9... | collective-permute-start | bytes 1179656 | tf_op jit(solution)/shard_map/ppermute | solution.py:289
  268.9 17.4 %collective-permute-start.9 = (bf16[192,768]{1,0:T(8,128)(2,1)S(1)}, bf16[192,768]{1,0:T(8,128)(2,1)S(1)}, u32[]{:S(2)}, u32[]{:S(2)}) collective-permute-start(bf16[192,768]{1,0:T(8,128)(2,1)S(1)} %multiply_convert_fusion.1), channel_id=1, source_target_pairs={{0,3},{1,0},{2,1},{3,2},{4,7},{5,4},{6,5},{7,6},{8,11},{9,8},{10,9... | collective-permute-start | bytes 884744 | tf_op jit(solution)/shard_map/ppermute | solution.py:345
  270.1 3.8 %copy-start.4 = (f32[192,2048]{1,0:T(8,128)S(1)}, f32[192,2048]{1,0:T(8,128)}, u32[]{:S(2)}) copy-start(f32[192,2048]{1,0:T(8,128)} %fusion.29) | copy-start | bytes 4718596
  270.9 12.7 %collective-permute-start.12 = (bf16[192,768]{1,0:T(8,128)(2,1)S(1)}, bf16[192,768]{1,0:T(8,128)(2,1)S(1)}, u32[]{:S(2)}, u32[]{:S(2)}) collective-permute-start(bf16[192,768]{1,0:T(8,128)(2,1)S(1)} %multiply_convert_fusion), channel_id=1, source_target_pairs={{0,2},{1,3},{2,0},{3,1},{4,6},{5,7},{6,4},{7,5},{8,10},{9,11},{10,... | collective-permute-start | bytes 884744 | tf_op jit(solution)/shard_map/ppermute | solution.py:347
  289.2 15.0 %copy-start.8 = (f32[64,2]{0,1:T(2,128)S(1)}, f32[64,2]{0,1:T(2,128)}, u32[]{:S(2)}) copy-start(f32[64,2]{0,1:T(2,128)} %param.18) | copy-start | bytes 1540
  290.8 35.1 %all-to-all-start.2 = ((bf16[64,3,2048]{2,1,0:T(4,128)(2,1)}), bf16[64,3,2048]{2,1,0:T(4,128)(2,1)}, u32[]{:S(2)}, u32[]{:S(2)}) async-start(bf16[64,3,2048]{2,1,0:T(4,128)(2,1)} %bitcast.66), calls=%async_computation.2 | async-start | bytes 2097152 | tf_op jit(solution)/shard_map/all_to_all | solution.py:356
  297.4 50.2 %collective-permute-start.15 = (f32[64,2048]{1,0:T(8,128)}, f32[64,2048]{1,0:T(8,128)}, u32[]{:S(2)}, u32[]{:S(2)}) collective-permute-start(f32[64,2048]{1,0:T(8,128)} %get-tuple-element.18), channel_id=1, source_target_pairs={{0,0},{1,1},{2,254},{3,255},{4,4},{5,5},{6,250},{7,251},{8,8},{9,9... | collective-permute-start | bytes 1572872 | tf_op jit(solution)/shard_map/ppermute | solution.py:325
Sparse Core Ops, SparseCore 0:
  30.7 40.2 all-gather.3

commit v4 on v3

--- a/solution.py
+++ b/solution.py
@@ -22,6 +22,8 @@
 
 
 SAFE_SCORE = 60.0
+STEP = 512
+PAIRS = 2
 
 
 def bf16_pieces(values):
@@ -53,7 +55,7 @@
 
 def attend_body(index_ref, qa_ref, qb_ref, own_ref, other_ref, out_ref, qt_ref, max_ref, acc_ref, *, blocks, heads):
     columns = heads * HALF
-    step = 256
+    step = STEP
     own_index = index_ref[0]
     core = own_index % 2
     picked = 3 * heads
@@ -89,11 +91,13 @@
     bounded = largest_query * largest_key <= SAFE_SCORE**2
     acc_ref[...] = jnp.zeros(acc_ref.shape, jnp.float32)
 
-    def operands(pair):
-        tile = jnp.concatenate([own_ref[pair], other_ref[pair]], axis=1)
+    def operands(pair, count=1):
+        tile = jnp.concatenate(
+            [r[pair + n] for n in range(count) for r in (own_ref, other_ref)], axis=1
+        )
         keys = tile[:KEY_ROWS].astype(jnp.float32).T.astype(jnp.bfloat16)
         values = jnp.concatenate(
-            [tile[KEY_ROWS:], jnp.ones((16, 2 * BLOCK), jnp.bfloat16)], axis=0
+            [tile[KEY_ROWS:], jnp.ones((16, tile.shape[1]), jnp.bfloat16)], axis=0
         )
         return keys, values
 
@@ -108,8 +112,8 @@
         index = jnp.where(which == 0, own_index, blocks - 1 - own_index)
         return index // 2, index * BLOCK + which * HALF
 
-    def plain(which, pair, first_row):
-        keys, values = operands(pair)
+    def plain(which, pair, first_row, count=1):
+        keys, values = operands(pair, count)
         for at in range(0, columns, step):
             cols = slice(at, at + step)
             scores = jnp.dot(keys, qt_ref[which, :, cols], preferred_element_type=jnp.float32)
@@ -146,7 +150,16 @@
                 plain(which, pair, None)
                 return inner
 
-            lax.fori_loop(0, last_pair, full, 0)
+            def many(group, inner):
+                plain(which, group * PAIRS, None, PAIRS)
+                return inner
+
+            groups = last_pair // PAIRS
+            if PAIRS > 1:
+                lax.fori_loop(0, groups, many, 0)
+                lax.fori_loop(groups * PAIRS, last_pair, full, 0)
+            else:
+                lax.fori_loop(0, last_pair, full, 0)
             plain(which, last_pair, first_row)
             return carry
 
@@ -299,11 +312,12 @@
     mirrored_queries = lax.ppermute(queries[HALF:], SP, mirror)
     near = lax.all_gather(block, "sp_1")
     near, mirrored_queries = lax.optimization_barrier((near, mirrored_queries))
+    held_residual = lax.ppermute(residual_in, SP_TP, whole)
+    held_routes = lax.ppermute(routes, SP_TP, whole)
     own = lax.all_gather(near, "sp_0").reshape(-1, *block.shape)
+    own, held_residual, held_routes = lax.optimization_barrier((own, held_residual, held_routes))
     down_own = expert_down[0]
     down_before, down_after = neighbours(down_own)
-    held_residual = lax.ppermute(residual_in, SP_TP, whole)
-    held_routes = lax.ppermute(routes, SP_TP, whole)
     other = lax.ppermute(own, "sp_2", [(0, 1), (1, 0)])
     attended = attend_rows(index.reshape(1), queries[:HALF], mirrored_queries, own, other)
     down_before, down_after, attended = lax.optimization_barrier(
@@ -340,6 +354,7 @@
 
     rows_before, rows_after = neighbours(rows_own)
     units_own = units(rows_own)
+    rows_before, hidden_state = lax.optimization_barrier((rows_before, hidden_state))
     rows_across = opposite(rows_before, rows_after)
     units_from_before = lax.ppermute(units(rows_after), "tp", up)
     units_from_after = lax.ppermute(units(rows_before), "tp", down)

time: 358 us -> 321 us (0.90)
  Pallas kernels: 53.7 us -> 29.7 us
  waiting for transfers between devices: 142 us -> 131 us
    pallas_call x1, Pallas kernels: 46.2 us -> 22.2 us  [attend_rows(): pl.pallas_call(functools.partial(attend_body, blocks=blocks, heads=heads)...]
    all_gather x1, waiting for transfers between devices: 38.3 us -> 20.3 us  [local(): own = lax.all_gather(near, 'sp_0').reshape(-1, *block.shape)]
    ppermute x1, waiting for transfers between devices: 19 us -> 5.99 us  [local(): hidden_state = lax.ppermute(held_hidden, SP_TP, whole)]
    all_to_all x1, waiting for transfers between devices: 0.01 us -> 12.8 us  [local(): lax.all_to_all(partial.reshape(head_devices, -1, partial.shape[1]), 'tp',...]
    ppermute x1, waiting for transfers between devices: 5.36 us -> 15.3 us  [local(): held_routes = lax.ppermute(routes, SP_TP, whole)]
    ppermute x4, waiting for transfers between devices: 20.7 us -> 10.7 us  [neighbours(): return (lax.ppermute(array, 'tp', up), lax.ppermute(array, 'tp', down))]
    all_to_all x1, waiting for transfers between devices: 21.1 us -> 28 us  [local(): returned = lax.all_to_all(leaving, SP, 0, 0, tiled=True).transpose(1, 0, 2)]
    ppermute x1, starting transfers between devices: 6.76 us -> 2.23 us  [local(): hidden_state = lax.ppermute(held_hidden, SP_TP, whole)]
  transfers between devices with their start and end apart: 20 -> 20, of which waited for: 9 -> 10; matrix products, arithmetic and copies ran while one was open for 11% -> 12% of each run, Pallas kernels for 13% -> 7%
where the time goes in v4:
time: 321 us; the launch traced here: 319 us
  waiting for transfers between devices  131 us (41%)
  starting transfers between devices  79.7 us (25%)
  Pallas kernels  29.7 us (9%)
  matrix products  29.2 us (9%)
  local copies, waits for them, and re-layouts  21.8 us (7%)
  between operations  13.6 us (4%)
  blocking collectives  13.5 us (4%)
    all_to_all x1, starting transfers between devices, local(): lax.all_to_all(slots.transpose(1, 0, 2), SP_TP, 0, 0, axis_index_groups=r...  31.1 us
    all_to_all x1, waiting for transfers between devices, local(): returned = lax.all_to_all(leaving, SP, 0, 0, tiled=True).transpose(1, 0, 2)  28 us
    pallas_call x1, Pallas kernels, attend_rows(): pl.pallas_call(functools.partial(attend_body, blocks=blocks, heads=heads)...  22.2 us
    all_gather x1, waiting for transfers between devices, local(): own = lax.all_gather(near, 'sp_0').reshape(-1, *block.shape)  20.3 us
    ppermute x1, waiting for transfers between devices, local(): held_routes = lax.ppermute(routes, SP_TP, whole)  15.3 us
    all_to_all x1, waiting for transfers between devices, local(): lax.all_to_all(slots.transpose(1, 0, 2), SP_TP, 0, 0, axis_index_groups=r...  15 us
    all_gather x1, blocking collectives, local(): near = lax.all_gather(block, 'sp_1')  13.5 us
    all_to_all x1, waiting for transfers between devices, local(): lax.all_to_all(partial.reshape(head_devices, -1, partial.shape[1]), 'tp',...  12.8 us
  transfers between devices with their start and end apart: 20, of which 10 were waited for; matrix products, arithmetic and copies ran while one was open for 12% of the time, Pallas kernels for 7%

profile of v4, /device:TPU:6, one launch (start us, length us, event | category | flops | bytes accessed | tf_op | source)
XLA Modules:
  0.0 318.8 jit_solution(6926277030396038165)
XLA Ops:
  6.5 1.1 fusion.40
  7.7 7.8 %collective-permute-start.2 = (bf16[128,512]{1,0:T(8,128)(2,1)S(1)}, bf16[128,512]{1,0:T(8,128)(2,1)S(1)}, u32[]{:S(2)}, u32[]{:S(2)}) collective-permute-start(bf16[128,512]{1,0:T(8,128)(2,1)S(1)} %get-tuple-element.29), channel_id=1, source_target_pairs={{0,252},{4,248},{8,244},{12,240},{16,236},{20,232},{24,228},{28,22... | collective-permute-start | bytes 393224 | tf_op jit(solution)/shard_map/ppermute | solution.py:312
  15.5 1.6 prepare_keys.1
  17.1 13.5 %all-gather = bf16[640,256]{1,0:T(8,128)(2,1)} all-gather(bf16[160,256]{1,0:T(8,128)(2,1)} %prepare_keys.1), channel_id=2, replica_groups=mesh['sp_0'=8,'sp_1'=4,'sp_2'=2,'tp'=4] {'sp_1'}, dimensions={0}, use_global_device_ids=true | all-gather | bytes 409600 | tf_op jit(solution)/shard_map/all_gather | solution.py:313
  31.1 1.5 collective-permute-start.1
  32.7 1.9 collective-permute-start.3
  35.4 7.0 %collective-permute-start.4 = (s32[64,2]{1,0:T(8,128)S(1)}, s32[64,2]{1,0:T(8,128)S(1)}, u32[]{:S(2)}, u32[]{:S(2)}) collective-permute-start(s32[64,2]{1,0:T(8,128)S(1)} %copy.21.routes_ref), channel_id=1, source_target_pairs={{0,0},{1,1},{2,254},{3,255},{4,4},{5,5},{6,250},{7,251},{8,8},{9,9... | collective-permute-start | bytes 1544 | tf_op jit(solution)/shard_map/ppermute | solution.py:316
  42.4 15.3 %collective-permute-done.4 = s32[64,2]{1,0:T(8,128)S(1)} collective-permute-done((s32[64,2]{1,0:T(8,128)S(1)}, s32[64,2]{1,0:T(8,128)S(1)}, u32[]{:S(2)}, u32[]{:S(2)}) %collective-permute-start.4) | collective-permute-done | bytes 544 | tf_op jit(solution)/shard_map/ppermute | solution.py:316
  57.7 20.3 %all-gather.4.cloned.1.call-done.own_ref = bf16[32,160,256]{2,1,0:T(8,128)(2,1)} async-done(((bf16[4,160,256]{2,1,0:T(8,128)(2,1)}), bf16[32,160,256]{2,1,0:T(8,128)(2,1)}) %all-gather.4.cloned.1.call-update) | async-done | bytes 2621456 | tf_op jit(solution)/shard_map/all_gather | solution.py:317
  78.0 5.2 %collective-permute-done.5.other_ref = bf16[32,160,256]{2,1,0:T(8,128)(2,1)} collective-permute-done((bf16[32,160,256]{2,1,0:T(8,128)(2,1)}, bf16[32,160,256]{2,1,0:T(8,128)(2,1)}, u32[]{:S(2)}, u32[]{:S(2)}) %collective-permute-start.5) | collective-permute-done | bytes 2621472 | tf_op jit(solution)/shard_map/ppermute | solution.py:321
  83.2 1.7 copy-done.1
  85.0 22.2 %attend_rows.1 = bf16[2,128,512]{2,1,0:T(8,128)(2,1)S(1)} custom-call(s32[1]{0:T(128)} %bitcast.1.index_ref, bf16[128,512]{1,0:T(8,128)(2,1)S(1)} %get-tuple-element.30.qa_ref, bf16[128,512]{1,0:T(8,128)(2,1)S(1)} %collective-permute-done.2.qb_ref, bf16[32,160,256]{2,1,0:T(8,128)(2,1)S(1)} %copy-done.1, bf16[32,160,256]{2,1,0:T(8,128)(2,1)} %collective-permute-done.5.other_ref), custom_call_target="tpu_custom_call" | custom-call | tf_op jit(solution)/shard_map/attend_rows/pallas_call | solution.py:196
  107.1 1.8 convolution_convert_fusion
  109.0 4.8 %all-to-all-start = ((bf16[4,64,2048]{2,1,0:T(8,128)(2,1)}), bf16[4,64,2048]{2,1,0:T(8,128)(2,1)}, u32[]{:S(2)}, u32[]{:S(2)}) async-start(bf16[4,64,2048]{2,1,0:T(8,128)(2,1)} %bitcast.67), calls=%async_computation | async-start | bytes 2097152 | tf_op jit(solution)/shard_map/all_to_all | solution.py:330
  114.4 12.8 %all-to-all-done.parts_ref = bf16[4,64,2048]{2,1,0:T(8,128)(2,1)} async-done(((bf16[4,64,2048]{2,1,0:T(8,128)(2,1)}), bf16[4,64,2048]{2,1,0:T(8,128)(2,1)}, u32[]{:S(2)}, u32[]{:S(2)}) %all-to-all-start) | async-done | bytes 1048608 | tf_op jit(solution)/shard_map/all_to_all | solution.py:330
  127.3 3.0 dispatch.1
  130.2 2.8 copy.22
  133.0 31.1 %all-to-all-start.1 = ((bf16[64,3,2048]{2,1,0:T(4,128)(2,1)}), bf16[64,3,2048]{2,1,0:T(4,128)(2,1)}, u32[]{:S(2)}, u32[]{:S(2)}) async-start(bf16[64,3,2048]{2,1,0:T(4,128)(2,1)} %copy.22), calls=%async_computation.1 | async-start | bytes 2097152 | tf_op jit(solution)/shard_map/all_to_all | solution.py:345
  164.1 2.7 slice.22
  166.8 2.8 slice.23
  169.6 2.0 collective-permute-start.15
  171.6 2.2 collective-permute-start.9
  173.9 15.0 %all-to-all-done.1 = bf16[64,3,2048]{2,1,0:T(4,128)(2,1)} async-done(((bf16[64,3,2048]{2,1,0:T(4,128)(2,1)}), bf16[64,3,2048]{2,1,0:T(4,128)(2,1)}, u32[]{:S(2)}, u32[]{:S(2)}) %all-to-all-start.1) | async-done | bytes 786464 | tf_op jit(solution)/shard_map/all_to_all | solution.py:345
  188.9 2.7 copy.23
  191.6 3.2 %collective-permute-start.8 = (bf16[192,2048]{1,0:T(8,128)(2,1)}, bf16[192,2048]{1,0:T(8,128)(2,1)}, u32[]{:S(2)}, u32[]{:S(2)}) collective-permute-start(bf16[192,2048]{1,0:T(8,128)(2,1)} %bitcast.9), channel_id=1, source_target_pairs={{0,1},{1,2},{2,3},{3,0},{4,5},{5,6},{6,7},{7,4},{8,9},{9,10},{10,1... | collective-permute-start | bytes 2359304 | tf_op jit(solution)/shard_map/ppermute | solution.py:297
  194.8 3.7 %fusion.18 = f32[192,768]{1,0:T(8,128)} fusion(bf16[192,2048]{1,0:T(8,128)(2,1)} %bitcast.9, bf16[1,2048,768]{2,1,0:T(8,128)(2,1)} %param.19), kind=kOutput, calls=%fused_computation.18 | convolution fusion | flops 603979776 | bytes 4521984 | tf_op jit(solution)/shard_map/dot_general | solution.py:351
  198.6 5.1 %fusion.29 = f32[192,2048]{1,0:T(8,128)} fusion(bf16[192,2048]{1,0:T(8,128)(2,1)} %bitcast.9, bf16[1,2048,768]{2,1,0:T(8,128)(2,1)S(1)} %copy-done, f32[192,768]{1,0:T(8,128)} %fusion.18, bf16[1,768,2048]{2,1,0:T(8,128)(2,1)} %param.21), kind=kOutput, calls=%fused_computation.28 | convolution fusion | flops 1208844288 | bytes 9240576 | tf_op jit(solution)/shard_map/dot_general | solution.py:363
  203.7 6.0 %collective-permute-done.9.hidden_ref = f32[64,2048]{1,0:T(8,128)} collective-permute-done((f32[64,2048]{1,0:T(8,128)}, f32[64,2048]{1,0:T(8,128)}, u32[]{:S(2)}, u32[]{:S(2)}) %collective-permute-start.9) | collective-permute-done | bytes 524320 | tf_op jit(solution)/shard_map/ppermute | solution.py:339
  209.7 10.7 %collective-permute-done.8 = bf16[192,2048]{1,0:T(8,128)(2,1)} collective-permute-done((bf16[192,2048]{1,0:T(8,128)(2,1)}, bf16[192,2048]{1,0:T(8,128)(2,1)}, u32[]{:S(2)}, u32[]{:S(2)}) %collective-permute-start.8) | collective-permute-done | bytes 786464 | tf_op jit(solution)/shard_map/ppermute | solution.py:297
  220.4 1.0 slice.20
  221.4 2.9 fusion.14
  224.4 2.0 fusion.16
  226.4 1.9 multiply_convert_fusion.2
  228.3 1.5 collective-permute-start.7
  229.9 1.0 slice.24
  230.9 2.0 collective-permute-start.12
  233.0 1.9 multiply_convert_fusion.1
  234.9 10.1 %collective-permute-done.11 = bf16[96,2048]{1,0:T(8,128)(2,1)S(1)} collective-permute-done((bf16[96,2048]{1,0:T(8,128)(2,1)S(1)}, bf16[96,2048]{1,0:T(8,128)(2,1)S(1)}, u32[]{:S(2)}, u32[]{:S(2)}) %collective-permute-start.11) | collective-permute-done | bytes 393248 | tf_op jit(solution)/shard_map/ppermute | solution.py:302
  246.9 4.5 %collective-permute-start.13 = (bf16[192,768]{1,0:T(8,128)(2,1)S(1)}, bf16[192,768]{1,0:T(8,128)(2,1)S(1)}, u32[]{:S(2)}, u32[]{:S(2)}) collective-permute-start(bf16[192,768]{1,0:T(8,128)(2,1)S(1)} %multiply_convert_fusion), channel_id=1, source_target_pairs={{0,2},{1,3},{2,0},{3,1},{4,6},{5,7},{6,4},{7,5},{8,10},{9,11},{10,... | collective-permute-start | bytes 884744 | tf_op jit(solution)/shard_map/ppermute | solution.py:362
  251.4 2.7 convolution_add_fusion.1
  254.1 7.1 %collective-permute-done.13 = bf16[192,768]{1,0:T(8,128)(2,1)S(1)} collective-permute-done((bf16[192,768]{1,0:T(8,128)(2,1)S(1)}, bf16[192,768]{1,0:T(8,128)(2,1)S(1)}, u32[]{:S(2)}, u32[]{:S(2)}) %collective-permute-start.13) | collective-permute-done | bytes 294944 | tf_op jit(solution)/shard_map/ppermute | solution.py:362
  261.3 2.7 fusion
  264.0 2.8 fusion.21
  266.8 1.6 copy.30
  268.4 9.1 %all-to-all-start.2 = ((bf16[64,3,2048]{2,1,0:T(4,128)(2,1)}), bf16[64,3,2048]{2,1,0:T(4,128)(2,1)}, u32[]{:S(2)}, u32[]{:S(2)}) async-start(bf16[64,3,2048]{2,1,0:T(4,128)(2,1)} %bitcast.66), calls=%async_computation.2 | async-start | bytes 2097152 | tf_op jit(solution)/shard_map/all_to_all | solution.py:371
  278.3 28.0 %all-to-all-done.2 = bf16[64,3,2048]{2,1,0:T(4,128)(2,1)} async-done(((bf16[64,3,2048]{2,1,0:T(4,128)(2,1)}), bf16[64,3,2048]{2,1,0:T(4,128)(2,1)}, u32[]{:S(2)}, u32[]{:S(2)}) %all-to-all-start.2) | async-done | bytes 786464 | tf_op jit(solution)/shard_map/all_to_all | solution.py:371
  306.3 2.7 copy.31
  309.0 3.0 combine.1
  (38 shorter events, 4.7 us)
Async XLA Ops:
  6.5 192.1 %copy-start = (bf16[1,2048,768]{2,1,0:T(8,128)(2,1)S(1)}, bf16[1,2048,768]{2,1,0:T(8,128)(2,1)}, u32[]{:S(2)}) copy-start(bf16[1,2048,768]{2,1,0:T(8,128)(2,1)} %param.20) | copy-start | bytes 9437188
  6.5 71.4 %all-gather.4.cloned.1.call-start = ((), (), s32[]{:S(2)}) async-start(), calls=%async_computation.3 | async-start | bytes 2949120 | tf_op jit(solution)/shard_map/all_gather | solution.py:317
  7.7 22.9 %collective-permute-start.2 = (bf16[128,512]{1,0:T(8,128)(2,1)S(1)}, bf16[128,512]{1,0:T(8,128)(2,1)S(1)}, u32[]{:S(2)}, u32[]{:S(2)}) collective-permute-start(bf16[128,512]{1,0:T(8,128)(2,1)S(1)} %get-tuple-element.29), channel_id=1, source_target_pairs={{0,252},{4,248},{8,244},{12,240},{16,236},{20,232},{24,228},{28,22... | collective-permute-start | bytes 393224 | tf_op jit(solution)/shard_map/ppermute | solution.py:312
  30.6 76.5 %collective-permute-start = (bf16[768,2048]{1,0:T(8,128)(2,1)}, bf16[768,2048]{1,0:T(8,128)(2,1)}, u32[]{:S(2)}, u32[]{:S(2)}) collective-permute-start(bf16[768,2048]{1,0:T(8,128)(2,1)} %bitcast.74), channel_id=1, source_target_pairs={{0,1},{1,2},{2,3},{3,0},{4,5},{5,6},{6,7},{7,4},{8,9},{9,10},{10,1... | collective-permute-start | bytes 9437192 | tf_op jit(solution)/shard_map/ppermute | solution.py:297
  31.1 76.0 %collective-permute-start.1 = (bf16[768,2048]{1,0:T(8,128)(2,1)}, bf16[768,2048]{1,0:T(8,128)(2,1)}, u32[]{:S(2)}, u32[]{:S(2)}) collective-permute-start(bf16[768,2048]{1,0:T(8,128)(2,1)} %bitcast.75), channel_id=1, source_target_pairs={{0,3},{1,0},{2,1},{3,2},{4,7},{5,4},{6,5},{7,6},{8,11},{9,8},{10,9... | collective-permute-start | bytes 9437192 | tf_op jit(solution)/shard_map/ppermute | solution.py:297
  32.7 25.0 %collective-permute-start.3 = (bf16[64,2048]{1,0:T(8,128)(2,1)}, bf16[64,2048]{1,0:T(8,128)(2,1)}, u32[]{:S(2)}, u32[]{:S(2)}) collective-permute-start(bf16[64,2048]{1,0:T(8,128)(2,1)} %param.14), channel_id=1, source_target_pairs={{0,0},{1,1},{2,254},{3,255},{4,4},{5,5},{6,250},{7,251},{8,8},{9,9... | collective-permute-start | bytes 786440 | tf_op jit(solution)/shard_map/ppermute | solution.py:315
  35.4 73.6 %copy-start.5 = (s32[64,2]{1,0:T(8,128)}, s32[64,2]{1,0:T(8,128)S(1)}, u32[]{:S(2)}) copy-start(s32[64,2]{1,0:T(8,128)S(1)} %copy.21.routes_ref) | copy-start | bytes 1540
  35.4 22.3 %collective-permute-start.4 = (s32[64,2]{1,0:T(8,128)S(1)}, s32[64,2]{1,0:T(8,128)S(1)}, u32[]{:S(2)}, u32[]{:S(2)}) collective-permute-start(s32[64,2]{1,0:T(8,128)S(1)} %copy.21.routes_ref), channel_id=1, source_target_pairs={{0,0},{1,1},{2,254},{3,255},{4,4},{5,5},{6,250},{7,251},{8,8},{9,9... | collective-permute-start | bytes 1544 | tf_op jit(solution)/shard_map/ppermute | solution.py:316
  78.0 5.3 %collective-permute-start.5 = (bf16[32,160,256]{2,1,0:T(8,128)(2,1)}, bf16[32,160,256]{2,1,0:T(8,128)(2,1)}, u32[]{:S(2)}, u32[]{:S(2)}) collective-permute-start(bf16[32,160,256]{2,1,0:T(8,128)(2,1)} %all-gather.4.cloned.1.call-done.own_ref), channel_id=1, source_target_pairs={{0,4},{4,0},{1,5},{5,1},{2,6},{6,2},{3,7},{7,3},{8,12},{12,8},{9,1... | collective-permute-start | bytes 7864328 | tf_op jit(solution)/shard_map/ppermute | solution.py:321
  83.2 1.7 copy-start.1
  85.0 22.2 %copy-start.3 = (bf16[512,2048]{1,0:T(8,128)(2,1)S(1)}, bf16[512,2048]{1,0:T(8,128)(2,1)}, u32[]{:S(2)}) copy-start(bf16[512,2048]{1,0:T(8,128)(2,1)} %param.15) | copy-start | bytes 6291460
  109.0 18.3 %all-to-all-start = ((bf16[4,64,2048]{2,1,0:T(8,128)(2,1)}), bf16[4,64,2048]{2,1,0:T(8,128)(2,1)}, u32[]{:S(2)}, u32[]{:S(2)}) async-start(bf16[4,64,2048]{2,1,0:T(8,128)(2,1)} %bitcast.67), calls=%async_computation | async-start | bytes 2097152 | tf_op jit(solution)/shard_map/all_to_all | solution.py:330
  133.0 55.9 %all-to-all-start.1 = ((bf16[64,3,2048]{2,1,0:T(4,128)(2,1)}), bf16[64,3,2048]{2,1,0:T(4,128)(2,1)}, u32[]{:S(2)}, u32[]{:S(2)}) async-start(bf16[64,3,2048]{2,1,0:T(4,128)(2,1)} %copy.22), calls=%async_computation.1 | async-start | bytes 2097152 | tf_op jit(solution)/shard_map/all_to_all | solution.py:345
  166.8 87.3 %collective-permute-start.14 = (bf16[384,2048]{1,0:T(8,128)(2,1)}, bf16[384,2048]{1,0:T(8,128)(2,1)}, u32[]{:S(2)}, u32[]{:S(2)}) collective-permute-start(bf16[384,2048]{1,0:T(8,128)(2,1)} %slice.22), channel_id=1, source_target_pairs={{0,1},{1,2},{2,3},{3,0},{4,5},{5,6},{6,7},{7,4},{8,9},{9,10},{10,1... | collective-permute-start | bytes 4718600 | tf_op jit(solution)/shard_map/ppermute | solution.py:302
  169.6 84.5 %collective-permute-start.15 = (bf16[384,2048]{1,0:T(8,128)(2,1)}, bf16[384,2048]{1,0:T(8,128)(2,1)}, u32[]{:S(2)}, u32[]{:S(2)}) collective-permute-start(bf16[384,2048]{1,0:T(8,128)(2,1)} %slice.23), channel_id=1, source_target_pairs={{0,3},{1,0},{2,1},{3,2},{4,7},{5,4},{6,5},{7,6},{8,11},{9,8},{10,9... | collective-permute-start | bytes 4718600 | tf_op jit(solution)/shard_map/ppermute | solution.py:302
  171.6 38.1 %collective-permute-start.9 = (f32[64,2048]{1,0:T(8,128)}, f32[64,2048]{1,0:T(8,128)}, u32[]{:S(2)}, u32[]{:S(2)}) collective-permute-start(f32[64,2048]{1,0:T(8,128)} %get-tuple-element.25), channel_id=1, source_target_pairs={{0,0},{1,1},{2,254},{3,255},{4,4},{5,5},{6,250},{7,251},{8,8},{9,9... | collective-permute-start | bytes 1572872 | tf_op jit(solution)/shard_map/ppermute | solution.py:339
  191.6 32.8 %collective-permute-start.6 = (bf16[192,2048]{1,0:T(8,128)(2,1)}, bf16[192,2048]{1,0:T(8,128)(2,1)}, u32[]{:S(2)}, u32[]{:S(2)}) collective-permute-start(bf16[192,2048]{1,0:T(8,128)(2,1)} %bitcast.9), channel_id=1, source_target_pairs={{0,3},{1,0},{2,1},{3,2},{4,7},{5,4},{6,5},{7,6},{8,11},{9,8},{10,9... | collective-permute-start | bytes 2359304 | tf_op jit(solution)/shard_map/ppermute | solution.py:297
  191.6 28.8 %collective-permute-start.8 = (bf16[192,2048]{1,0:T(8,128)(2,1)}, bf16[192,2048]{1,0:T(8,128)(2,1)}, u32[]{:S(2)}, u32[]{:S(2)}) collective-permute-start(bf16[192,2048]{1,0:T(8,128)(2,1)} %bitcast.9), channel_id=1, source_target_pairs={{0,1},{1,2},{2,3},{3,0},{4,5},{5,6},{6,7},{7,4},{8,9},{9,10},{10,1... | collective-permute-start | bytes 2359304 | tf_op jit(solution)/shard_map/ppermute | solution.py:297
  203.7 20.7 %copy-start.2 = (bf16[1,2048,768]{2,1,0:T(8,128)(2,1)S(1)}, bf16[1,2048,768]{2,1,0:T(8,128)(2,1)}, u32[]{:S(2)}) copy-start(bf16[1,2048,768]{2,1,0:T(8,128)(2,1)} %param.19) | copy-start | bytes 9437188
  228.3 23.1 %collective-permute-start.7 = (bf16[192,768]{1,0:T(8,128)(2,1)S(1)}, bf16[192,768]{1,0:T(8,128)(2,1)S(1)}, u32[]{:S(2)}, u32[]{:S(2)}) collective-permute-start(bf16[192,768]{1,0:T(8,128)(2,1)S(1)} %multiply_convert_fusion.2), channel_id=1, source_target_pairs={{0,1},{1,2},{2,3},{3,0},{4,5},{5,6},{6,7},{7,4},{8,9},{9,10},{10,1... | collective-permute-start | bytes 884744 | tf_op jit(solution)/shard_map/ppermute | solution.py:359
  229.8 15.1 %collective-permute-start.11 = (bf16[96,2048]{1,0:T(8,128)(2,1)S(1)}, bf16[96,2048]{1,0:T(8,128)(2,1)S(1)}, u32[]{:S(2)}, u32[]{:S(2)}) collective-permute-start(bf16[96,2048]{1,0:T(8,128)(2,1)S(1)} %slice.20), channel_id=1, source_target_pairs={{0,1},{1,2},{2,3},{3,0},{4,5},{5,6},{6,7},{7,4},{8,9},{9,10},{10,1... | collective-permute-start | bytes 1179656 | tf_op jit(solution)/shard_map/ppermute | solution.py:302
  230.9 14.3 %collective-permute-start.12 = (bf16[96,2048]{1,0:T(8,128)(2,1)S(1)}, bf16[96,2048]{1,0:T(8,128)(2,1)S(1)}, u32[]{:S(2)}, u32[]{:S(2)}) collective-permute-start(bf16[96,2048]{1,0:T(8,128)(2,1)S(1)} %slice.24), channel_id=1, source_target_pairs={{0,3},{1,0},{2,1},{3,2},{4,7},{5,4},{6,5},{7,6},{8,11},{9,8},{10,9... | collective-permute-start | bytes 1179656 | tf_op jit(solution)/shard_map/ppermute | solution.py:302
  245.0 19.0 %collective-permute-start.10 = (bf16[192,768]{1,0:T(8,128)(2,1)S(1)}, bf16[192,768]{1,0:T(8,128)(2,1)S(1)}, u32[]{:S(2)}, u32[]{:S(2)}) collective-permute-start(bf16[192,768]{1,0:T(8,128)(2,1)S(1)} %multiply_convert_fusion.1), channel_id=1, source_target_pairs={{0,3},{1,0},{2,1},{3,2},{4,7},{5,4},{6,5},{7,6},{8,11},{9,8},{10,9... | collective-permute-start | bytes 884744 | tf_op jit(solution)/shard_map/ppermute | solution.py:360
  246.1 5.3 %copy-start.4 = (f32[192,2048]{1,0:T(8,128)S(1)}, f32[192,2048]{1,0:T(8,128)}, u32[]{:S(2)}) copy-start(f32[192,2048]{1,0:T(8,128)} %fusion.29) | copy-start | bytes 4718596
  246.9 14.4 %collective-permute-start.13 = (bf16[192,768]{1,0:T(8,128)(2,1)S(1)}, bf16[192,768]{1,0:T(8,128)(2,1)S(1)}, u32[]{:S(2)}, u32[]{:S(2)}) collective-permute-start(bf16[192,768]{1,0:T(8,128)(2,1)S(1)} %multiply_convert_fusion), channel_id=1, source_target_pairs={{0,2},{1,3},{2,0},{3,1},{4,6},{5,7},{6,4},{7,5},{8,10},{9,11},{10,... | collective-permute-start | bytes 884744 | tf_op jit(solution)/shard_map/ppermute | solution.py:362
  266.8 10.8 %copy-start.6 = (f32[64,2]{0,1:T(2,128)S(1)}, f32[64,2]{0,1:T(2,128)}, u32[]{:S(2)}) copy-start(f32[64,2]{0,1:T(2,128)} %param.18) | copy-start | bytes 1540
  268.4 37.8 %all-to-all-start.2 = ((bf16[64,3,2048]{2,1,0:T(4,128)(2,1)}), bf16[64,3,2048]{2,1,0:T(4,128)(2,1)}, u32[]{:S(2)}, u32[]{:S(2)}) async-start(bf16[64,3,2048]{2,1,0:T(4,128)(2,1)} %bitcast.66), calls=%async_computation.2 | async-start | bytes 2097152 | tf_op jit(solution)/shard_map/all_to_all | solution.py:371
Sparse Core Ops, SparseCore 0:
  30.7 47.2 all-gather.3

commit v5 on v4

--- a/solution.py
+++ b/solution.py
@@ -223,19 +223,42 @@
     return first, second, named, earlier
 
 
-def dispatch_body(parts_ref, residual_ref, gain_ref, routes_ref, hidden_ref, slots_ref, *, capacity):
+def spread_rows(tiles_ref, rows, slot, capacity):
+    count, width = rows.shape
+    per_row = width // 128
+    for j in range(per_row):
+        at = pl.ds(slot * per_row + j, count, stride=capacity * per_row)
+        tiles_ref[at, :] = rows[:, j * 128 : (j + 1) * 128]
+
+
+def joined_rows(tiles_ref, slot, capacity, count, width):
+    per_row = width // 128
+    return jnp.concatenate(
+        [
+            tiles_ref[pl.ds(slot * per_row + j, count, stride=capacity * per_row), :]
+            for j in range(per_row)
+        ],
+        axis=1,
+    )
+
+
+def dispatch_body(parts_ref, residual_ref, gain_ref, routes_ref, hidden_ref, slots_ref, tiles_ref, *, capacity):
     mixed = jnp.sum(parts_ref[...].astype(jnp.float32), axis=0)
     hidden = residual_ref[...].astype(jnp.float32) + mixed
     hidden_ref[...] = hidden
     scale = lax.rsqrt(jnp.mean(hidden * hidden, axis=1, keepdims=True) + NORM_EPS)
     normed = (hidden * scale * gain_ref[...]).astype(jnp.bfloat16)
-    experts = slots_ref.shape[1]
+    experts = slots_ref.shape[0]
     _, _, named, earlier = routing(routes_ref, experts)
     for slot in range(capacity):
         chosen = jnp.where(earlier == slot, named, 0.0).T.astype(jnp.bfloat16)
-        slots_ref[slot] = jnp.dot(chosen, normed, preferred_element_type=jnp.float32).astype(
-            jnp.bfloat16
-        )
+        spread_rows(
+            tiles_ref,
+            jnp.dot(chosen, normed, preferred_element_type=jnp.float32),
+            slot,
+            capacity,
+        )
+    slots_ref[...] = tiles_ref[...].reshape(slots_ref.shape).astype(jnp.bfloat16)
 
 
 def dispatch(parts, residual, gain, routes, experts, capacity):
@@ -244,20 +267,59 @@
         functools.partial(dispatch_body, capacity=capacity),
         out_shape=[
             jax.ShapeDtypeStruct((rows, width), jnp.float32),
-            jax.ShapeDtypeStruct((capacity, experts, width), jnp.bfloat16),
+            jax.ShapeDtypeStruct((experts, capacity * width // 128, 128), jnp.bfloat16),
         ],
+        scratch_shapes=[pltpu.VMEM((experts * capacity * width // 128, 128), jnp.float32)],
         name="dispatch",
     )(parts, residual, gain.reshape(1, width), routes)
 
 
-def combine_body(returned_ref, hidden_ref, routes_ref, weight_ref, out_ref):
-    capacity, experts, _ = returned_ref.shape
+def arrange_body(arrived_ref, rows_ref, tiles_ref, *, capacity):
+    count = arrived_ref.shape[0]
+    tiles_ref[...] = arrived_ref[...].astype(jnp.float32).reshape(tiles_ref.shape)
+    for slot in range(capacity):
+        rows_ref[slot * count : (slot + 1) * count, :] = joined_rows(
+            tiles_ref, slot, capacity, count, rows_ref.shape[1]
+        ).astype(jnp.bfloat16)
+
+
+def arrange(arrived, capacity):
+    count, lines, lanes = arrived.shape
+    return pl.pallas_call(
+        functools.partial(arrange_body, capacity=capacity),
+        out_shape=jax.ShapeDtypeStruct((capacity * count, lines * lanes // capacity), jnp.bfloat16),
+        scratch_shapes=[pltpu.VMEM((count * lines, lanes), jnp.float32)],
+        name="arrange",
+    )(arrived)
+
+
+def spread_body(rows_ref, leaving_ref, tiles_ref, *, capacity):
+    count = leaving_ref.shape[0]
+    for slot in range(capacity):
+        spread_rows(tiles_ref, rows_ref[slot * count : (slot + 1) * count, :], slot, capacity)
+    leaving_ref[...] = tiles_ref[...].reshape(leaving_ref.shape).astype(jnp.bfloat16)
+
+
+def spread(rows, capacity):
+    count, width = rows.shape[0] // capacity, rows.shape[1]
+    lines = capacity * width // 128
+    return pl.pallas_call(
+        functools.partial(spread_body, capacity=capacity),
+        out_shape=jax.ShapeDtypeStruct((count, lines, 128), jnp.bfloat16),
+        scratch_shapes=[pltpu.VMEM((count * lines, 128), jnp.float32)],
+        name="spread",
+    )(rows)
+
+
+def combine_body(returned_ref, hidden_ref, routes_ref, weight_ref, out_ref, tiles_ref, *, capacity):
+    experts = returned_ref.shape[0]
+    tiles_ref[...] = returned_ref[...].astype(jnp.float32).reshape(tiles_ref.shape)
     first, second, _, earlier = routing(routes_ref, experts)
     weight = first * weight_ref[:, 0:1] + second * weight_ref[:, 1:2]
     total = hidden_ref[...]
     for slot in range(capacity):
         rest = jnp.where(earlier == slot, weight, 0.0)
-        rows = returned_ref[slot]
+        rows = joined_rows(tiles_ref, slot, capacity, experts, out_ref.shape[1]).astype(jnp.bfloat16)
         for _ in range(3):
             piece = rest.astype(jnp.bfloat16)
             rest = rest - piece.astype(jnp.float32)
@@ -265,10 +327,12 @@
     out_ref[...] = total.astype(jnp.bfloat16)
 
 
-def combine(returned, hidden, routes, route_weight):
-    return pl.pallas_call(
-        combine_body,
+def combine(returned, hidden, routes, route_weight, capacity):
+    experts, lines, lanes = returned.shape
+    return pl.pallas_call(
+        functools.partial(combine_body, capacity=capacity),
         out_shape=jax.ShapeDtypeStruct(hidden.shape, jnp.bfloat16),
+        scratch_shapes=[pltpu.VMEM((experts * lines, lanes), jnp.float32)],
         name="combine",
     )(returned, hidden, routes, route_weight)
 
@@ -315,15 +379,16 @@
     held_residual = lax.ppermute(residual_in, SP_TP, whole)
     held_routes = lax.ppermute(routes, SP_TP, whole)
     own = lax.all_gather(near, "sp_0").reshape(-1, *block.shape)
-    own, held_residual, held_routes = lax.optimization_barrier((own, held_residual, held_routes))
-    down_own = expert_down[0]
-    down_before, down_after = neighbours(down_own)
+    low, high = jnp.split(expert_down[0], 2)
+    before_low, after_high = lax.ppermute(low, "tp", up), lax.ppermute(high, "tp", down)
+    before_high, after_low = lax.ppermute(high, "tp", up), lax.ppermute(low, "tp", down)
+    own, held_residual, held_routes, before_low, after_high = lax.optimization_barrier(
+        (own, held_residual, held_routes, before_low, after_high)
+    )
     other = lax.ppermute(own, "sp_2", [(0, 1), (1, 0)])
     attended = attend_rows(index.reshape(1), queries[:HALF], mirrored_queries, own, other)
-    down_before, down_after, attended = lax.optimization_barrier(
-        (down_before, down_after, attended)
-    )
-    down_across = opposite(down_before, down_after)
+    attended, before_high, after_low = lax.optimization_barrier((attended, before_high, after_low))
+    across_low, across_high = lax.ppermute(before_low, "tp", up), lax.ppermute(after_high, "tp", down)
     partial = jnp.dot(
         attended.reshape(-1, attended.shape[2]), out_weight, preferred_element_type=jnp.float32
     ).astype(jnp.bfloat16)
@@ -336,16 +401,20 @@
     held_hidden, slots = dispatch(
         parts, held_residual, norm_gain, ranked_routes, seq_devices, capacity
     )
+    slots, across_low, across_high = lax.optimization_barrier((slots, across_low, across_high))
+    down_own = expert_down[0]
+    down_before = jnp.concatenate([before_low, before_high])
+    down_after = jnp.concatenate([after_low, after_high])
+    down_across = jnp.concatenate([across_low, across_high])
     hidden_state = lax.ppermute(held_hidden, SP_TP, whole)
-    width = slots.shape[2]
     ranks = [
         [(i if 2 * t < head_devices else seq_devices - 1 - i) * head_devices + t for i in range(seq_devices)]
         for t in range(head_devices)
     ]
     incoming = lax.all_to_all(
-        slots.transpose(1, 0, 2), SP_TP, 0, 0, axis_index_groups=ranks, tiled=True
-    )
-    rows_own = incoming.transpose(1, 0, 2).reshape(-1, width)
+        slots, SP_TP, 0, 0, axis_index_groups=ranks, tiled=True
+    )
+    rows_own = arrange(incoming, capacity)
 
     def units(rows):
         gate_value = jnp.dot(rows, expert_gate[0], preferred_element_type=jnp.float32)
@@ -354,8 +423,8 @@
 
     rows_before, rows_after = neighbours(rows_own)
     units_own = units(rows_own)
-    rows_before, hidden_state = lax.optimization_barrier((rows_before, hidden_state))
     rows_across = opposite(rows_before, rows_after)
+    rows_across, hidden_state = lax.optimization_barrier((rows_across, hidden_state))
     units_from_before = lax.ppermute(units(rows_after), "tp", up)
     units_from_after = lax.ppermute(units(rows_before), "tp", down)
     across = [(i, (i + 2) % head_devices) for i in range(head_devices)]
@@ -367,9 +436,8 @@
         (units_from_across, down_across),
     ):
         summed = summed + jnp.dot(got, weight, preferred_element_type=jnp.float32)
-    leaving = summed.astype(jnp.bfloat16).reshape(capacity, seq_devices, width).transpose(1, 0, 2)
-    returned = lax.all_to_all(leaving, SP, 0, 0, tiled=True).transpose(1, 0, 2)
-    return combine(returned, hidden_state, routes, route_weight)
+    returned = lax.all_to_all(spread(summed, capacity), SP, 0, 0, tiled=True)
+    return combine(returned, hidden_state, routes, route_weight, capacity)
 
 
 def solution(mesh):

time: 321 us -> 310 us (0.966)
  starting transfers between devices: 79.7 us -> 64.2 us
  local copies, waits for them, and re-layouts: 21.8 us -> 9.69 us
  waiting for transfers between devices: 131 us -> 139 us
  Pallas kernels: 29.7 us -> 35.6 us
    all_to_all x1, waiting for transfers between devices: 12.8 us -> 37.4 us  [local(): lax.all_to_all(partial.reshape(head_devices, -1, partial.shape[1]), 'tp',...]
    ppermute x0 -> x6, waiting for transfers between devices: none -> 18.7 us  [the longest x1 8.42 us: local(): lax.ppermute(high, 'tp', up)]
    all_to_all x2, starting transfers between devices: 40.2 us -> 24.6 us  [the longest x1 15.4 us: local(): returned = lax.all_to_all(spread(summed, capacity), SP, 0, 0, tiled=True)]
    ppermute x2 -> x1, waiting for transfers between devices: 10.1 us -> 0.01 us  [opposite(): lax.ppermute(before[:half], 'tp', up)]
    all_gather x1, waiting for transfers between devices: 20.3 us -> 11.2 us  [local(): own = lax.all_gather(near, 'sp_0').reshape(-1, *block.shape)]
    ppermute x1, waiting for transfers between devices: 7.12 us -> 0.26 us  [local(): units_from_across = lax.ppermute(units(rows_across), 'tp', across)]
    ppermute x1, waiting for transfers between devices: 0.01 us -> 6.4 us  [local(): units_from_before = lax.ppermute(units(rows_after), 'tp', up)]
    ppermute x0 -> x6, starting transfers between devices: none -> 6.08 us  [the longest x1 2.02 us: local(): lax.ppermute(low, 'tp', down)]
  transfers between devices with their start and end apart: 20 -> 22, of which waited for: 10 -> 13; matrix products, arithmetic and copies ran while one was open for 12% -> 11% of each run, Pallas kernels for 7% -> 10%
where the time goes in v5:
time: 310 us; the launch traced here: 307 us
  waiting for transfers between devices  139 us (45%)
  starting transfers between devices  64.2 us (21%)
  Pallas kernels  35.6 us (11%)
  matrix products  30.5 us (10%)
  between operations  13.6 us (4%)
  blocking collectives  13.5 us (4%)
  local copies, waits for them, and re-layouts  9.69 us (3%)
    all_to_all x1, waiting for transfers between devices, local(): lax.all_to_all(partial.reshape(head_devices, -1, partial.shape[1]), 'tp',...  37.4 us
    all_to_all x1, waiting for transfers between devices, local(): returned = lax.all_to_all(spread(summed, capacity), SP, 0, 0, tiled=True)  22.4 us
    pallas_call x1, Pallas kernels, attend_rows(): pl.pallas_call(functools.partial(attend_body, blocks=blocks, heads=heads)...  22.2 us
    all_to_all x1, waiting for transfers between devices, local(): lax.all_to_all(slots, SP_TP, 0, 0, axis_index_groups=ranks, tiled=True)  16.8 us
    ppermute x1, waiting for transfers between devices, local(): held_routes = lax.ppermute(routes, SP_TP, whole)  16 us
    all_to_all x1, starting transfers between devices, local(): returned = lax.all_to_all(spread(summed, capacity), SP, 0, 0, tiled=True)  15.4 us
    all_gather x1, blocking collectives, local(): near = lax.all_gather(block, 'sp_1')  13.5 us
    all_gather x1, waiting for transfers between devices, local(): own = lax.all_gather(near, 'sp_0').reshape(-1, *block.shape)  11.2 us
  transfers between devices with their start and end apart: 22, of which 13 were waited for; matrix products, arithmetic and copies ran while one was open for 11% of the time, Pallas kernels for 10%

profile of v5, /device:TPU:6, one launch (start us, length us, event | category | flops | bytes accessed | tf_op | source)
XLA Modules:
  0.0 307.2 jit_solution(11677848941060630828)
XLA Ops:
  6.5 1.1 fusion.57
  7.7 7.8 %collective-permute-start = (bf16[128,512]{1,0:T(8,128)(2,1)S(1)}, bf16[128,512]{1,0:T(8,128)(2,1)S(1)}, u32[]{:S(2)}, u32[]{:S(2)}) collective-permute-start(bf16[128,512]{1,0:T(8,128)(2,1)S(1)} %get-tuple-element.41), channel_id=1, source_target_pairs={{0,252},{4,248},{8,244},{12,240},{16,236},{20,232},{24,228},{28,22... | collective-permute-start | bytes 393224 | tf_op jit(solution)/shard_map/ppermute | solution.py:376
  15.5 1.6 prepare_keys.1
  17.1 13.5 %all-gather = bf16[640,256]{1,0:T(8,128)(2,1)} all-gather(bf16[160,256]{1,0:T(8,128)(2,1)} %prepare_keys.1), channel_id=2, replica_groups=mesh['sp_0'=8,'sp_1'=4,'sp_2'=2,'tp'=4] {'sp_1'}, dimensions={0}, use_global_device_ids=true | all-gather | bytes 409600 | tf_op jit(solution)/shard_map/all_gather | solution.py:377
  30.6 3.9 %slice_bitcast_fusion = (bf16[384,2048]{1,0:T(8,128)(2,1)}, bf16[384,2048]{1,0:T(8,128)(2,1)}) fusion(bf16[1,768,2048]{2,1,0:T(8,128)(2,1)} %param.21), kind=kLoop, calls=%fused_computation.34 | loop fusion | bytes 6291456 | tf_op jit(solution)/shard_map/split | solution.py:382
  35.0 1.5 collective-permute-start.4
  36.6 1.9 collective-permute-start.1
  38.6 7.0 %collective-permute-start.2 = (s32[64,2]{1,0:T(8,128)S(1)}, s32[64,2]{1,0:T(8,128)S(1)}, u32[]{:S(2)}, u32[]{:S(2)}) collective-permute-start(s32[64,2]{1,0:T(8,128)S(1)} %copy.15.routes_ref), channel_id=1, source_target_pairs={{0,0},{1,1},{2,254},{3,255},{4,4},{5,5},{6,250},{7,251},{8,8},{9,9... | collective-permute-start | bytes 1544 | tf_op jit(solution)/shard_map/ppermute | solution.py:380
  45.6 16.0 %collective-permute-done.2 = s32[64,2]{1,0:T(8,128)S(1)} collective-permute-done((s32[64,2]{1,0:T(8,128)S(1)}, s32[64,2]{1,0:T(8,128)S(1)}, u32[]{:S(2)}, u32[]{:S(2)}) %collective-permute-start.2) | collective-permute-done | bytes 544 | tf_op jit(solution)/shard_map/ppermute | solution.py:380
  61.6 7.7 %collective-permute-done.3 = bf16[384,2048]{1,0:T(8,128)(2,1)} collective-permute-done((bf16[384,2048]{1,0:T(8,128)(2,1)}, bf16[384,2048]{1,0:T(8,128)(2,1)}, u32[]{:S(2)}, u32[]{:S(2)}) %collective-permute-start.3) | collective-permute-done | bytes 1572896 | tf_op jit(solution)/shard_map/ppermute | solution.py:383
  69.2 1.4 collective-permute-done.4
  70.7 11.2 %all-gather.4.cloned.1.call-done.own_ref = bf16[32,160,256]{2,1,0:T(8,128)(2,1)} async-done(((bf16[4,160,256]{2,1,0:T(8,128)(2,1)}), bf16[32,160,256]{2,1,0:T(8,128)(2,1)}) %all-gather.4.cloned.1.call-update) | async-done | bytes 2621456 | tf_op jit(solution)/shard_map/all_gather | solution.py:381
  81.9 2.0 collective-permute-start.7
  83.9 1.2 collective-permute-start.8
  85.9 1.2 collective-permute-done.5.other_ref
  87.1 1.7 copy-done.1
  88.8 22.2 %attend_rows.1 = bf16[2,128,512]{2,1,0:T(8,128)(2,1)S(1)} custom-call(s32[1]{0:T(128)} %bitcast.index_ref, bf16[128,512]{1,0:T(8,128)(2,1)S(1)} %get-tuple-element.42.qa_ref, bf16[128,512]{1,0:T(8,128)(2,1)S(1)} %collective-permute-done.qb_ref, bf16[32,160,256]{2,1,0:T(8,128)(2,1)S(1)} %copy-done.1, bf16[32,160,256]{2,1,0:T(8,128)(2,1)} %collective-permute-done.5.other_ref), custom_call_target="tpu_custom_call" | custom-call | tf_op jit(solution)/shard_map/attend_rows/pallas_call | solution.py:196
  111.0 8.4 %collective-permute-done.6 = bf16[384,2048]{1,0:T(8,128)(2,1)} collective-permute-done((bf16[384,2048]{1,0:T(8,128)(2,1)}, bf16[384,2048]{1,0:T(8,128)(2,1)}, u32[]{:S(2)}, u32[]{:S(2)}) %collective-permute-start.6) | collective-permute-done | bytes 1572896 | tf_op jit(solution)/shard_map/ppermute | solution.py:384
  119.4 1.2 collective-permute-done.7
  120.6 1.7 convolution_convert_fusion
  122.4 4.7 %all-to-all-start = ((bf16[4,64,2048]{2,1,0:T(8,128)(2,1)}), bf16[4,64,2048]{2,1,0:T(8,128)(2,1)}, u32[]{:S(2)}, u32[]{:S(2)}) async-start(bf16[4,64,2048]{2,1,0:T(8,128)(2,1)} %bitcast.57), calls=%async_computation | async-start | bytes 2097152 | tf_op jit(solution)/shard_map/all_to_all | solution.py:395
  127.7 37.4 %all-to-all-done.parts_ref = bf16[4,64,2048]{2,1,0:T(8,128)(2,1)} async-done(((bf16[4,64,2048]{2,1,0:T(8,128)(2,1)}), bf16[4,64,2048]{2,1,0:T(8,128)(2,1)}, u32[]{:S(2)}, u32[]{:S(2)}) %all-to-all-start) | async-done | bytes 1048608 | tf_op jit(solution)/shard_map/all_to_all | solution.py:395
  165.1 3.3 %dispatch.1 = (f32[64,2048]{1,0:T(8,128)}, bf16[64,48,128]{2,1,0:T(8,128)(2,1)}) custom-call(bf16[4,64,2048]{2,1,0:T(8,128)(2,1)} %all-to-all-done.parts_ref, bf16[64,2048]{1,0:T(8,128)(2,1)} %collective-permute-done.1.residual_ref, f32[1,2048]{1,0:T(1,128)} %bitcast.59, s32[64,2]{1,0:T(8,128)} %subtract_select_fusion.routes_ref), custom_call_target="tpu_custom_call" | custom-call | tf_op jit(solution)/shard_map/dispatch/pallas_call | solution.py:266
  168.4 9.2 %all-to-all-start.1 = ((bf16[64,48,128]{2,1,0:T(8,128)(2,1)}), bf16[64,48,128]{2,1,0:T(8,128)(2,1)}, u32[]{:S(2)}, u32[]{:S(2)}) async-start(bf16[64,48,128]{2,1,0:T(8,128)(2,1)} %get-tuple-element.31), calls=%async_computation.1 | async-start | bytes 1572864 | tf_op jit(solution)/shard_map/all_to_all | solution.py:414
  177.6 2.3 collective-permute-start.16
  179.9 16.8 %all-to-all-done.1.arrived_ref = bf16[64,48,128]{2,1,0:T(8,128)(2,1)} async-done(((bf16[64,48,128]{2,1,0:T(8,128)(2,1)}), bf16[64,48,128]{2,1,0:T(8,128)(2,1)}, u32[]{:S(2)}, u32[]{:S(2)}) %all-to-all-start.1) | async-done | bytes 786464 | tf_op jit(solution)/shard_map/all_to_all | solution.py:414
  196.7 2.6 arrange.1
  199.3 3.2 %collective-permute-start.12 = (bf16[192,2048]{1,0:T(8,128)(2,1)}, bf16[192,2048]{1,0:T(8,128)(2,1)}, u32[]{:S(2)}, u32[]{:S(2)}) collective-permute-start(bf16[192,2048]{1,0:T(8,128)(2,1)} %arrange.1), channel_id=1, source_target_pairs={{0,1},{1,2},{2,3},{3,0},{4,5},{5,6},{6,7},{7,4},{8,9},{9,10},{10,1... | collective-permute-start | bytes 2359304 | tf_op jit(solution)/shard_map/ppermute | solution.py:361
  202.5 3.7 %fusion.28 = f32[192,768]{1,0:T(8,128)} fusion(bf16[192,2048]{1,0:T(8,128)(2,1)} %arrange.1, bf16[1,2048,768]{2,1,0:T(8,128)(2,1)} %param.19), kind=kOutput, calls=%fused_computation.28 | convolution fusion | flops 603979776 | bytes 4521984 | tf_op jit(solution)/shard_map/dot_general | solution.py:420
  206.2 5.2 %fusion.12 = f32[192,2048]{1,0:T(8,128)} fusion(bf16[1,768,2048]{2,1,0:T(8,128)(2,1)} %param.21, bf16[192,2048]{1,0:T(8,128)(2,1)} %arrange.1, bf16[1,2048,768]{2,1,0:T(8,128)(2,1)S(1)} %copy-done, f32[192,768]{1,0:T(8,128)} %fusion.28), kind=kOutput, calls=%fused_computation.12 | convolution fusion | flops 1208844288 | bytes 9240576 | tf_op jit(solution)/shard_map/dot_general | solution.py:432
  211.4 8.9 %collective-permute-done.10 = bf16[192,2048]{1,0:T(8,128)(2,1)} collective-permute-done((bf16[192,2048]{1,0:T(8,128)(2,1)}, bf16[192,2048]{1,0:T(8,128)(2,1)}, u32[]{:S(2)}, u32[]{:S(2)}) %collective-permute-start.10) | collective-permute-done | bytes 786464 | tf_op jit(solution)/shard_map/ppermute | solution.py:361
  220.3 1.0 slice.19
  221.5 1.0 slice.18
  222.5 3.3 %collective-permute-start.14 = (bf16[96,2048]{1,0:T(8,128)(2,1)S(1)}, bf16[96,2048]{1,0:T(8,128)(2,1)S(1)}, u32[]{:S(2)}, u32[]{:S(2)}) collective-permute-start(bf16[96,2048]{1,0:T(8,128)(2,1)S(1)} %slice.18), channel_id=1, source_target_pairs={{0,1},{1,2},{2,3},{3,0},{4,5},{5,6},{6,7},{7,4},{8,9},{9,10},{10,1... | collective-permute-start | bytes 1179656 | tf_op jit(solution)/shard_map/ppermute | solution.py:366
  225.8 2.9 fusion.26
  228.7 2.1 multiply_convert_fusion.2
  231.0 1.9 fusion.24
  233.0 1.9 multiply_convert_fusion.1
  234.9 2.0 collective-permute-start.13
  238.6 1.0 collective-permute-start.17
  239.6 6.4 %collective-permute-done.11 = bf16[192,768]{1,0:T(8,128)(2,1)S(1)} collective-permute-done((bf16[192,768]{1,0:T(8,128)(2,1)S(1)}, bf16[192,768]{1,0:T(8,128)(2,1)S(1)}, u32[]{:S(2)}, u32[]{:S(2)}) %collective-permute-start.11) | collective-permute-done | bytes 294944 | tf_op jit(solution)/shard_map/ppermute | solution.py:428
  246.0 2.7 fusion.36
  249.0 2.7 fusion.8
  251.7 4.0 %fusion.33.rows_ref = f32[192,2048]{1,0:T(8,128)} fusion(f32[192,2048]{1,0:T(8,128)S(1)} %fusion.8, f32[192,2048]{1,0:T(8,128)S(1)} %fusion.36, bf16[192,768]{1,0:T(8,128)(2,1)S(1)} %collective-permute-done.13, bf16[384,2048]{1,0:T(8,128)(2,1)} %collective-permute-done.4, bf16[384,2048]{1,0:T(8,128)(2,1)} %collective-permute-done.7), kind=kOutput, calls=%fused_computation.32 | convolution fusion | flops 611057664 | bytes 8159232 | tf_op jit(solution)/shard_map/dot_general | solution.py:438
  255.7 2.8 spread.1
  258.6 15.4 %all-to-all-start.2 = ((bf16[64,48,128]{2,1,0:T(8,128)(2,1)}), bf16[64,48,128]{2,1,0:T(8,128)(2,1)}, u32[]{:S(2)}, u32[]{:S(2)}) async-start(bf16[64,48,128]{2,1,0:T(8,128)(2,1)} %spread.1), calls=%async_computation.2 | async-start | bytes 1572864 | tf_op jit(solution)/shard_map/all_to_all | solution.py:439
  274.7 22.4 %all-to-all-done.2.returned_ref = bf16[64,48,128]{2,1,0:T(8,128)(2,1)} async-done(((bf16[64,48,128]{2,1,0:T(8,128)(2,1)}), bf16[64,48,128]{2,1,0:T(8,128)(2,1)}, u32[]{:S(2)}, u32[]{:S(2)}) %all-to-all-start.2) | async-done | bytes 786464 | tf_op jit(solution)/shard_map/all_to_all | solution.py:439
  297.1 3.2 %combine.1 = bf16[64,2048]{1,0:T(8,128)(2,1)} custom-call(bf16[64,48,128]{2,1,0:T(8,128)(2,1)} %all-to-all-done.2.returned_ref, f32[64,2048]{1,0:T(8,128)} %collective-permute-done.16.hidden_ref, s32[64,2]{1,0:T(8,128)} %copy-done.4, f32[64,2]{1,0:T(8,128)} %copy.17.weight_ref), custom_call_target="tpu_custom_call" | custom-call | tf_op jit(solution)/shard_map/combine/pallas_call | solution.py:332
  (40 shorter events, 5.0 us)
Async XLA Ops:
  6.5 199.7 %copy-start = (bf16[1,2048,768]{2,1,0:T(8,128)(2,1)S(1)}, bf16[1,2048,768]{2,1,0:T(8,128)(2,1)}, u32[]{:S(2)}) copy-start(bf16[1,2048,768]{2,1,0:T(8,128)(2,1)} %param.20) | copy-start | bytes 9437188
  6.5 75.3 %all-gather.4.cloned.1.call-start = ((), (), s32[]{:S(2)}) async-start(), calls=%async_computation.3 | async-start | bytes 2949120 | tf_op jit(solution)/shard_map/all_gather | solution.py:381
  7.7 22.9 %collective-permute-start = (bf16[128,512]{1,0:T(8,128)(2,1)S(1)}, bf16[128,512]{1,0:T(8,128)(2,1)S(1)}, u32[]{:S(2)}, u32[]{:S(2)}) collective-permute-start(bf16[128,512]{1,0:T(8,128)(2,1)S(1)} %get-tuple-element.41), channel_id=1, source_target_pairs={{0,252},{4,248},{8,244},{12,240},{16,236},{20,232},{24,228},{28,22... | collective-permute-start | bytes 393224 | tf_op jit(solution)/shard_map/ppermute | solution.py:376
  30.6 7.9 %copy-start.5 = (s32[64,2]{0,1:T(2,128)S(1)}, s32[64,2]{0,1:T(2,128)}, u32[]{:S(2)}) copy-start(s32[64,2]{0,1:T(2,128)} %param.17) | copy-start | bytes 1540
  34.6 34.7 %collective-permute-start.3 = (bf16[384,2048]{1,0:T(8,128)(2,1)}, bf16[384,2048]{1,0:T(8,128)(2,1)}, u32[]{:S(2)}, u32[]{:S(2)}) collective-permute-start(bf16[384,2048]{1,0:T(8,128)(2,1)} %get-tuple-element.40), channel_id=1, source_target_pairs={{0,1},{1,2},{2,3},{3,0},{4,5},{5,6},{6,7},{7,4},{8,9},{9,10},{10,1... | collective-permute-start | bytes 4718600 | tf_op jit(solution)/shard_map/ppermute | solution.py:383
  35.0 35.6 %collective-permute-start.4 = (bf16[384,2048]{1,0:T(8,128)(2,1)}, bf16[384,2048]{1,0:T(8,128)(2,1)}, u32[]{:S(2)}, u32[]{:S(2)}) collective-permute-start(bf16[384,2048]{1,0:T(8,128)(2,1)} %get-tuple-element.39), channel_id=1, source_target_pairs={{0,3},{1,0},{2,1},{3,2},{4,7},{5,4},{6,5},{7,6},{8,11},{9,8},{10,9... | collective-permute-start | bytes 4718600 | tf_op jit(solution)/shard_map/ppermute | solution.py:383
  36.6 25.0 %collective-permute-start.1 = (bf16[64,2048]{1,0:T(8,128)(2,1)}, bf16[64,2048]{1,0:T(8,128)(2,1)}, u32[]{:S(2)}, u32[]{:S(2)}) collective-permute-start(bf16[64,2048]{1,0:T(8,128)(2,1)} %param.14), channel_id=1, source_target_pairs={{0,0},{1,1},{2,254},{3,255},{4,4},{5,5},{6,250},{7,251},{8,8},{9,9... | collective-permute-start | bytes 786440 | tf_op jit(solution)/shard_map/ppermute | solution.py:379
  38.6 83.8 %copy-start.4 = (s32[64,2]{1,0:T(8,128)}, s32[64,2]{1,0:T(8,128)S(1)}, u32[]{:S(2)}) copy-start(s32[64,2]{1,0:T(8,128)S(1)} %copy.15.routes_ref) | copy-start | bytes 1540
  38.6 23.0 %collective-permute-start.2 = (s32[64,2]{1,0:T(8,128)S(1)}, s32[64,2]{1,0:T(8,128)S(1)}, u32[]{:S(2)}, u32[]{:S(2)}) collective-permute-start(s32[64,2]{1,0:T(8,128)S(1)} %copy.15.routes_ref), channel_id=1, source_target_pairs={{0,0},{1,1},{2,254},{3,255},{4,4},{5,5},{6,250},{7,251},{8,8},{9,9... | collective-permute-start | bytes 1544 | tf_op jit(solution)/shard_map/ppermute | solution.py:380
  81.8 5.3 %collective-permute-start.5 = (bf16[32,160,256]{2,1,0:T(8,128)(2,1)}, bf16[32,160,256]{2,1,0:T(8,128)(2,1)}, u32[]{:S(2)}, u32[]{:S(2)}) collective-permute-start(bf16[32,160,256]{2,1,0:T(8,128)(2,1)} %all-gather.4.cloned.1.call-done.own_ref), channel_id=1, source_target_pairs={{0,4},{4,0},{1,5},{5,1},{2,6},{6,2},{3,7},{7,3},{8,12},{12,8},{9,1... | collective-permute-start | bytes 7864328 | tf_op jit(solution)/shard_map/ppermute | solution.py:388
  81.8 37.6 %collective-permute-start.6 = (bf16[384,2048]{1,0:T(8,128)(2,1)}, bf16[384,2048]{1,0:T(8,128)(2,1)}, u32[]{:S(2)}, u32[]{:S(2)}) collective-permute-start(bf16[384,2048]{1,0:T(8,128)(2,1)} %get-tuple-element.39), channel_id=1, source_target_pairs={{0,1},{1,2},{2,3},{3,0},{4,5},{5,6},{6,7},{7,4},{8,9},{9,10},{10,1... | collective-permute-start | bytes 4718600 | tf_op jit(solution)/shard_map/ppermute | solution.py:384
  81.9 38.8 %collective-permute-start.7 = (bf16[384,2048]{1,0:T(8,128)(2,1)}, bf16[384,2048]{1,0:T(8,128)(2,1)}, u32[]{:S(2)}, u32[]{:S(2)}) collective-permute-start(bf16[384,2048]{1,0:T(8,128)(2,1)} %get-tuple-element.40), channel_id=1, source_target_pairs={{0,3},{1,0},{2,1},{3,2},{4,7},{5,4},{6,5},{7,6},{8,11},{9,8},{10,9... | collective-permute-start | bytes 4718600 | tf_op jit(solution)/shard_map/ppermute | solution.py:384
  83.9 84.5 %collective-permute-start.8 = (bf16[384,2048]{1,0:T(8,128)(2,1)}, bf16[384,2048]{1,0:T(8,128)(2,1)}, u32[]{:S(2)}, u32[]{:S(2)}) collective-permute-start(bf16[384,2048]{1,0:T(8,128)(2,1)} %collective-permute-done.3), channel_id=1, source_target_pairs={{0,1},{1,2},{2,3},{3,0},{4,5},{5,6},{6,7},{7,4},{8,9},{9,10},{10,1... | collective-permute-start | bytes 4718600 | tf_op jit(solution)/shard_map/ppermute | solution.py:391
  85.1 83.3 %collective-permute-start.9 = (bf16[384,2048]{1,0:T(8,128)(2,1)}, bf16[384,2048]{1,0:T(8,128)(2,1)}, u32[]{:S(2)}, u32[]{:S(2)}) collective-permute-start(bf16[384,2048]{1,0:T(8,128)(2,1)} %collective-permute-done.4), channel_id=1, source_target_pairs={{0,3},{1,0},{2,1},{3,2},{4,7},{5,4},{6,5},{7,6},{8,11},{9,8},{10,9... | collective-permute-start | bytes 4718600 | tf_op jit(solution)/shard_map/ppermute | solution.py:391
  87.1 1.7 copy-start.1
  88.8 31.8 %copy-start.3 = (bf16[512,2048]{1,0:T(8,128)(2,1)S(1)}, bf16[512,2048]{1,0:T(8,128)(2,1)}, u32[]{:S(2)}) copy-start(bf16[512,2048]{1,0:T(8,128)(2,1)} %param.15) | copy-start | bytes 6291460
  122.4 42.8 %all-to-all-start = ((bf16[4,64,2048]{2,1,0:T(8,128)(2,1)}), bf16[4,64,2048]{2,1,0:T(8,128)(2,1)}, u32[]{:S(2)}, u32[]{:S(2)}) async-start(bf16[4,64,2048]{2,1,0:T(8,128)(2,1)} %bitcast.57), calls=%async_computation | async-start | bytes 2097152 | tf_op jit(solution)/shard_map/all_to_all | solution.py:395
  168.4 28.3 %all-to-all-start.1 = ((bf16[64,48,128]{2,1,0:T(8,128)(2,1)}), bf16[64,48,128]{2,1,0:T(8,128)(2,1)}, u32[]{:S(2)}, u32[]{:S(2)}) async-start(bf16[64,48,128]{2,1,0:T(8,128)(2,1)} %get-tuple-element.31), calls=%async_computation.1 | async-start | bytes 1572864 | tf_op jit(solution)/shard_map/all_to_all | solution.py:414
  177.6 59.4 %collective-permute-start.16 = (f32[64,2048]{1,0:T(8,128)}, f32[64,2048]{1,0:T(8,128)}, u32[]{:S(2)}, u32[]{:S(2)}) collective-permute-start(f32[64,2048]{1,0:T(8,128)} %get-tuple-element.34), channel_id=1, source_target_pairs={{0,0},{1,1},{2,254},{3,255},{4,4},{5,5},{6,250},{7,251},{8,8},{9,9... | collective-permute-start | bytes 1572872 | tf_op jit(solution)/shard_map/ppermute | solution.py:409
  199.3 21.1 %collective-permute-start.10 = (bf16[192,2048]{1,0:T(8,128)(2,1)}, bf16[192,2048]{1,0:T(8,128)(2,1)}, u32[]{:S(2)}, u32[]{:S(2)}) collective-permute-start(bf16[192,2048]{1,0:T(8,128)(2,1)} %arrange.1), channel_id=1, source_target_pairs={{0,3},{1,0},{2,1},{3,2},{4,7},{5,4},{6,5},{7,6},{8,11},{9,8},{10,9... | collective-permute-start | bytes 2359304 | tf_op jit(solution)/shard_map/ppermute | solution.py:361
  199.3 22.2 %collective-permute-start.12 = (bf16[192,2048]{1,0:T(8,128)(2,1)}, bf16[192,2048]{1,0:T(8,128)(2,1)}, u32[]{:S(2)}, u32[]{:S(2)}) collective-permute-start(bf16[192,2048]{1,0:T(8,128)(2,1)} %arrange.1), channel_id=1, source_target_pairs={{0,1},{1,2},{2,3},{3,0},{4,5},{5,6},{6,7},{7,4},{8,9},{9,10},{10,1... | collective-permute-start | bytes 2359304 | tf_op jit(solution)/shard_map/ppermute | solution.py:361
  221.4 15.5 %collective-permute-start.15 = (bf16[96,2048]{1,0:T(8,128)(2,1)S(1)}, bf16[96,2048]{1,0:T(8,128)(2,1)S(1)}, u32[]{:S(2)}, u32[]{:S(2)}) collective-permute-start(bf16[96,2048]{1,0:T(8,128)(2,1)S(1)} %slice.19), channel_id=1, source_target_pairs={{0,3},{1,0},{2,1},{3,2},{4,7},{5,4},{6,5},{7,6},{8,11},{9,8},{10,9... | collective-permute-start | bytes 1179656 | tf_op jit(solution)/shard_map/ppermute | solution.py:366
  222.5 14.4 %collective-permute-start.14 = (bf16[96,2048]{1,0:T(8,128)(2,1)S(1)}, bf16[96,2048]{1,0:T(8,128)(2,1)S(1)}, u32[]{:S(2)}, u32[]{:S(2)}) collective-permute-start(bf16[96,2048]{1,0:T(8,128)(2,1)S(1)} %slice.18), channel_id=1, source_target_pairs={{0,1},{1,2},{2,3},{3,0},{4,5},{5,6},{6,7},{7,4},{8,9},{9,10},{10,1... | collective-permute-start | bytes 1179656 | tf_op jit(solution)/shard_map/ppermute | solution.py:366
  228.7 2.3 copy-start.2
  230.8 15.2 %collective-permute-start.11 = (bf16[192,768]{1,0:T(8,128)(2,1)S(1)}, bf16[192,768]{1,0:T(8,128)(2,1)S(1)}, u32[]{:S(2)}, u32[]{:S(2)}) collective-permute-start(bf16[192,768]{1,0:T(8,128)(2,1)S(1)} %multiply_convert_fusion.2), channel_id=1, source_target_pairs={{0,1},{1,2},{2,3},{3,0},{4,5},{5,6},{6,7},{7,4},{8,9},{9,10},{10,1... | collective-permute-start | bytes 884744 | tf_op jit(solution)/shard_map/ppermute | solution.py:428
  234.9 16.8 %collective-permute-start.13 = (bf16[192,768]{1,0:T(8,128)(2,1)S(1)}, bf16[192,768]{1,0:T(8,128)(2,1)S(1)}, u32[]{:S(2)}, u32[]{:S(2)}) collective-permute-start(bf16[192,768]{1,0:T(8,128)(2,1)S(1)} %multiply_convert_fusion.1), channel_id=1, source_target_pairs={{0,3},{1,0},{2,1},{3,2},{4,7},{5,4},{6,5},{7,6},{8,11},{9,8},{10,9... | collective-permute-start | bytes 884744 | tf_op jit(solution)/shard_map/ppermute | solution.py:429
  237.8 8.2 %copy-start.7 = (f32[192,2048]{1,0:T(8,128)S(1)}, f32[192,2048]{1,0:T(8,128)}, u32[]{:S(2)}) copy-start(f32[192,2048]{1,0:T(8,128)} %fusion.12) | copy-start | bytes 4718596
  238.6 10.4 %collective-permute-start.17 = (bf16[192,768]{1,0:T(8,128)(2,1)S(1)}, bf16[192,768]{1,0:T(8,128)(2,1)S(1)}, u32[]{:S(2)}, u32[]{:S(2)}) collective-permute-start(bf16[192,768]{1,0:T(8,128)(2,1)S(1)} %multiply_convert_fusion), channel_id=1, source_target_pairs={{0,2},{1,3},{2,0},{3,1},{4,6},{5,7},{6,4},{7,5},{8,10},{9,11},{10,... | collective-permute-start | bytes 884744 | tf_op jit(solution)/shard_map/ppermute | solution.py:431
  255.7 18.3 %copy-start.6 = (f32[64,2]{0,1:T(2,128)S(1)}, f32[64,2]{0,1:T(2,128)}, u32[]{:S(2)}) copy-start(f32[64,2]{0,1:T(2,128)} %param.18) | copy-start | bytes 1540
  258.6 38.5 %all-to-all-start.2 = ((bf16[64,48,128]{2,1,0:T(8,128)(2,1)}), bf16[64,48,128]{2,1,0:T(8,128)(2,1)}, u32[]{:S(2)}, u32[]{:S(2)}) async-start(bf16[64,48,128]{2,1,0:T(8,128)(2,1)} %spread.1), calls=%async_computation.2 | async-start | bytes 1572864 | tf_op jit(solution)/shard_map/all_to_all | solution.py:439
Sparse Core Ops, SparseCore 0:
  30.7 51.0 all-gather.3

commit v6 on v5

--- a/solution.py
+++ b/solution.py
@@ -337,7 +337,7 @@
     )(returned, hidden, routes, route_weight)
 
 
-def local(
+def layer(
     queries,
     key_value_pairs,
     forget_gate_total,
@@ -374,21 +374,23 @@
     flipped = 2 * lax.axis_index("tp") >= head_devices
     block = prepare_keys(key_value_pairs, forget_gate_total.T)
     mirrored_queries = lax.ppermute(queries[HALF:], SP, mirror)
+    down_own = expert_down[0]
+    down_before = lax.ppermute(down_own, "tp", up)
+    down_after = lax.ppermute(down_own, "tp", down)
     near = lax.all_gather(block, "sp_1")
     near, mirrored_queries = lax.optimization_barrier((near, mirrored_queries))
     held_residual = lax.ppermute(residual_in, SP_TP, whole)
     held_routes = lax.ppermute(routes, SP_TP, whole)
     own = lax.all_gather(near, "sp_0").reshape(-1, *block.shape)
-    low, high = jnp.split(expert_down[0], 2)
-    before_low, after_high = lax.ppermute(low, "tp", up), lax.ppermute(high, "tp", down)
-    before_high, after_low = lax.ppermute(high, "tp", up), lax.ppermute(low, "tp", down)
-    own, held_residual, held_routes, before_low, after_high = lax.optimization_barrier(
-        (own, held_residual, held_routes, before_low, after_high)
-    )
+    own, held_residual, held_routes = lax.optimization_barrier((own, held_residual, held_routes))
     other = lax.ppermute(own, "sp_2", [(0, 1), (1, 0)])
     attended = attend_rows(index.reshape(1), queries[:HALF], mirrored_queries, own, other)
-    attended, before_high, after_low = lax.optimization_barrier((attended, before_high, after_low))
-    across_low, across_high = lax.ppermute(before_low, "tp", up), lax.ppermute(after_high, "tp", down)
+    down_before, down_after, attended = lax.optimization_barrier(
+        (down_before, down_after, attended)
+    )
+    half = down_own.shape[0] // 2
+    across_low = lax.ppermute(down_before[:half], "tp", up)
+    across_high = lax.ppermute(down_after[half:], "tp", down)
     partial = jnp.dot(
         attended.reshape(-1, attended.shape[2]), out_weight, preferred_element_type=jnp.float32
     ).astype(jnp.bfloat16)
@@ -401,10 +403,6 @@
     held_hidden, slots = dispatch(
         parts, held_residual, norm_gain, ranked_routes, seq_devices, capacity
     )
-    slots, across_low, across_high = lax.optimization_barrier((slots, across_low, across_high))
-    down_own = expert_down[0]
-    down_before = jnp.concatenate([before_low, before_high])
-    down_after = jnp.concatenate([after_low, after_high])
     down_across = jnp.concatenate([across_low, across_high])
     hidden_state = lax.ppermute(held_hidden, SP_TP, whole)
     ranks = [
@@ -456,4 +454,4 @@
         P(SP, "tp", None),
     )
     out_specs = P(SP_TP, None)
-    return jax.shard_map(local, mesh=finer, in_specs=in_specs, out_specs=out_specs, check_vma=False)
+    return jax.shard_map(layer, mesh=finer, in_specs=in_specs, out_specs=out_specs, check_vma=False)

time: 310 us -> 308 us (level)
  waiting for transfers between devices: 139 us -> 118 us
  starting transfers between devices: 64.2 us -> 78.6 us
    all_to_all x3, waiting for transfers between devices: 76.6 us -> 42.5 us  [the longest x1 22.4 us: layer(): returned = lax.all_to_all(spread(summed, capacity), SP, 0, 0, tiled=True)]
    ppermute x2, waiting for transfers between devices: 8.94 us -> 25.1 us  [neighbours(): return (lax.ppermute(array, 'tp', up), lax.ppermute(array, 'tp', down))]
    ppermute x14 -> x12, waiting for transfers between devices: 42.6 us -> 28.4 us  [the longest x1 15.3 us: layer(): held_routes = lax.ppermute(routes, SP_TP, whole)]
    all_to_all x3, starting transfers between devices: 29.3 us -> 41.5 us  [the longest x1 30.3 us: layer(): lax.all_to_all(slots, SP_TP, 0, 0, axis_index_groups=ranks, tiled=True)]
    all_gather x1, waiting for transfers between devices: 11.2 us -> 20.3 us  [layer(): own = lax.all_gather(near, 'sp_0').reshape(-1, *block.shape)]
    slice x1 -> x3, local copies, waits for them, and re-layouts: 1.13 us -> 6.64 us  [the longest x1 2.78 us: layer(): across_high = lax.ppermute(down_after[half:], 'tp', down)]
    split x1 -> x0, local copies, waits for them, and re-layouts: 3.95 us -> none  [local(): low, high = jnp.split(expert_down[0], 2)]
    ppermute x14 -> x12, starting transfers between devices: 28.3 us -> 29.4 us  [the longest x1 7.83 us: layer(): mirrored_queries = lax.ppermute(queries[HALF:], SP, mirror)]
  transfers between devices with their start and end apart: 22 -> 20, of which waited for: 13 -> 9; matrix products, arithmetic and copies ran while one was open for 11% -> 11% of each run, Pallas kernels for 10% -> 9%
where the time goes in v6:
time: 308 us; the launch traced here: 303 us
  waiting for transfers between devices  118 us (38%)
  starting transfers between devices  78.6 us (26%)
  Pallas kernels  35.7 us (12%)
  matrix products  30.4 us (10%)
  between operations  13.7 us (4%)
  blocking collectives  13.5 us (4%)
  local copies, waits for them, and re-layouts  11.9 us (4%)
    all_to_all x1, starting transfers between devices, layer(): lax.all_to_all(slots, SP_TP, 0, 0, axis_index_groups=ranks, tiled=True)  30.3 us
    ppermute x2, waiting for transfers between devices, neighbours(): return (lax.ppermute(array, 'tp', up), lax.ppermute(array, 'tp', down))  25.1 us
    all_to_all x1, waiting for transfers between devices, layer(): returned = lax.all_to_all(spread(summed, capacity), SP, 0, 0, tiled=True)  22.4 us
    pallas_call x1, Pallas kernels, attend_rows(): pl.pallas_call(functools.partial(attend_body, blocks=blocks, heads=heads)...  22.2 us
    all_gather x1, waiting for transfers between devices, layer(): own = lax.all_gather(near, 'sp_0').reshape(-1, *block.shape)  20.3 us
    ppermute x1, waiting for transfers between devices, layer(): held_routes = lax.ppermute(routes, SP_TP, whole)  15.3 us
    all_gather x1, blocking collectives, layer(): near = lax.all_gather(block, 'sp_1')  13.5 us
    all_to_all x1, waiting for transfers between devices, layer(): lax.all_to_all(partial.reshape(head_devices, -1, partial.shape[1]), 'tp',...  12.8 us
  transfers between devices with their start and end apart: 20, of which 9 were waited for; matrix products, arithmetic and copies ran while one was open for 11% of the time, Pallas kernels for 9%

profile of v6, /device:TPU:6, one launch (start us, length us, event | category | flops | bytes accessed | tf_op | source)
XLA Modules:
  0.0 302.8 jit_solution(17721819784377360353)
XLA Ops:
  6.5 1.1 fusion.39
  7.7 7.8 %collective-permute-start.2 = (bf16[128,512]{1,0:T(8,128)(2,1)S(1)}, bf16[128,512]{1,0:T(8,128)(2,1)S(1)}, u32[]{:S(2)}, u32[]{:S(2)}) collective-permute-start(bf16[128,512]{1,0:T(8,128)(2,1)S(1)} %get-tuple-element.29), channel_id=1, source_target_pairs={{0,252},{4,248},{8,244},{12,240},{16,236},{20,232},{24,228},{28,22... | collective-permute-start | bytes 393224 | tf_op jit(solution)/shard_map/ppermute | solution.py:376
  15.5 1.6 prepare_keys.1
  17.1 13.5 %all-gather = bf16[640,256]{1,0:T(8,128)(2,1)} all-gather(bf16[160,256]{1,0:T(8,128)(2,1)} %prepare_keys.1), channel_id=2, replica_groups=mesh['sp_0'=8,'sp_1'=4,'sp_2'=2,'tp'=4] {'sp_1'}, dimensions={0}, use_global_device_ids=true | all-gather | bytes 409600 | tf_op jit(solution)/shard_map/all_gather | solution.py:380
  30.6 0.9 collective-permute-start.1
  31.5 2.4 collective-permute-start
  33.9 1.9 collective-permute-start.3
  36.6 7.0 %collective-permute-start.4 = (s32[64,2]{1,0:T(8,128)S(1)}, s32[64,2]{1,0:T(8,128)S(1)}, u32[]{:S(2)}, u32[]{:S(2)}) collective-permute-start(s32[64,2]{1,0:T(8,128)S(1)} %copy.15.routes_ref), channel_id=1, source_target_pairs={{0,0},{1,1},{2,254},{3,255},{4,4},{5,5},{6,250},{7,251},{8,8},{9,9... | collective-permute-start | bytes 1544 | tf_op jit(solution)/shard_map/ppermute | solution.py:383
  43.6 15.3 %collective-permute-done.4 = s32[64,2]{1,0:T(8,128)S(1)} collective-permute-done((s32[64,2]{1,0:T(8,128)S(1)}, s32[64,2]{1,0:T(8,128)S(1)}, u32[]{:S(2)}, u32[]{:S(2)}) %collective-permute-start.4) | collective-permute-done | bytes 544 | tf_op jit(solution)/shard_map/ppermute | solution.py:383
  58.9 20.3 %all-gather.4.cloned.1.call-done.own_ref = bf16[32,160,256]{2,1,0:T(8,128)(2,1)} async-done(((bf16[4,160,256]{2,1,0:T(8,128)(2,1)}), bf16[32,160,256]{2,1,0:T(8,128)(2,1)}) %all-gather.4.cloned.1.call-update) | async-done | bytes 2621456 | tf_op jit(solution)/shard_map/all_gather | solution.py:384
  79.2 5.2 %collective-permute-done.5.other_ref = bf16[32,160,256]{2,1,0:T(8,128)(2,1)} collective-permute-done((bf16[32,160,256]{2,1,0:T(8,128)(2,1)}, bf16[32,160,256]{2,1,0:T(8,128)(2,1)}, u32[]{:S(2)}, u32[]{:S(2)}) %collective-permute-start.5) | collective-permute-done | bytes 2621472 | tf_op jit(solution)/shard_map/ppermute | solution.py:386
  84.4 1.7 copy-done.1
  86.2 22.2 %attend_rows.1 = bf16[2,128,512]{2,1,0:T(8,128)(2,1)S(1)} custom-call(s32[1]{0:T(128)} %bitcast.1.index_ref, bf16[128,512]{1,0:T(8,128)(2,1)S(1)} %get-tuple-element.30.qa_ref, bf16[128,512]{1,0:T(8,128)(2,1)S(1)} %collective-permute-done.2.qb_ref, bf16[32,160,256]{2,1,0:T(8,128)(2,1)S(1)} %copy-done.1, bf16[32,160,256]{2,1,0:T(8,128)(2,1)} %collective-permute-done.5.other_ref), custom_call_target="tpu_custom_call" | custom-call | tf_op jit(solution)/shard_map/attend_rows/pallas_call | solution.py:196
  108.4 1.8 convolution_convert_fusion
  110.2 4.5 %all-to-all-start = ((bf16[4,64,2048]{2,1,0:T(8,128)(2,1)}), bf16[4,64,2048]{2,1,0:T(8,128)(2,1)}, u32[]{:S(2)}, u32[]{:S(2)}) async-start(bf16[4,64,2048]{2,1,0:T(8,128)(2,1)} %bitcast.55), calls=%async_computation | async-start | bytes 2097152 | tf_op jit(solution)/shard_map/all_to_all | solution.py:397
  115.3 12.8 %all-to-all-done.parts_ref = bf16[4,64,2048]{2,1,0:T(8,128)(2,1)} async-done(((bf16[4,64,2048]{2,1,0:T(8,128)(2,1)}), bf16[4,64,2048]{2,1,0:T(8,128)(2,1)}, u32[]{:S(2)}, u32[]{:S(2)}) %all-to-all-start) | async-done | bytes 1048608 | tf_op jit(solution)/shard_map/all_to_all | solution.py:397
  128.1 3.3 %dispatch.1 = (f32[64,2048]{1,0:T(8,128)}, bf16[64,48,128]{2,1,0:T(8,128)(2,1)}) custom-call(bf16[4,64,2048]{2,1,0:T(8,128)(2,1)} %all-to-all-done.parts_ref, bf16[64,2048]{1,0:T(8,128)(2,1)} %collective-permute-done.3.residual_ref, f32[1,2048]{1,0:T(1,128)} %bitcast.57, s32[64,2]{1,0:T(8,128)} %subtract_select_fusion.routes_ref), custom_call_target="tpu_custom_call" | custom-call | tf_op jit(solution)/shard_map/dispatch/pallas_call | solution.py:266
  131.4 30.3 %all-to-all-start.1 = ((bf16[64,48,128]{2,1,0:T(8,128)(2,1)}), bf16[64,48,128]{2,1,0:T(8,128)(2,1)}, u32[]{:S(2)}, u32[]{:S(2)}) async-start(bf16[64,48,128]{2,1,0:T(8,128)(2,1)} %get-tuple-element.23), calls=%async_computation.1 | async-start | bytes 1572864 | tf_op jit(solution)/shard_map/all_to_all | solution.py:412
  161.8 2.7 slice.22
  164.5 2.8 slice.23
  167.3 3.2 %collective-permute-start.14 = (bf16[384,2048]{1,0:T(8,128)(2,1)}, bf16[384,2048]{1,0:T(8,128)(2,1)}, u32[]{:S(2)}, u32[]{:S(2)}) collective-permute-start(bf16[384,2048]{1,0:T(8,128)(2,1)} %slice.22), channel_id=1, source_target_pairs={{0,1},{1,2},{2,3},{3,0},{4,5},{5,6},{6,7},{7,4},{8,9},{9,10},{10,1... | collective-permute-start | bytes 4718600 | tf_op jit(solution)/shard_map/ppermute | solution.py:392
  170.5 3.1 %collective-permute-start.12 = (f32[64,2048]{1,0:T(8,128)}, f32[64,2048]{1,0:T(8,128)}, u32[]{:S(2)}, u32[]{:S(2)}) collective-permute-start(f32[64,2048]{1,0:T(8,128)} %get-tuple-element.26), channel_id=1, source_target_pairs={{0,0},{1,1},{2,254},{3,255},{4,4},{5,5},{6,250},{7,251},{8,8},{9,9... | collective-permute-start | bytes 1572872 | tf_op jit(solution)/shard_map/ppermute | solution.py:407
  173.6 7.3 %all-to-all-done.1.arrived_ref = bf16[64,48,128]{2,1,0:T(8,128)(2,1)} async-done(((bf16[64,48,128]{2,1,0:T(8,128)(2,1)}), bf16[64,48,128]{2,1,0:T(8,128)(2,1)}, u32[]{:S(2)}, u32[]{:S(2)}) %all-to-all-start.1) | async-done | bytes 786464 | tf_op jit(solution)/shard_map/all_to_all | solution.py:412
  180.9 2.6 arrange.1
  183.5 3.9 %collective-permute-start.8 = (bf16[192,2048]{1,0:T(8,128)(2,1)}, bf16[192,2048]{1,0:T(8,128)(2,1)}, u32[]{:S(2)}, u32[]{:S(2)}) collective-permute-start(bf16[192,2048]{1,0:T(8,128)(2,1)} %arrange.1), channel_id=1, source_target_pairs={{0,1},{1,2},{2,3},{3,0},{4,5},{5,6},{6,7},{7,4},{8,9},{9,10},{10,1... | collective-permute-start | bytes 2359304 | tf_op jit(solution)/shard_map/ppermute | solution.py:361
  187.4 3.7 %fusion.18 = f32[192,768]{1,0:T(8,128)} fusion(bf16[192,2048]{1,0:T(8,128)(2,1)} %arrange.1, bf16[1,2048,768]{2,1,0:T(8,128)(2,1)} %param.19), kind=kOutput, calls=%fused_computation.18 | convolution fusion | flops 603979776 | bytes 4521984 | tf_op jit(solution)/shard_map/dot_general | solution.py:418
  191.1 5.1 %fusion.28 = f32[192,2048]{1,0:T(8,128)} fusion(bf16[192,2048]{1,0:T(8,128)(2,1)} %arrange.1, bf16[1,2048,768]{2,1,0:T(8,128)(2,1)S(1)} %copy-done, f32[192,768]{1,0:T(8,128)} %fusion.18, bf16[1,768,2048]{2,1,0:T(8,128)(2,1)} %param.21), kind=kOutput, calls=%fused_computation.26 | convolution fusion | flops 1208844288 | bytes 9240576 | tf_op jit(solution)/shard_map/dot_general | solution.py:430
  196.2 25.1 %collective-permute-done.8 = bf16[192,2048]{1,0:T(8,128)(2,1)} collective-permute-done((bf16[192,2048]{1,0:T(8,128)(2,1)}, bf16[192,2048]{1,0:T(8,128)(2,1)}, u32[]{:S(2)}, u32[]{:S(2)}) %collective-permute-start.8) | collective-permute-done | bytes 786464 | tf_op jit(solution)/shard_map/ppermute | solution.py:361
  221.3 1.0 slice.24
  222.4 3.8 %collective-permute-start.10 = (bf16[96,2048]{1,0:T(8,128)(2,1)S(1)}, bf16[96,2048]{1,0:T(8,128)(2,1)S(1)}, u32[]{:S(2)}, u32[]{:S(2)}) collective-permute-start(bf16[96,2048]{1,0:T(8,128)(2,1)S(1)} %slice.24), channel_id=1, source_target_pairs={{0,1},{1,2},{2,3},{3,0},{4,5},{5,6},{6,7},{7,4},{8,9},{9,10},{10,1... | collective-permute-start | bytes 1179656 | tf_op jit(solution)/shard_map/ppermute | solution.py:366
  226.1 1.0 slice.25
  227.2 2.9 fusion.14
  230.2 2.0 fusion.16
  232.1 1.9 multiply_convert_fusion.1
  234.1 1.9 multiply_convert_fusion.2
  236.1 2.1 collective-permute-done.11
  238.1 1.2 collective-permute-start.7
  239.5 0.8 fusion.12
  240.3 0.8 multiply_convert_fusion
  241.1 1.7 collective-permute-start.13
  242.8 7.8 %collective-permute-done.7 = bf16[192,768]{1,0:T(8,128)(2,1)S(1)} collective-permute-done((bf16[192,768]{1,0:T(8,128)(2,1)S(1)}, bf16[192,768]{1,0:T(8,128)(2,1)S(1)}, u32[]{:S(2)}, u32[]{:S(2)}) %collective-permute-start.7) | collective-permute-done | bytes 294944 | tf_op jit(solution)/shard_map/ppermute | solution.py:426
  250.6 2.8 convolution_add_fusion.1
  253.4 2.7 fusion
  256.1 4.0 %fusion.20.rows_ref = f32[192,2048]{1,0:T(8,128)} fusion(f32[192,2048]{1,0:T(8,128)S(1)} %fusion, f32[192,2048]{1,0:T(8,128)S(1)} %convolution_add_fusion.1, bf16[192,768]{1,0:T(8,128)(2,1)S(1)} %collective-permute-done.9, bf16[768,2048]{1,0:T(8,128)(2,1)} %collective-permute-done.1), kind=kOutput, calls=%fused_computation.21 | convolution fusion | flops 604766208 | bytes 8159232 | tf_op jit(solution)/shard_map/dot_general | solution.py:436
  260.1 2.9 spread.1
  262.9 6.7 %all-to-all-start.2 = ((bf16[64,48,128]{2,1,0:T(8,128)(2,1)}), bf16[64,48,128]{2,1,0:T(8,128)(2,1)}, u32[]{:S(2)}, u32[]{:S(2)}) async-start(bf16[64,48,128]{2,1,0:T(8,128)(2,1)} %spread.1), calls=%async_computation.2 | async-start | bytes 1572864 | tf_op jit(solution)/shard_map/all_to_all | solution.py:437
  270.3 22.4 %all-to-all-done.2.returned_ref = bf16[64,48,128]{2,1,0:T(8,128)(2,1)} async-done(((bf16[64,48,128]{2,1,0:T(8,128)(2,1)}), bf16[64,48,128]{2,1,0:T(8,128)(2,1)}, u32[]{:S(2)}, u32[]{:S(2)}) %all-to-all-start.2) | async-done | bytes 786464 | tf_op jit(solution)/shard_map/all_to_all | solution.py:437
  292.7 3.2 %combine.1 = bf16[64,2048]{1,0:T(8,128)(2,1)} custom-call(bf16[64,48,128]{2,1,0:T(8,128)(2,1)} %all-to-all-done.2.returned_ref, f32[64,2048]{1,0:T(8,128)} %collective-permute-done.12.hidden_ref, s32[64,2]{1,0:T(8,128)} %copy-done.5, f32[64,2]{1,0:T(8,128)} %copy.17.weight_ref), custom_call_target="tpu_custom_call" | custom-call | tf_op jit(solution)/shard_map/combine/pallas_call | solution.py:332
  (35 shorter events, 2.4 us)
Async XLA Ops:
  6.5 184.6 %copy-start = (bf16[1,2048,768]{2,1,0:T(8,128)(2,1)S(1)}, bf16[1,2048,768]{2,1,0:T(8,128)(2,1)}, u32[]{:S(2)}) copy-start(bf16[1,2048,768]{2,1,0:T(8,128)(2,1)} %param.20) | copy-start | bytes 9437188
  6.5 72.6 %all-gather.4.cloned.1.call-start = ((), (), s32[]{:S(2)}) async-start(), calls=%async_computation.3 | async-start | bytes 2949120 | tf_op jit(solution)/shard_map/all_gather | solution.py:384
  7.7 22.9 %collective-permute-start.2 = (bf16[128,512]{1,0:T(8,128)(2,1)S(1)}, bf16[128,512]{1,0:T(8,128)(2,1)S(1)}, u32[]{:S(2)}, u32[]{:S(2)}) collective-permute-start(bf16[128,512]{1,0:T(8,128)(2,1)S(1)} %get-tuple-element.29), channel_id=1, source_target_pairs={{0,252},{4,248},{8,244},{12,240},{16,236},{20,232},{24,228},{28,22... | collective-permute-start | bytes 393224 | tf_op jit(solution)/shard_map/ppermute | solution.py:376
  30.6 77.7 %collective-permute-start.1 = (bf16[768,2048]{1,0:T(8,128)(2,1)}, bf16[768,2048]{1,0:T(8,128)(2,1)}, u32[]{:S(2)}, u32[]{:S(2)}) collective-permute-start(bf16[768,2048]{1,0:T(8,128)(2,1)} %bitcast.59), channel_id=1, source_target_pairs={{0,3},{1,0},{2,1},{3,2},{4,7},{5,4},{6,5},{7,6},{8,11},{9,8},{10,9... | collective-permute-start | bytes 9437192 | tf_op jit(solution)/shard_map/ppermute | solution.py:379
  31.5 76.8 %collective-permute-start = (bf16[768,2048]{1,0:T(8,128)(2,1)}, bf16[768,2048]{1,0:T(8,128)(2,1)}, u32[]{:S(2)}, u32[]{:S(2)}) collective-permute-start(bf16[768,2048]{1,0:T(8,128)(2,1)} %bitcast.60), channel_id=1, source_target_pairs={{0,1},{1,2},{2,3},{3,0},{4,5},{5,6},{6,7},{7,4},{8,9},{9,10},{10,1... | collective-permute-start | bytes 9437192 | tf_op jit(solution)/shard_map/ppermute | solution.py:378
  33.9 25.0 %collective-permute-start.3 = (bf16[64,2048]{1,0:T(8,128)(2,1)}, bf16[64,2048]{1,0:T(8,128)(2,1)}, u32[]{:S(2)}, u32[]{:S(2)}) collective-permute-start(bf16[64,2048]{1,0:T(8,128)(2,1)} %param.14), channel_id=1, source_target_pairs={{0,0},{1,1},{2,254},{3,255},{4,4},{5,5},{6,250},{7,251},{8,8},{9,9... | collective-permute-start | bytes 786440 | tf_op jit(solution)/shard_map/ppermute | solution.py:382
  36.6 73.6 %copy-start.5 = (s32[64,2]{1,0:T(8,128)}, s32[64,2]{1,0:T(8,128)S(1)}, u32[]{:S(2)}) copy-start(s32[64,2]{1,0:T(8,128)S(1)} %copy.15.routes_ref) | copy-start | bytes 1540
  36.6 22.3 %collective-permute-start.4 = (s32[64,2]{1,0:T(8,128)S(1)}, s32[64,2]{1,0:T(8,128)S(1)}, u32[]{:S(2)}, u32[]{:S(2)}) collective-permute-start(s32[64,2]{1,0:T(8,128)S(1)} %copy.15.routes_ref), channel_id=1, source_target_pairs={{0,0},{1,1},{2,254},{3,255},{4,4},{5,5},{6,250},{7,251},{8,8},{9,9... | collective-permute-start | bytes 1544 | tf_op jit(solution)/shard_map/ppermute | solution.py:383
  79.2 5.3 %collective-permute-start.5 = (bf16[32,160,256]{2,1,0:T(8,128)(2,1)}, bf16[32,160,256]{2,1,0:T(8,128)(2,1)}, u32[]{:S(2)}, u32[]{:S(2)}) collective-permute-start(bf16[32,160,256]{2,1,0:T(8,128)(2,1)} %all-gather.4.cloned.1.call-done.own_ref), channel_id=1, source_target_pairs={{0,4},{4,0},{1,5},{5,1},{2,6},{6,2},{3,7},{7,3},{8,12},{12,8},{9,1... | collective-permute-start | bytes 7864328 | tf_op jit(solution)/shard_map/ppermute | solution.py:386
  84.4 1.7 copy-start.1
  86.2 22.2 %copy-start.3 = (bf16[512,2048]{1,0:T(8,128)(2,1)S(1)}, bf16[512,2048]{1,0:T(8,128)(2,1)}, u32[]{:S(2)}) copy-start(bf16[512,2048]{1,0:T(8,128)(2,1)} %param.15) | copy-start | bytes 6291460
  110.2 17.9 %all-to-all-start = ((bf16[4,64,2048]{2,1,0:T(8,128)(2,1)}), bf16[4,64,2048]{2,1,0:T(8,128)(2,1)}, u32[]{:S(2)}, u32[]{:S(2)}) async-start(bf16[4,64,2048]{2,1,0:T(8,128)(2,1)} %bitcast.55), calls=%async_computation | async-start | bytes 2097152 | tf_op jit(solution)/shard_map/all_to_all | solution.py:397
  131.4 49.5 %all-to-all-start.1 = ((bf16[64,48,128]{2,1,0:T(8,128)(2,1)}), bf16[64,48,128]{2,1,0:T(8,128)(2,1)}, u32[]{:S(2)}, u32[]{:S(2)}) async-start(bf16[64,48,128]{2,1,0:T(8,128)(2,1)} %get-tuple-element.23), calls=%async_computation.1 | async-start | bytes 1572864 | tf_op jit(solution)/shard_map/all_to_all | solution.py:412
  167.3 86.1 %collective-permute-start.15 = (bf16[384,2048]{1,0:T(8,128)(2,1)}, bf16[384,2048]{1,0:T(8,128)(2,1)}, u32[]{:S(2)}, u32[]{:S(2)}) collective-permute-start(bf16[384,2048]{1,0:T(8,128)(2,1)} %slice.23), channel_id=1, source_target_pairs={{0,3},{1,0},{2,1},{3,2},{4,7},{5,4},{6,5},{7,6},{8,11},{9,8},{10,9... | collective-permute-start | bytes 4718600 | tf_op jit(solution)/shard_map/ppermute | solution.py:393
  167.3 86.1 %collective-permute-start.14 = (bf16[384,2048]{1,0:T(8,128)(2,1)}, bf16[384,2048]{1,0:T(8,128)(2,1)}, u32[]{:S(2)}, u32[]{:S(2)}) collective-permute-start(bf16[384,2048]{1,0:T(8,128)(2,1)} %slice.22), channel_id=1, source_target_pairs={{0,1},{1,2},{2,3},{3,0},{4,5},{5,6},{6,7},{7,4},{8,9},{9,10},{10,1... | collective-permute-start | bytes 4718600 | tf_op jit(solution)/shard_map/ppermute | solution.py:392
  170.5 69.0 %collective-permute-start.12 = (f32[64,2048]{1,0:T(8,128)}, f32[64,2048]{1,0:T(8,128)}, u32[]{:S(2)}, u32[]{:S(2)}) collective-permute-start(f32[64,2048]{1,0:T(8,128)} %get-tuple-element.26), channel_id=1, source_target_pairs={{0,0},{1,1},{2,254},{3,255},{4,4},{5,5},{6,250},{7,251},{8,8},{9,9... | collective-permute-start | bytes 1572872 | tf_op jit(solution)/shard_map/ppermute | solution.py:407
  183.5 37.8 %collective-permute-start.8 = (bf16[192,2048]{1,0:T(8,128)(2,1)}, bf16[192,2048]{1,0:T(8,128)(2,1)}, u32[]{:S(2)}, u32[]{:S(2)}) collective-permute-start(bf16[192,2048]{1,0:T(8,128)(2,1)} %arrange.1), channel_id=1, source_target_pairs={{0,1},{1,2},{2,3},{3,0},{4,5},{5,6},{6,7},{7,4},{8,9},{9,10},{10,1... | collective-permute-start | bytes 2359304 | tf_op jit(solution)/shard_map/ppermute | solution.py:361
  187.4 38.8 %collective-permute-start.6 = (bf16[192,2048]{1,0:T(8,128)(2,1)}, bf16[192,2048]{1,0:T(8,128)(2,1)}, u32[]{:S(2)}, u32[]{:S(2)}) collective-permute-start(bf16[192,2048]{1,0:T(8,128)(2,1)} %arrange.1), channel_id=1, source_target_pairs={{0,3},{1,0},{2,1},{3,2},{4,7},{5,4},{6,5},{7,6},{8,11},{9,8},{10,9... | collective-permute-start | bytes 2359304 | tf_op jit(solution)/shard_map/ppermute | solution.py:361
  196.2 33.9 %copy-start.2 = (bf16[1,2048,768]{2,1,0:T(8,128)(2,1)S(1)}, bf16[1,2048,768]{2,1,0:T(8,128)(2,1)}, u32[]{:S(2)}) copy-start(bf16[1,2048,768]{2,1,0:T(8,128)(2,1)} %param.19) | copy-start | bytes 9437188
  222.4 13.6 %collective-permute-start.10 = (bf16[96,2048]{1,0:T(8,128)(2,1)S(1)}, bf16[96,2048]{1,0:T(8,128)(2,1)S(1)}, u32[]{:S(2)}, u32[]{:S(2)}) collective-permute-start(bf16[96,2048]{1,0:T(8,128)(2,1)S(1)} %slice.24), channel_id=1, source_target_pairs={{0,1},{1,2},{2,3},{3,0},{4,5},{5,6},{6,7},{7,4},{8,9},{9,10},{10,1... | collective-permute-start | bytes 1179656 | tf_op jit(solution)/shard_map/ppermute | solution.py:366
  227.2 11.0 %collective-permute-start.11 = (bf16[96,2048]{1,0:T(8,128)(2,1)S(1)}, bf16[96,2048]{1,0:T(8,128)(2,1)S(1)}, u32[]{:S(2)}, u32[]{:S(2)}) collective-permute-start(bf16[96,2048]{1,0:T(8,128)(2,1)S(1)} %slice.25), channel_id=1, source_target_pairs={{0,3},{1,0},{2,1},{3,2},{4,7},{5,4},{6,5},{7,6},{8,11},{9,8},{10,9... | collective-permute-start | bytes 1179656 | tf_op jit(solution)/shard_map/ppermute | solution.py:366
  236.0 20.1 %collective-permute-start.9 = (bf16[192,768]{1,0:T(8,128)(2,1)S(1)}, bf16[192,768]{1,0:T(8,128)(2,1)S(1)}, u32[]{:S(2)}, u32[]{:S(2)}) collective-permute-start(bf16[192,768]{1,0:T(8,128)(2,1)S(1)} %multiply_convert_fusion.1), channel_id=1, source_target_pairs={{0,3},{1,0},{2,1},{3,2},{4,7},{5,4},{6,5},{7,6},{8,11},{9,8},{10,9... | collective-permute-start | bytes 884744 | tf_op jit(solution)/shard_map/ppermute | solution.py:427
  238.1 12.4 %collective-permute-start.7 = (bf16[192,768]{1,0:T(8,128)(2,1)S(1)}, bf16[192,768]{1,0:T(8,128)(2,1)S(1)}, u32[]{:S(2)}, u32[]{:S(2)}) collective-permute-start(bf16[192,768]{1,0:T(8,128)(2,1)S(1)} %multiply_convert_fusion.2), channel_id=1, source_target_pairs={{0,1},{1,2},{2,3},{3,0},{4,5},{5,6},{6,7},{7,4},{8,9},{9,10},{10,1... | collective-permute-start | bytes 884744 | tf_op jit(solution)/shard_map/ppermute | solution.py:426
  240.3 10.3 %copy-start.4 = (f32[192,2048]{1,0:T(8,128)S(1)}, f32[192,2048]{1,0:T(8,128)}, u32[]{:S(2)}) copy-start(f32[192,2048]{1,0:T(8,128)} %fusion.28) | copy-start | bytes 4718596
  241.1 12.3 %collective-permute-start.13 = (bf16[192,768]{1,0:T(8,128)(2,1)S(1)}, bf16[192,768]{1,0:T(8,128)(2,1)S(1)}, u32[]{:S(2)}, u32[]{:S(2)}) collective-permute-start(bf16[192,768]{1,0:T(8,128)(2,1)S(1)} %multiply_convert_fusion), channel_id=1, source_target_pairs={{0,2},{1,3},{2,0},{3,1},{4,6},{5,7},{6,4},{7,5},{8,10},{9,11},{10,... | collective-permute-start | bytes 884744 | tf_op jit(solution)/shard_map/ppermute | solution.py:429
  260.1 9.6 %copy-start.6 = (f32[64,2]{0,1:T(2,128)S(1)}, f32[64,2]{0,1:T(2,128)}, u32[]{:S(2)}) copy-start(f32[64,2]{0,1:T(2,128)} %param.18) | copy-start | bytes 1540
  262.9 29.8 %all-to-all-start.2 = ((bf16[64,48,128]{2,1,0:T(8,128)(2,1)}), bf16[64,48,128]{2,1,0:T(8,128)(2,1)}, u32[]{:S(2)}, u32[]{:S(2)}) async-start(bf16[64,48,128]{2,1,0:T(8,128)(2,1)} %spread.1), calls=%async_computation.2 | async-start | bytes 1572864 | tf_op jit(solution)/shard_map/all_to_all | solution.py:437
Sparse Core Ops, SparseCore 0:
  30.7 48.4 all-gather.3

commit v7 on v6

--- a/solution.py
+++ b/solution.py
@@ -379,14 +379,16 @@
     down_after = lax.ppermute(down_own, "tp", down)
     near = lax.all_gather(block, "sp_1")
     near, mirrored_queries = lax.optimization_barrier((near, mirrored_queries))
-    held_residual = lax.ppermute(residual_in, SP_TP, whole)
-    held_routes = lax.ppermute(routes, SP_TP, whole)
     own = lax.all_gather(near, "sp_0").reshape(-1, *block.shape)
-    own, held_residual, held_routes = lax.optimization_barrier((own, held_residual, held_routes))
+    own, swapped_residual, swapped_routes = lax.optimization_barrier((own, residual_in, routes))
+    held_residual = lax.ppermute(swapped_residual, SP_TP, whole)
+    held_routes = lax.ppermute(swapped_routes, SP_TP, whole)
     other = lax.ppermute(own, "sp_2", [(0, 1), (1, 0)])
-    attended = attend_rows(index.reshape(1), queries[:HALF], mirrored_queries, own, other)
-    down_before, down_after, attended = lax.optimization_barrier(
-        (down_before, down_after, attended)
+    attended = attend_rows(
+        index.reshape(1), queries[:HALF], mirrored_queries, own, other
+    )
+    down_before, down_after, attended, held_residual, held_routes = lax.optimization_barrier(
+        (down_before, down_after, attended, held_residual, held_routes)
     )
     half = down_own.shape[0] // 2
     across_low = lax.ppermute(down_before[:half], "tp", up)
@@ -404,7 +406,6 @@
         parts, held_residual, norm_gain, ranked_routes, seq_devices, capacity
     )
     down_across = jnp.concatenate([across_low, across_high])
-    hidden_state = lax.ppermute(held_hidden, SP_TP, whole)
     ranks = [
         [(i if 2 * t < head_devices else seq_devices - 1 - i) * head_devices + t for i in range(seq_devices)]
         for t in range(head_devices)
@@ -412,6 +413,8 @@
     incoming = lax.all_to_all(
         slots, SP_TP, 0, 0, axis_index_groups=ranks, tiled=True
     )
+    incoming, held_hidden = lax.optimization_barrier((incoming, held_hidden))
+    hidden_state = lax.ppermute(held_hidden, SP_TP, whole)
     rows_own = arrange(incoming, capacity)
 
     def units(rows):

time: 308 us -> 307 us (level)
  waiting for transfers between devices: 118 us -> 112 us
  starting transfers between devices: 78.6 us -> 83.6 us
    all_gather x1, waiting for transfers between devices: 20.3 us -> 38.3 us  [layer(): own = lax.all_gather(near, 'sp_0').reshape(-1, *block.shape)]
    ppermute x2, waiting for transfers between devices: 15.3 us -> 0.01 us  [the longest x1 0.01 us: layer(): held_routes = lax.ppermute(swapped_routes, SP_TP, whole)]
    ppermute x2, waiting for transfers between devices: 25.1 us -> 18.9 us  [neighbours(): return (lax.ppermute(array, 'tp', up), lax.ppermute(array, 'tp', down))]
    ppermute x1, waiting for transfers between devices: 5.25 us -> 0.01 us  [layer(): other = lax.ppermute(own, 'sp_2', [(0, 1), (1, 0)])]
    all_to_all x1, waiting for transfers between devices: 7.25 us -> 11.6 us  [layer(): lax.all_to_all(slots, SP_TP, 0, 0, axis_index_groups=ranks, tiled=True)]
    ppermute x1, starting transfers between devices: 3.23 us -> 0.01 us  [layer(): across_low = lax.ppermute(down_before[:half], 'tp', up)]
    all_to_all x1, starting transfers between devices: 6.69 us -> 9.81 us  [layer(): returned = lax.all_to_all(spread(summed, capacity), SP, 0, 0, tiled=True)]
  transfers between devices with their start and end apart: 20 -> 20, of which waited for: 9 -> 7; matrix products, arithmetic and copies ran while one was open for 11% -> 12% of each run, Pallas kernels for 9% -> 9%
where the time goes in v7:
time: 307 us; the launch traced here: 302 us
  waiting for transfers between devices  112 us (36%)
  starting transfers between devices  83.6 us (27%)
  Pallas kernels  35.7 us (12%)
  matrix products  30.4 us (10%)
  between operations  13.7 us (4%)
  blocking collectives  13.5 us (4%)
  local copies, waits for them, and re-layouts  12.6 us (4%)
    all_gather x1, waiting for transfers between devices, layer(): own = lax.all_gather(near, 'sp_0').reshape(-1, *block.shape)  38.3 us
    all_to_all x1, starting transfers between devices, layer(): lax.all_to_all(slots, SP_TP, 0, 0, axis_index_groups=ranks, tiled=True)  33.1 us
    pallas_call x1, Pallas kernels, attend_rows(): pl.pallas_call(functools.partial(attend_body, blocks=blocks, heads=heads)...  22.2 us
    all_to_all x1, waiting for transfers between devices, layer(): returned = lax.all_to_all(spread(summed, capacity), SP, 0, 0, tiled=True)  21.7 us
    ppermute x2, waiting for transfers between devices, neighbours(): return (lax.ppermute(array, 'tp', up), lax.ppermute(array, 'tp', down))  18.9 us
    all_gather x1, blocking collectives, layer(): near = lax.all_gather(block, 'sp_1')  13.5 us
    all_to_all x1, waiting for transfers between devices, layer(): lax.all_to_all(partial.reshape(head_devices, -1, partial.shape[1]), 'tp',...  13.2 us
    all_to_all x1, waiting for transfers between devices, layer(): lax.all_to_all(slots, SP_TP, 0, 0, axis_index_groups=ranks, tiled=True)  11.6 us
  transfers between devices with their start and end apart: 20, of which 7 were waited for; matrix products, arithmetic and copies ran while one was open for 12% of the time, Pallas kernels for 9%

profile of v7, /device:TPU:6, one launch (start us, length us, event | category | flops | bytes accessed | tf_op | source)
XLA Modules:
  0.0 302.0 jit_solution(310252993314276017)
XLA Ops:
  6.5 1.1 fusion.39
  7.7 7.8 %collective-permute-start.2 = (bf16[128,512]{1,0:T(8,128)(2,1)S(1)}, bf16[128,512]{1,0:T(8,128)(2,1)S(1)}, u32[]{:S(2)}, u32[]{:S(2)}) collective-permute-start(bf16[128,512]{1,0:T(8,128)(2,1)S(1)} %get-tuple-element.37), channel_id=1, source_target_pairs={{0,252},{4,248},{8,244},{12,240},{16,236},{20,232},{24,228},{28,22... | collective-permute-start | bytes 393224 | tf_op jit(solution)/shard_map/ppermute | solution.py:376
  15.5 1.6 prepare_keys.1
  17.1 13.5 %all-gather = bf16[640,256]{1,0:T(8,128)(2,1)} all-gather(bf16[160,256]{1,0:T(8,128)(2,1)} %prepare_keys.1), channel_id=2, replica_groups=mesh['sp_0'=8,'sp_1'=4,'sp_2'=2,'tp'=4] {'sp_1'}, dimensions={0}, use_global_device_ids=true | all-gather | bytes 409600 | tf_op jit(solution)/shard_map/all_gather | solution.py:380
  31.1 1.5 collective-permute-start.1
  32.7 38.3 %all-gather.4.cloned.1.call-done.own_ref = bf16[32,160,256]{2,1,0:T(8,128)(2,1)} async-done(((bf16[4,160,256]{2,1,0:T(8,128)(2,1)}), bf16[32,160,256]{2,1,0:T(8,128)(2,1)}) %all-gather.4.cloned.1.call-update) | async-done | bytes 2621456 | tf_op jit(solution)/shard_map/all_gather | solution.py:382
  71.0 6.3 %collective-permute-start.4 = (bf16[64,2048]{1,0:T(8,128)(2,1)}, bf16[64,2048]{1,0:T(8,128)(2,1)}, u32[]{:S(2)}, u32[]{:S(2)}) collective-permute-start(bf16[64,2048]{1,0:T(8,128)(2,1)} %param.14), channel_id=1, source_target_pairs={{0,0},{1,1},{2,254},{3,255},{4,4},{5,5},{6,250},{7,251},{8,8},{9,9... | collective-permute-start | bytes 786440 | tf_op jit(solution)/shard_map/ppermute | solution.py:384
  77.3 0.8 copy.15
  78.1 2.5 collective-permute-start.5
  80.7 1.7 copy-done.1
  82.4 22.2 %attend_rows.1 = bf16[2,128,512]{2,1,0:T(8,128)(2,1)S(1)} custom-call(s32[1]{0:T(128)} %bitcast.1.index_ref, bf16[128,512]{1,0:T(8,128)(2,1)S(1)} %get-tuple-element.38.qa_ref, bf16[128,512]{1,0:T(8,128)(2,1)S(1)} %collective-permute-done.2.qb_ref, bf16[32,160,256]{2,1,0:T(8,128)(2,1)S(1)} %copy-done.1, bf16[32,160,256]{2,1,0:T(8,128)(2,1)} %collective-permute-done.3.other_ref), custom_call_target="tpu_custom_call" | custom-call | tf_op jit(solution)/shard_map/attend_rows/pallas_call | solution.py:196
  104.6 1.8 convolution_convert_fusion
  106.5 4.8 %all-to-all-start = ((bf16[4,64,2048]{2,1,0:T(8,128)(2,1)}), bf16[4,64,2048]{2,1,0:T(8,128)(2,1)}, u32[]{:S(2)}, u32[]{:S(2)}) async-start(bf16[4,64,2048]{2,1,0:T(8,128)(2,1)} %bitcast.55), calls=%async_computation | async-start | bytes 2097152 | tf_op jit(solution)/shard_map/all_to_all | solution.py:399
  111.9 13.2 %all-to-all-done.parts_ref = bf16[4,64,2048]{2,1,0:T(8,128)(2,1)} async-done(((bf16[4,64,2048]{2,1,0:T(8,128)(2,1)}), bf16[4,64,2048]{2,1,0:T(8,128)(2,1)}, u32[]{:S(2)}, u32[]{:S(2)}) %all-to-all-start) | async-done | bytes 1048608 | tf_op jit(solution)/shard_map/all_to_all | solution.py:399
  125.1 3.3 %dispatch.1 = (f32[64,2048]{1,0:T(8,128)}, bf16[64,48,128]{2,1,0:T(8,128)(2,1)}) custom-call(bf16[4,64,2048]{2,1,0:T(8,128)(2,1)} %all-to-all-done.parts_ref, bf16[64,2048]{1,0:T(8,128)(2,1)} %collective-permute-done.4.residual_ref, f32[1,2048]{1,0:T(1,128)} %bitcast.57, s32[64,2]{1,0:T(8,128)} %subtract_select_fusion.routes_ref), custom_call_target="tpu_custom_call" | custom-call | tf_op jit(solution)/shard_map/dispatch/pallas_call | solution.py:266
  128.3 33.1 %all-to-all-start.1 = ((bf16[64,48,128]{2,1,0:T(8,128)(2,1)}), bf16[64,48,128]{2,1,0:T(8,128)(2,1)}, u32[]{:S(2)}, u32[]{:S(2)}) async-start(bf16[64,48,128]{2,1,0:T(8,128)(2,1)} %get-tuple-element.29), calls=%async_computation.1 | async-start | bytes 1572864 | tf_op jit(solution)/shard_map/all_to_all | solution.py:413
  161.5 2.7 slice.22
  164.2 2.8 slice.23
  167.0 2.0 collective-permute-start.15
  169.0 11.6 %all-to-all-done.1.arrived_ref = bf16[64,48,128]{2,1,0:T(8,128)(2,1)} async-done(((bf16[64,48,128]{2,1,0:T(8,128)(2,1)}), bf16[64,48,128]{2,1,0:T(8,128)(2,1)}, u32[]{:S(2)}, u32[]{:S(2)}) %all-to-all-start.1) | async-done | bytes 786464 | tf_op jit(solution)/shard_map/all_to_all | solution.py:413
  180.6 2.6 arrange.1
  183.2 3.9 %collective-permute-start.8 = (bf16[192,2048]{1,0:T(8,128)(2,1)}, bf16[192,2048]{1,0:T(8,128)(2,1)}, u32[]{:S(2)}, u32[]{:S(2)}) collective-permute-start(bf16[192,2048]{1,0:T(8,128)(2,1)} %arrange.1), channel_id=1, source_target_pairs={{0,1},{1,2},{2,3},{3,0},{4,5},{5,6},{6,7},{7,4},{8,9},{9,10},{10,1... | collective-permute-start | bytes 2359304 | tf_op jit(solution)/shard_map/ppermute | solution.py:361
  187.1 4.3 %collective-permute-start.12 = (f32[64,2048]{1,0:T(8,128)}, f32[64,2048]{1,0:T(8,128)}, u32[]{:S(2)}, u32[]{:S(2)}) collective-permute-start(f32[64,2048]{1,0:T(8,128)} %get-tuple-element.34), channel_id=1, source_target_pairs={{0,0},{1,1},{2,254},{3,255},{4,4},{5,5},{6,250},{7,251},{8,8},{9,9... | collective-permute-start | bytes 1572872 | tf_op jit(solution)/shard_map/ppermute | solution.py:417
  191.4 3.8 %fusion.18 = f32[192,768]{1,0:T(8,128)} fusion(bf16[192,2048]{1,0:T(8,128)(2,1)} %arrange.1, bf16[1,2048,768]{2,1,0:T(8,128)(2,1)} %param.19), kind=kOutput, calls=%fused_computation.18 | convolution fusion | flops 603979776 | bytes 4521984 | tf_op jit(solution)/shard_map/dot_general | solution.py:421
  195.2 5.1 %fusion.28 = f32[192,2048]{1,0:T(8,128)} fusion(bf16[192,2048]{1,0:T(8,128)(2,1)} %arrange.1, bf16[1,2048,768]{2,1,0:T(8,128)(2,1)S(1)} %copy-done, f32[192,768]{1,0:T(8,128)} %fusion.18, bf16[1,768,2048]{2,1,0:T(8,128)(2,1)} %param.21), kind=kOutput, calls=%fused_computation.26 | convolution fusion | flops 1208844288 | bytes 9240576 | tf_op jit(solution)/shard_map/dot_general | solution.py:433
  200.3 17.5 %collective-permute-done.8 = bf16[192,2048]{1,0:T(8,128)(2,1)} collective-permute-done((bf16[192,2048]{1,0:T(8,128)(2,1)}, bf16[192,2048]{1,0:T(8,128)(2,1)}, u32[]{:S(2)}, u32[]{:S(2)}) %collective-permute-start.8) | collective-permute-done | bytes 786464 | tf_op jit(solution)/shard_map/ppermute | solution.py:361
  217.8 1.0 slice.24
  218.8 1.6 collective-permute-start.10
  220.4 1.4 collective-permute-done.6
  221.8 1.0 slice.25
  223.4 2.9 fusion.16
  226.4 1.9 fusion.14
  228.3 1.9 multiply_convert_fusion.2
  230.2 1.9 multiply_convert_fusion.1
  232.2 2.8 collective-permute-start.7
  235.0 0.8 fusion.12
  235.8 0.8 multiply_convert_fusion
  236.7 1.9 collective-permute-start.13
  238.5 8.2 %collective-permute-done.7 = bf16[192,768]{1,0:T(8,128)(2,1)S(1)} collective-permute-done((bf16[192,768]{1,0:T(8,128)(2,1)S(1)}, bf16[192,768]{1,0:T(8,128)(2,1)S(1)}, u32[]{:S(2)}, u32[]{:S(2)}) %collective-permute-start.7) | collective-permute-done | bytes 294944 | tf_op jit(solution)/shard_map/ppermute | solution.py:429
  246.7 2.7 convolution_add_fusion.1
  249.4 2.7 fusion
  252.2 4.0 %fusion.20.rows_ref = f32[192,2048]{1,0:T(8,128)} fusion(f32[192,2048]{1,0:T(8,128)S(1)} %fusion, f32[192,2048]{1,0:T(8,128)S(1)} %convolution_add_fusion.1, bf16[192,768]{1,0:T(8,128)(2,1)S(1)} %collective-permute-done.9, bf16[768,2048]{1,0:T(8,128)(2,1)} %collective-permute-done.1), kind=kOutput, calls=%fused_computation.21 | convolution fusion | flops 604766208 | bytes 8159232 | tf_op jit(solution)/shard_map/dot_general | solution.py:439
  256.1 2.9 spread.1
  259.0 9.8 %all-to-all-start.2 = ((bf16[64,48,128]{2,1,0:T(8,128)(2,1)}), bf16[64,48,128]{2,1,0:T(8,128)(2,1)}, u32[]{:S(2)}, u32[]{:S(2)}) async-start(bf16[64,48,128]{2,1,0:T(8,128)(2,1)} %spread.1), calls=%async_computation.2 | async-start | bytes 1572864 | tf_op jit(solution)/shard_map/all_to_all | solution.py:440
  268.9 0.7 copy.16.routes_ref
  269.6 0.7 copy.17.weight_ref
  270.3 21.7 %all-to-all-done.2.returned_ref = bf16[64,48,128]{2,1,0:T(8,128)(2,1)} async-done(((bf16[64,48,128]{2,1,0:T(8,128)(2,1)}), bf16[64,48,128]{2,1,0:T(8,128)(2,1)}, u32[]{:S(2)}, u32[]{:S(2)}) %all-to-all-start.2) | async-done | bytes 786464 | tf_op jit(solution)/shard_map/all_to_all | solution.py:440
  292.0 3.2 %combine.1 = bf16[64,2048]{1,0:T(8,128)(2,1)} custom-call(bf16[64,48,128]{2,1,0:T(8,128)(2,1)} %all-to-all-done.2.returned_ref, f32[64,2048]{1,0:T(8,128)} %collective-permute-done.12.hidden_ref, s32[64,2]{1,0:T(8,128)} %copy.16.routes_ref, f32[64,2]{1,0:T(8,128)} %copy.17.weight_ref), custom_call_target="tpu_custom_call" | custom-call | tf_op jit(solution)/shard_map/combine/pallas_call | solution.py:332
  (36 shorter events, 1.9 us)
Async XLA Ops:
  6.5 188.6 %copy-start = (bf16[1,2048,768]{2,1,0:T(8,128)(2,1)S(1)}, bf16[1,2048,768]{2,1,0:T(8,128)(2,1)}, u32[]{:S(2)}) copy-start(bf16[1,2048,768]{2,1,0:T(8,128)(2,1)} %param.20) | copy-start | bytes 9437188
  6.5 64.5 %all-gather.4.cloned.1.call-start = ((), (), s32[]{:S(2)}) async-start(), calls=%async_computation.3 | async-start | bytes 2949120 | tf_op jit(solution)/shard_map/all_gather | solution.py:382
  7.7 22.9 %collective-permute-start.2 = (bf16[128,512]{1,0:T(8,128)(2,1)S(1)}, bf16[128,512]{1,0:T(8,128)(2,1)S(1)}, u32[]{:S(2)}, u32[]{:S(2)}) collective-permute-start(bf16[128,512]{1,0:T(8,128)(2,1)S(1)} %get-tuple-element.37), channel_id=1, source_target_pairs={{0,252},{4,248},{8,244},{12,240},{16,236},{20,232},{24,228},{28,22... | collective-permute-start | bytes 393224 | tf_op jit(solution)/shard_map/ppermute | solution.py:376
  30.6 74.0 %collective-permute-start = (bf16[768,2048]{1,0:T(8,128)(2,1)}, bf16[768,2048]{1,0:T(8,128)(2,1)}, u32[]{:S(2)}, u32[]{:S(2)}) collective-permute-start(bf16[768,2048]{1,0:T(8,128)(2,1)} %bitcast.59), channel_id=1, source_target_pairs={{0,1},{1,2},{2,3},{3,0},{4,5},{5,6},{6,7},{7,4},{8,9},{9,10},{10,1... | collective-permute-start | bytes 9437192 | tf_op jit(solution)/shard_map/ppermute | solution.py:378
  31.1 73.4 %collective-permute-start.1 = (bf16[768,2048]{1,0:T(8,128)(2,1)}, bf16[768,2048]{1,0:T(8,128)(2,1)}, u32[]{:S(2)}, u32[]{:S(2)}) collective-permute-start(bf16[768,2048]{1,0:T(8,128)(2,1)} %bitcast.60), channel_id=1, source_target_pairs={{0,3},{1,0},{2,1},{3,2},{4,7},{5,4},{6,5},{7,6},{8,11},{9,8},{10,9... | collective-permute-start | bytes 9437192 | tf_op jit(solution)/shard_map/ppermute | solution.py:379
  71.0 9.7 %collective-permute-start.3 = (bf16[32,160,256]{2,1,0:T(8,128)(2,1)}, bf16[32,160,256]{2,1,0:T(8,128)(2,1)}, u32[]{:S(2)}, u32[]{:S(2)}) collective-permute-start(bf16[32,160,256]{2,1,0:T(8,128)(2,1)} %all-gather.4.cloned.1.call-done.own_ref), channel_id=1, source_target_pairs={{0,4},{4,0},{1,5},{5,1},{2,6},{6,2},{3,7},{7,3},{8,12},{12,8},{9,1... | collective-permute-start | bytes 7864328 | tf_op jit(solution)/shard_map/ppermute | solution.py:386
  71.0 33.6 %collective-permute-start.4 = (bf16[64,2048]{1,0:T(8,128)(2,1)}, bf16[64,2048]{1,0:T(8,128)(2,1)}, u32[]{:S(2)}, u32[]{:S(2)}) collective-permute-start(bf16[64,2048]{1,0:T(8,128)(2,1)} %param.14), channel_id=1, source_target_pairs={{0,0},{1,1},{2,254},{3,255},{4,4},{5,5},{6,250},{7,251},{8,8},{9,9... | collective-permute-start | bytes 786440 | tf_op jit(solution)/shard_map/ppermute | solution.py:384
  78.1 26.5 %collective-permute-start.5 = (s32[64,2]{1,0:T(8,128)S(1)}, s32[64,2]{1,0:T(8,128)S(1)}, u32[]{:S(2)}, u32[]{:S(2)}) collective-permute-start(s32[64,2]{1,0:T(8,128)S(1)} %copy.15), channel_id=1, source_target_pairs={{0,0},{1,1},{2,254},{3,255},{4,4},{5,5},{6,250},{7,251},{8,8},{9,9... | collective-permute-start | bytes 1544 | tf_op jit(solution)/shard_map/ppermute | solution.py:385
  80.7 1.7 copy-start.1
  82.4 22.2 %copy-start.3 = (bf16[512,2048]{1,0:T(8,128)(2,1)S(1)}, bf16[512,2048]{1,0:T(8,128)(2,1)}, u32[]{:S(2)}) copy-start(bf16[512,2048]{1,0:T(8,128)(2,1)} %param.15) | copy-start | bytes 6291460
  106.5 18.6 %all-to-all-start = ((bf16[4,64,2048]{2,1,0:T(8,128)(2,1)}), bf16[4,64,2048]{2,1,0:T(8,128)(2,1)}, u32[]{:S(2)}, u32[]{:S(2)}) async-start(bf16[4,64,2048]{2,1,0:T(8,128)(2,1)} %bitcast.55), calls=%async_computation | async-start | bytes 2097152 | tf_op jit(solution)/shard_map/all_to_all | solution.py:399
  128.3 52.3 %all-to-all-start.1 = ((bf16[64,48,128]{2,1,0:T(8,128)(2,1)}), bf16[64,48,128]{2,1,0:T(8,128)(2,1)}, u32[]{:S(2)}, u32[]{:S(2)}) async-start(bf16[64,48,128]{2,1,0:T(8,128)(2,1)} %get-tuple-element.29), calls=%async_computation.1 | async-start | bytes 1572864 | tf_op jit(solution)/shard_map/all_to_all | solution.py:413
  164.2 85.2 %collective-permute-start.14 = (bf16[384,2048]{1,0:T(8,128)(2,1)}, bf16[384,2048]{1,0:T(8,128)(2,1)}, u32[]{:S(2)}, u32[]{:S(2)}) collective-permute-start(bf16[384,2048]{1,0:T(8,128)(2,1)} %slice.22), channel_id=1, source_target_pairs={{0,1},{1,2},{2,3},{3,0},{4,5},{5,6},{6,7},{7,4},{8,9},{9,10},{10,1... | collective-permute-start | bytes 4718600 | tf_op jit(solution)/shard_map/ppermute | solution.py:394
  167.0 82.4 %collective-permute-start.15 = (bf16[384,2048]{1,0:T(8,128)(2,1)}, bf16[384,2048]{1,0:T(8,128)(2,1)}, u32[]{:S(2)}, u32[]{:S(2)}) collective-permute-start(bf16[384,2048]{1,0:T(8,128)(2,1)} %slice.23), channel_id=1, source_target_pairs={{0,3},{1,0},{2,1},{3,2},{4,7},{5,4},{6,5},{7,6},{8,11},{9,8},{10,9... | collective-permute-start | bytes 4718600 | tf_op jit(solution)/shard_map/ppermute | solution.py:395
  183.2 38.6 %collective-permute-start.6 = (bf16[192,2048]{1,0:T(8,128)(2,1)}, bf16[192,2048]{1,0:T(8,128)(2,1)}, u32[]{:S(2)}, u32[]{:S(2)}) collective-permute-start(bf16[192,2048]{1,0:T(8,128)(2,1)} %arrange.1), channel_id=1, source_target_pairs={{0,3},{1,0},{2,1},{3,2},{4,7},{5,4},{6,5},{7,6},{8,11},{9,8},{10,9... | collective-permute-start | bytes 2359304 | tf_op jit(solution)/shard_map/ppermute | solution.py:361
  183.2 34.6 %collective-permute-start.8 = (bf16[192,2048]{1,0:T(8,128)(2,1)}, bf16[192,2048]{1,0:T(8,128)(2,1)}, u32[]{:S(2)}, u32[]{:S(2)}) collective-permute-start(bf16[192,2048]{1,0:T(8,128)(2,1)} %arrange.1), channel_id=1, source_target_pairs={{0,1},{1,2},{2,3},{3,0},{4,5},{5,6},{6,7},{7,4},{8,9},{9,10},{10,1... | collective-permute-start | bytes 2359304 | tf_op jit(solution)/shard_map/ppermute | solution.py:361
  187.1 48.0 %collective-permute-start.12 = (f32[64,2048]{1,0:T(8,128)}, f32[64,2048]{1,0:T(8,128)}, u32[]{:S(2)}, u32[]{:S(2)}) collective-permute-start(f32[64,2048]{1,0:T(8,128)} %get-tuple-element.34), channel_id=1, source_target_pairs={{0,0},{1,1},{2,254},{3,255},{4,4},{5,5},{6,250},{7,251},{8,8},{9,9... | collective-permute-start | bytes 1572872 | tf_op jit(solution)/shard_map/ppermute | solution.py:417
  200.3 26.1 %copy-start.2 = (bf16[1,2048,768]{2,1,0:T(8,128)(2,1)S(1)}, bf16[1,2048,768]{2,1,0:T(8,128)(2,1)}, u32[]{:S(2)}) copy-start(bf16[1,2048,768]{2,1,0:T(8,128)(2,1)} %param.19) | copy-start | bytes 9437188
  218.8 13.3 %collective-permute-start.10 = (bf16[96,2048]{1,0:T(8,128)(2,1)S(1)}, bf16[96,2048]{1,0:T(8,128)(2,1)S(1)}, u32[]{:S(2)}, u32[]{:S(2)}) collective-permute-start(bf16[96,2048]{1,0:T(8,128)(2,1)S(1)} %slice.24), channel_id=1, source_target_pairs={{0,1},{1,2},{2,3},{3,0},{4,5},{5,6},{6,7},{7,4},{8,9},{9,10},{10,1... | collective-permute-start | bytes 1179656 | tf_op jit(solution)/shard_map/ppermute | solution.py:366
  222.8 12.1 %collective-permute-start.11 = (bf16[96,2048]{1,0:T(8,128)(2,1)S(1)}, bf16[96,2048]{1,0:T(8,128)(2,1)S(1)}, u32[]{:S(2)}, u32[]{:S(2)}) collective-permute-start(bf16[96,2048]{1,0:T(8,128)(2,1)S(1)} %slice.25), channel_id=1, source_target_pairs={{0,3},{1,0},{2,1},{3,2},{4,7},{5,4},{6,5},{7,6},{8,11},{9,8},{10,9... | collective-permute-start | bytes 1179656 | tf_op jit(solution)/shard_map/ppermute | solution.py:366
  232.2 14.5 %collective-permute-start.7 = (bf16[192,768]{1,0:T(8,128)(2,1)S(1)}, bf16[192,768]{1,0:T(8,128)(2,1)S(1)}, u32[]{:S(2)}, u32[]{:S(2)}) collective-permute-start(bf16[192,768]{1,0:T(8,128)(2,1)S(1)} %multiply_convert_fusion.2), channel_id=1, source_target_pairs={{0,1},{1,2},{2,3},{3,0},{4,5},{5,6},{6,7},{7,4},{8,9},{9,10},{10,1... | collective-permute-start | bytes 884744 | tf_op jit(solution)/shard_map/ppermute | solution.py:429
  235.0 17.2 %collective-permute-start.9 = (bf16[192,768]{1,0:T(8,128)(2,1)S(1)}, bf16[192,768]{1,0:T(8,128)(2,1)S(1)}, u32[]{:S(2)}, u32[]{:S(2)}) collective-permute-start(bf16[192,768]{1,0:T(8,128)(2,1)S(1)} %multiply_convert_fusion.1), channel_id=1, source_target_pairs={{0,3},{1,0},{2,1},{3,2},{4,7},{5,4},{6,5},{7,6},{8,11},{9,8},{10,9... | collective-permute-start | bytes 884744 | tf_op jit(solution)/shard_map/ppermute | solution.py:430
  235.8 10.8 %copy-start.4 = (f32[192,2048]{1,0:T(8,128)S(1)}, f32[192,2048]{1,0:T(8,128)}, u32[]{:S(2)}) copy-start(f32[192,2048]{1,0:T(8,128)} %fusion.28) | copy-start | bytes 4718596
  236.7 12.8 %collective-permute-start.13 = (bf16[192,768]{1,0:T(8,128)(2,1)S(1)}, bf16[192,768]{1,0:T(8,128)(2,1)S(1)}, u32[]{:S(2)}, u32[]{:S(2)}) collective-permute-start(bf16[192,768]{1,0:T(8,128)(2,1)S(1)} %multiply_convert_fusion), channel_id=1, source_target_pairs={{0,2},{1,3},{2,0},{3,1},{4,6},{5,7},{6,4},{7,5},{8,10},{9,11},{10,... | collective-permute-start | bytes 884744 | tf_op jit(solution)/shard_map/ppermute | solution.py:432
  256.1 12.7 %copy-start.5 = (s32[64,2]{0,1:T(2,128)S(1)}, s32[64,2]{0,1:T(2,128)}, u32[]{:S(2)}) copy-start(s32[64,2]{0,1:T(2,128)} %param.17) | copy-start | bytes 1540
  256.1 13.4 %copy-start.6 = (f32[64,2]{0,1:T(2,128)S(1)}, f32[64,2]{0,1:T(2,128)}, u32[]{:S(2)}) copy-start(f32[64,2]{0,1:T(2,128)} %param.18) | copy-start | bytes 1540
  259.0 32.9 %all-to-all-start.2 = ((bf16[64,48,128]{2,1,0:T(8,128)(2,1)}), bf16[64,48,128]{2,1,0:T(8,128)(2,1)}, u32[]{:S(2)}, u32[]{:S(2)}) async-start(bf16[64,48,128]{2,1,0:T(8,128)(2,1)} %spread.1), calls=%async_computation.2 | async-start | bytes 1572864 | tf_op jit(solution)/shard_map/all_to_all | solution.py:440
Sparse Core Ops, SparseCore 0:
  30.7 40.2 all-gather.3

commit v8 on v7

--- a/solution.py
+++ b/solution.py
@@ -377,18 +377,18 @@
     down_own = expert_down[0]
     down_before = lax.ppermute(down_own, "tp", up)
     down_after = lax.ppermute(down_own, "tp", down)
+    held_residual = lax.ppermute(residual_in, SP_TP, whole)
+    held_routes = lax.ppermute(routes, SP_TP, whole)
     near = lax.all_gather(block, "sp_1")
     near, mirrored_queries = lax.optimization_barrier((near, mirrored_queries))
     own = lax.all_gather(near, "sp_0").reshape(-1, *block.shape)
-    own, swapped_residual, swapped_routes = lax.optimization_barrier((own, residual_in, routes))
-    held_residual = lax.ppermute(swapped_residual, SP_TP, whole)
-    held_routes = lax.ppermute(swapped_routes, SP_TP, whole)
+    own, held_residual, held_routes = lax.optimization_barrier((own, held_residual, held_routes))
     other = lax.ppermute(own, "sp_2", [(0, 1), (1, 0)])
     attended = attend_rows(
         index.reshape(1), queries[:HALF], mirrored_queries, own, other
     )
-    down_before, down_after, attended, held_residual, held_routes = lax.optimization_barrier(
-        (down_before, down_after, attended, held_residual, held_routes)
+    down_before, down_after, attended = lax.optimization_barrier(
+        (down_before, down_after, attended)
     )
     half = down_own.shape[0] // 2
     across_low = lax.ppermute(down_before[:half], "tp", up)

time: 307 us -> 306 us (level)
  starting transfers between devices: 83.6 us -> 80.5 us
    all_gather x1, waiting for transfers between devices: 38.3 us -> 20.3 us  [layer(): own = lax.all_gather(near, 'sp_0').reshape(-1, *block.shape)]
    ppermute x2, waiting for transfers between devices: 0.01 us -> 15.3 us  [the longest x1 15.3 us: layer(): held_routes = lax.ppermute(routes, SP_TP, whole)]
    ppermute x1, waiting for transfers between devices: 0.01 us -> 5.25 us  [layer(): other = lax.ppermute(own, 'sp_2', [(0, 1), (1, 0)])]
    all_to_all x1, starting transfers between devices: 33.1 us -> 30 us  [layer(): lax.all_to_all(slots, SP_TP, 0, 0, axis_index_groups=ranks, tiled=True)]
  transfers between devices with their start and end apart: 20 -> 20, of which waited for: 7 -> 9; matrix products, arithmetic and copies ran while one was open for 12% -> 11% of each run, Pallas kernels for 9% -> 9%
where the time goes in v8:
time: 306 us; the launch traced here: 301 us
  waiting for transfers between devices  115 us (38%)
  starting transfers between devices  80.5 us (26%)
  Pallas kernels  35.7 us (12%)
  matrix products  30.4 us (10%)
  between operations  13.6 us (4%)
  blocking collectives  13.5 us (4%)
  local copies, waits for them, and re-layouts  11.9 us (4%)
    all_to_all x1, starting transfers between devices, layer(): lax.all_to_all(slots, SP_TP, 0, 0, axis_index_groups=ranks, tiled=True)  30 us
    all_to_all x1, waiting for transfers between devices, layer(): returned = lax.all_to_all(spread(summed, capacity), SP, 0, 0, tiled=True)  22.4 us
    pallas_call x1, Pallas kernels, attend_rows(): pl.pallas_call(functools.partial(attend_body, blocks=blocks, heads=heads)...  22.2 us
    all_gather x1, waiting for transfers between devices, layer(): own = lax.all_gather(near, 'sp_0').reshape(-1, *block.shape)  20.3 us
    ppermute x2, waiting for transfers between devices, neighbours(): return (lax.ppermute(array, 'tp', up), lax.ppermute(array, 'tp', down))  18.9 us
    ppermute x1, waiting for transfers between devices, layer(): held_routes = lax.ppermute(routes, SP_TP, whole)  15.3 us
    all_gather x1, blocking collectives, layer(): near = lax.all_gather(block, 'sp_1')  13.5 us
    all_to_all x1, waiting for transfers between devices, layer(): lax.all_to_all(partial.reshape(head_devices, -1, partial.shape[1]), 'tp',...  12.8 us
  transfers between devices with their start and end apart: 20, of which 9 were waited for; matrix products, arithmetic and copies ran while one was open for 11% of the time, Pallas kernels for 9%

profile of v8, /device:TPU:6, one launch (start us, length us, event | category | flops | bytes accessed | tf_op | source)
XLA Modules:
  0.0 301.1 jit_solution(701374753045594226)
XLA Ops:
  6.5 1.1 fusion.39
  7.7 7.8 %collective-permute-start.2 = (bf16[128,512]{1,0:T(8,128)(2,1)S(1)}, bf16[128,512]{1,0:T(8,128)(2,1)S(1)}, u32[]{:S(2)}, u32[]{:S(2)}) collective-permute-start(bf16[128,512]{1,0:T(8,128)(2,1)S(1)} %get-tuple-element.33), channel_id=1, source_target_pairs={{0,252},{4,248},{8,244},{12,240},{16,236},{20,232},{24,228},{28,22... | collective-permute-start | bytes 393224 | tf_op jit(solution)/shard_map/ppermute | solution.py:376
  15.5 1.6 prepare_keys.1
  17.1 13.5 %all-gather = bf16[640,256]{1,0:T(8,128)(2,1)} all-gather(bf16[160,256]{1,0:T(8,128)(2,1)} %prepare_keys.1), channel_id=2, replica_groups=mesh['sp_0'=8,'sp_1'=4,'sp_2'=2,'tp'=4] {'sp_1'}, dimensions={0}, use_global_device_ids=true | all-gather | bytes 409600 | tf_op jit(solution)/shard_map/all_gather | solution.py:382
  31.1 1.5 collective-permute-start.1
  32.7 1.9 collective-permute-start.3
  34.6 0.8 copy.15.routes_ref
  35.4 7.0 %collective-permute-start.4 = (s32[64,2]{1,0:T(8,128)S(1)}, s32[64,2]{1,0:T(8,128)S(1)}, u32[]{:S(2)}, u32[]{:S(2)}) collective-permute-start(s32[64,2]{1,0:T(8,128)S(1)} %copy.15.routes_ref), channel_id=1, source_target_pairs={{0,0},{1,1},{2,254},{3,255},{4,4},{5,5},{6,250},{7,251},{8,8},{9,9... | collective-permute-start | bytes 1544 | tf_op jit(solution)/shard_map/ppermute | solution.py:381
  42.4 15.3 %collective-permute-done.4 = s32[64,2]{1,0:T(8,128)S(1)} collective-permute-done((s32[64,2]{1,0:T(8,128)S(1)}, s32[64,2]{1,0:T(8,128)S(1)}, u32[]{:S(2)}, u32[]{:S(2)}) %collective-permute-start.4) | collective-permute-done | bytes 544 | tf_op jit(solution)/shard_map/ppermute | solution.py:381
  57.7 20.3 %all-gather.4.cloned.1.call-done.own_ref = bf16[32,160,256]{2,1,0:T(8,128)(2,1)} async-done(((bf16[4,160,256]{2,1,0:T(8,128)(2,1)}), bf16[32,160,256]{2,1,0:T(8,128)(2,1)}) %all-gather.4.cloned.1.call-update) | async-done | bytes 2621456 | tf_op jit(solution)/shard_map/all_gather | solution.py:384
  78.0 5.2 %collective-permute-done.5.other_ref = bf16[32,160,256]{2,1,0:T(8,128)(2,1)} collective-permute-done((bf16[32,160,256]{2,1,0:T(8,128)(2,1)}, bf16[32,160,256]{2,1,0:T(8,128)(2,1)}, u32[]{:S(2)}, u32[]{:S(2)}) %collective-permute-start.5) | collective-permute-done | bytes 2621472 | tf_op jit(solution)/shard_map/ppermute | solution.py:386
  83.2 1.7 copy-done.1
  85.0 22.2 %attend_rows.1 = bf16[2,128,512]{2,1,0:T(8,128)(2,1)S(1)} custom-call(s32[1]{0:T(128)} %bitcast.1.index_ref, bf16[128,512]{1,0:T(8,128)(2,1)S(1)} %get-tuple-element.34.qa_ref, bf16[128,512]{1,0:T(8,128)(2,1)S(1)} %collective-permute-done.2.qb_ref, bf16[32,160,256]{2,1,0:T(8,128)(2,1)S(1)} %copy-done.1, bf16[32,160,256]{2,1,0:T(8,128)(2,1)} %collective-permute-done.5.other_ref), custom_call_target="tpu_custom_call" | custom-call | tf_op jit(solution)/shard_map/attend_rows/pallas_call | solution.py:196
  107.1 1.8 convolution_convert_fusion
  109.0 4.8 %all-to-all-start = ((bf16[4,64,2048]{2,1,0:T(8,128)(2,1)}), bf16[4,64,2048]{2,1,0:T(8,128)(2,1)}, u32[]{:S(2)}, u32[]{:S(2)}) async-start(bf16[4,64,2048]{2,1,0:T(8,128)(2,1)} %bitcast.55), calls=%async_computation | async-start | bytes 2097152 | tf_op jit(solution)/shard_map/all_to_all | solution.py:399
  114.4 12.8 %all-to-all-done.parts_ref = bf16[4,64,2048]{2,1,0:T(8,128)(2,1)} async-done(((bf16[4,64,2048]{2,1,0:T(8,128)(2,1)}), bf16[4,64,2048]{2,1,0:T(8,128)(2,1)}, u32[]{:S(2)}, u32[]{:S(2)}) %all-to-all-start) | async-done | bytes 1048608 | tf_op jit(solution)/shard_map/all_to_all | solution.py:399
  127.3 3.3 %dispatch.1 = (f32[64,2048]{1,0:T(8,128)}, bf16[64,48,128]{2,1,0:T(8,128)(2,1)}) custom-call(bf16[4,64,2048]{2,1,0:T(8,128)(2,1)} %all-to-all-done.parts_ref, bf16[64,2048]{1,0:T(8,128)(2,1)} %collective-permute-done.3.residual_ref, f32[1,2048]{1,0:T(1,128)} %bitcast.57, s32[64,2]{1,0:T(8,128)} %subtract_select_fusion.routes_ref), custom_call_target="tpu_custom_call" | custom-call | tf_op jit(solution)/shard_map/dispatch/pallas_call | solution.py:266
  130.5 30.0 %all-to-all-start.1 = ((bf16[64,48,128]{2,1,0:T(8,128)(2,1)}), bf16[64,48,128]{2,1,0:T(8,128)(2,1)}, u32[]{:S(2)}, u32[]{:S(2)}) async-start(bf16[64,48,128]{2,1,0:T(8,128)(2,1)} %get-tuple-element.25), calls=%async_computation.1 | async-start | bytes 1572864 | tf_op jit(solution)/shard_map/all_to_all | solution.py:413
  160.6 2.7 slice.22
  163.3 2.8 slice.23
  166.1 2.0 collective-permute-start.15
  168.1 11.6 %all-to-all-done.1.arrived_ref = bf16[64,48,128]{2,1,0:T(8,128)(2,1)} async-done(((bf16[64,48,128]{2,1,0:T(8,128)(2,1)}), bf16[64,48,128]{2,1,0:T(8,128)(2,1)}, u32[]{:S(2)}, u32[]{:S(2)}) %all-to-all-start.1) | async-done | bytes 786464 | tf_op jit(solution)/shard_map/all_to_all | solution.py:413
  179.7 2.6 arrange.1
  182.3 3.9 %collective-permute-start.8 = (bf16[192,2048]{1,0:T(8,128)(2,1)}, bf16[192,2048]{1,0:T(8,128)(2,1)}, u32[]{:S(2)}, u32[]{:S(2)}) collective-permute-start(bf16[192,2048]{1,0:T(8,128)(2,1)} %arrange.1), channel_id=1, source_target_pairs={{0,1},{1,2},{2,3},{3,0},{4,5},{5,6},{6,7},{7,4},{8,9},{9,10},{10,1... | collective-permute-start | bytes 2359304 | tf_op jit(solution)/shard_map/ppermute | solution.py:361
  186.2 4.3 %collective-permute-start.12 = (f32[64,2048]{1,0:T(8,128)}, f32[64,2048]{1,0:T(8,128)}, u32[]{:S(2)}, u32[]{:S(2)}) collective-permute-start(f32[64,2048]{1,0:T(8,128)} %get-tuple-element.30), channel_id=1, source_target_pairs={{0,0},{1,1},{2,254},{3,255},{4,4},{5,5},{6,250},{7,251},{8,8},{9,9... | collective-permute-start | bytes 1572872 | tf_op jit(solution)/shard_map/ppermute | solution.py:417
  190.5 3.8 %fusion.18 = f32[192,768]{1,0:T(8,128)} fusion(bf16[192,2048]{1,0:T(8,128)(2,1)} %arrange.1, bf16[1,2048,768]{2,1,0:T(8,128)(2,1)} %param.19), kind=kOutput, calls=%fused_computation.18 | convolution fusion | flops 603979776 | bytes 4521984 | tf_op jit(solution)/shard_map/dot_general | solution.py:421
  194.2 5.1 %fusion.28 = f32[192,2048]{1,0:T(8,128)} fusion(bf16[192,2048]{1,0:T(8,128)(2,1)} %arrange.1, bf16[1,2048,768]{2,1,0:T(8,128)(2,1)S(1)} %copy-done, f32[192,768]{1,0:T(8,128)} %fusion.18, bf16[1,768,2048]{2,1,0:T(8,128)(2,1)} %param.21), kind=kOutput, calls=%fused_computation.26 | convolution fusion | flops 1208844288 | bytes 9240576 | tf_op jit(solution)/shard_map/dot_general | solution.py:433
  199.4 17.5 %collective-permute-done.8 = bf16[192,2048]{1,0:T(8,128)(2,1)} collective-permute-done((bf16[192,2048]{1,0:T(8,128)(2,1)}, bf16[192,2048]{1,0:T(8,128)(2,1)}, u32[]{:S(2)}, u32[]{:S(2)}) %collective-permute-start.8) | collective-permute-done | bytes 786464 | tf_op jit(solution)/shard_map/ppermute | solution.py:361
  216.9 1.0 slice.24
  217.9 1.6 collective-permute-start.10
  219.5 1.4 collective-permute-done.6
  220.9 1.0 slice.25
  222.5 2.9 fusion.16
  225.4 1.9 fusion.14
  227.4 1.9 multiply_convert_fusion.2
  229.3 1.9 multiply_convert_fusion.1
  231.2 2.8 collective-permute-start.7
  234.1 0.8 fusion.12
  234.9 0.8 multiply_convert_fusion
  235.7 1.9 collective-permute-start.13
  237.6 8.2 %collective-permute-done.7 = bf16[192,768]{1,0:T(8,128)(2,1)S(1)} collective-permute-done((bf16[192,768]{1,0:T(8,128)(2,1)S(1)}, bf16[192,768]{1,0:T(8,128)(2,1)S(1)}, u32[]{:S(2)}, u32[]{:S(2)}) %collective-permute-start.7) | collective-permute-done | bytes 294944 | tf_op jit(solution)/shard_map/ppermute | solution.py:429
  245.7 2.7 convolution_add_fusion.1
  248.5 2.7 fusion
  251.2 4.0 %fusion.20.rows_ref = f32[192,2048]{1,0:T(8,128)} fusion(f32[192,2048]{1,0:T(8,128)S(1)} %fusion, f32[192,2048]{1,0:T(8,128)S(1)} %convolution_add_fusion.1, bf16[192,768]{1,0:T(8,128)(2,1)S(1)} %collective-permute-done.9, bf16[768,2048]{1,0:T(8,128)(2,1)} %collective-permute-done.1), kind=kOutput, calls=%fused_computation.21 | convolution fusion | flops 604766208 | bytes 8159232 | tf_op jit(solution)/shard_map/dot_general | solution.py:439
  255.2 2.9 spread.1
  258.1 9.8 %all-to-all-start.2 = ((bf16[64,48,128]{2,1,0:T(8,128)(2,1)}), bf16[64,48,128]{2,1,0:T(8,128)(2,1)}, u32[]{:S(2)}, u32[]{:S(2)}) async-start(bf16[64,48,128]{2,1,0:T(8,128)(2,1)} %spread.1), calls=%async_computation.2 | async-start | bytes 1572864 | tf_op jit(solution)/shard_map/all_to_all | solution.py:440
  268.6 22.4 %all-to-all-done.2.returned_ref = bf16[64,48,128]{2,1,0:T(8,128)(2,1)} async-done(((bf16[64,48,128]{2,1,0:T(8,128)(2,1)}), bf16[64,48,128]{2,1,0:T(8,128)(2,1)}, u32[]{:S(2)}, u32[]{:S(2)}) %all-to-all-start.2) | async-done | bytes 786464 | tf_op jit(solution)/shard_map/all_to_all | solution.py:440
  291.0 3.2 %combine.1 = bf16[64,2048]{1,0:T(8,128)(2,1)} custom-call(bf16[64,48,128]{2,1,0:T(8,128)(2,1)} %all-to-all-done.2.returned_ref, f32[64,2048]{1,0:T(8,128)} %collective-permute-done.12.hidden_ref, s32[64,2]{1,0:T(8,128)} %copy-done.5, f32[64,2]{1,0:T(8,128)} %copy.17.weight_ref), custom_call_target="tpu_custom_call" | custom-call | tf_op jit(solution)/shard_map/combine/pallas_call | solution.py:332
  (35 shorter events, 2.6 us)
Async XLA Ops:
  6.5 187.7 %copy-start = (bf16[1,2048,768]{2,1,0:T(8,128)(2,1)S(1)}, bf16[1,2048,768]{2,1,0:T(8,128)(2,1)}, u32[]{:S(2)}) copy-start(bf16[1,2048,768]{2,1,0:T(8,128)(2,1)} %param.20) | copy-start | bytes 9437188
  6.5 71.4 %all-gather.4.cloned.1.call-start = ((), (), s32[]{:S(2)}) async-start(), calls=%async_computation.3 | async-start | bytes 2949120 | tf_op jit(solution)/shard_map/all_gather | solution.py:384
  7.7 22.9 %collective-permute-start.2 = (bf16[128,512]{1,0:T(8,128)(2,1)S(1)}, bf16[128,512]{1,0:T(8,128)(2,1)S(1)}, u32[]{:S(2)}, u32[]{:S(2)}) collective-permute-start(bf16[128,512]{1,0:T(8,128)(2,1)S(1)} %get-tuple-element.33), channel_id=1, source_target_pairs={{0,252},{4,248},{8,244},{12,240},{16,236},{20,232},{24,228},{28,22... | collective-permute-start | bytes 393224 | tf_op jit(solution)/shard_map/ppermute | solution.py:376
  30.6 76.5 %collective-permute-start = (bf16[768,2048]{1,0:T(8,128)(2,1)}, bf16[768,2048]{1,0:T(8,128)(2,1)}, u32[]{:S(2)}, u32[]{:S(2)}) collective-permute-start(bf16[768,2048]{1,0:T(8,128)(2,1)} %bitcast.59), channel_id=1, source_target_pairs={{0,1},{1,2},{2,3},{3,0},{4,5},{5,6},{6,7},{7,4},{8,9},{9,10},{10,1... | collective-permute-start | bytes 9437192 | tf_op jit(solution)/shard_map/ppermute | solution.py:378
  31.1 76.0 %collective-permute-start.1 = (bf16[768,2048]{1,0:T(8,128)(2,1)}, bf16[768,2048]{1,0:T(8,128)(2,1)}, u32[]{:S(2)}, u32[]{:S(2)}) collective-permute-start(bf16[768,2048]{1,0:T(8,128)(2,1)} %bitcast.60), channel_id=1, source_target_pairs={{0,3},{1,0},{2,1},{3,2},{4,7},{5,4},{6,5},{7,6},{8,11},{9,8},{10,9... | collective-permute-start | bytes 9437192 | tf_op jit(solution)/shard_map/ppermute | solution.py:379
  32.7 25.0 %collective-permute-start.3 = (bf16[64,2048]{1,0:T(8,128)(2,1)}, bf16[64,2048]{1,0:T(8,128)(2,1)}, u32[]{:S(2)}, u32[]{:S(2)}) collective-permute-start(bf16[64,2048]{1,0:T(8,128)(2,1)} %param.14), channel_id=1, source_target_pairs={{0,0},{1,1},{2,254},{3,255},{4,4},{5,5},{6,250},{7,251},{8,8},{9,9... | collective-permute-start | bytes 786440 | tf_op jit(solution)/shard_map/ppermute | solution.py:380
  35.4 73.6 %copy-start.5 = (s32[64,2]{1,0:T(8,128)}, s32[64,2]{1,0:T(8,128)S(1)}, u32[]{:S(2)}) copy-start(s32[64,2]{1,0:T(8,128)S(1)} %copy.15.routes_ref) | copy-start | bytes 1540
  35.4 22.3 %collective-permute-start.4 = (s32[64,2]{1,0:T(8,128)S(1)}, s32[64,2]{1,0:T(8,128)S(1)}, u32[]{:S(2)}, u32[]{:S(2)}) collective-permute-start(s32[64,2]{1,0:T(8,128)S(1)} %copy.15.routes_ref), channel_id=1, source_target_pairs={{0,0},{1,1},{2,254},{3,255},{4,4},{5,5},{6,250},{7,251},{8,8},{9,9... | collective-permute-start | bytes 1544 | tf_op jit(solution)/shard_map/ppermute | solution.py:381
  78.0 5.3 %collective-permute-start.5 = (bf16[32,160,256]{2,1,0:T(8,128)(2,1)}, bf16[32,160,256]{2,1,0:T(8,128)(2,1)}, u32[]{:S(2)}, u32[]{:S(2)}) collective-permute-start(bf16[32,160,256]{2,1,0:T(8,128)(2,1)} %all-gather.4.cloned.1.call-done.own_ref), channel_id=1, source_target_pairs={{0,4},{4,0},{1,5},{5,1},{2,6},{6,2},{3,7},{7,3},{8,12},{12,8},{9,1... | collective-permute-start | bytes 7864328 | tf_op jit(solution)/shard_map/ppermute | solution.py:386
  83.2 1.7 copy-start.1
  85.0 22.2 %copy-start.3 = (bf16[512,2048]{1,0:T(8,128)(2,1)S(1)}, bf16[512,2048]{1,0:T(8,128)(2,1)}, u32[]{:S(2)}) copy-start(bf16[512,2048]{1,0:T(8,128)(2,1)} %param.15) | copy-start | bytes 6291460
  109.0 18.3 %all-to-all-start = ((bf16[4,64,2048]{2,1,0:T(8,128)(2,1)}), bf16[4,64,2048]{2,1,0:T(8,128)(2,1)}, u32[]{:S(2)}, u32[]{:S(2)}) async-start(bf16[4,64,2048]{2,1,0:T(8,128)(2,1)} %bitcast.55), calls=%async_computation | async-start | bytes 2097152 | tf_op jit(solution)/shard_map/all_to_all | solution.py:399
  130.5 49.1 %all-to-all-start.1 = ((bf16[64,48,128]{2,1,0:T(8,128)(2,1)}), bf16[64,48,128]{2,1,0:T(8,128)(2,1)}, u32[]{:S(2)}, u32[]{:S(2)}) async-start(bf16[64,48,128]{2,1,0:T(8,128)(2,1)} %get-tuple-element.25), calls=%async_computation.1 | async-start | bytes 1572864 | tf_op jit(solution)/shard_map/all_to_all | solution.py:413
  163.3 85.2 %collective-permute-start.14 = (bf16[384,2048]{1,0:T(8,128)(2,1)}, bf16[384,2048]{1,0:T(8,128)(2,1)}, u32[]{:S(2)}, u32[]{:S(2)}) collective-permute-start(bf16[384,2048]{1,0:T(8,128)(2,1)} %slice.22), channel_id=1, source_target_pairs={{0,1},{1,2},{2,3},{3,0},{4,5},{5,6},{6,7},{7,4},{8,9},{9,10},{10,1... | collective-permute-start | bytes 4718600 | tf_op jit(solution)/shard_map/ppermute | solution.py:394
  166.1 82.4 %collective-permute-start.15 = (bf16[384,2048]{1,0:T(8,128)(2,1)}, bf16[384,2048]{1,0:T(8,128)(2,1)}, u32[]{:S(2)}, u32[]{:S(2)}) collective-permute-start(bf16[384,2048]{1,0:T(8,128)(2,1)} %slice.23), channel_id=1, source_target_pairs={{0,3},{1,0},{2,1},{3,2},{4,7},{5,4},{6,5},{7,6},{8,11},{9,8},{10,9... | collective-permute-start | bytes 4718600 | tf_op jit(solution)/shard_map/ppermute | solution.py:395
  182.3 38.6 %collective-permute-start.6 = (bf16[192,2048]{1,0:T(8,128)(2,1)}, bf16[192,2048]{1,0:T(8,128)(2,1)}, u32[]{:S(2)}, u32[]{:S(2)}) collective-permute-start(bf16[192,2048]{1,0:T(8,128)(2,1)} %arrange.1), channel_id=1, source_target_pairs={{0,3},{1,0},{2,1},{3,2},{4,7},{5,4},{6,5},{7,6},{8,11},{9,8},{10,9... | collective-permute-start | bytes 2359304 | tf_op jit(solution)/shard_map/ppermute | solution.py:361
  182.3 34.6 %collective-permute-start.8 = (bf16[192,2048]{1,0:T(8,128)(2,1)}, bf16[192,2048]{1,0:T(8,128)(2,1)}, u32[]{:S(2)}, u32[]{:S(2)}) collective-permute-start(bf16[192,2048]{1,0:T(8,128)(2,1)} %arrange.1), channel_id=1, source_target_pairs={{0,1},{1,2},{2,3},{3,0},{4,5},{5,6},{6,7},{7,4},{8,9},{9,10},{10,1... | collective-permute-start | bytes 2359304 | tf_op jit(solution)/shard_map/ppermute | solution.py:361
  186.2 48.0 %collective-permute-start.12 = (f32[64,2048]{1,0:T(8,128)}, f32[64,2048]{1,0:T(8,128)}, u32[]{:S(2)}, u32[]{:S(2)}) collective-permute-start(f32[64,2048]{1,0:T(8,128)} %get-tuple-element.30), channel_id=1, source_target_pairs={{0,0},{1,1},{2,254},{3,255},{4,4},{5,5},{6,250},{7,251},{8,8},{9,9... | collective-permute-start | bytes 1572872 | tf_op jit(solution)/shard_map/ppermute | solution.py:417
  199.4 26.1 %copy-start.2 = (bf16[1,2048,768]{2,1,0:T(8,128)(2,1)S(1)}, bf16[1,2048,768]{2,1,0:T(8,128)(2,1)}, u32[]{:S(2)}) copy-start(bf16[1,2048,768]{2,1,0:T(8,128)(2,1)} %param.19) | copy-start | bytes 9437188
  217.9 13.3 %collective-permute-start.10 = (bf16[96,2048]{1,0:T(8,128)(2,1)S(1)}, bf16[96,2048]{1,0:T(8,128)(2,1)S(1)}, u32[]{:S(2)}, u32[]{:S(2)}) collective-permute-start(bf16[96,2048]{1,0:T(8,128)(2,1)S(1)} %slice.24), channel_id=1, source_target_pairs={{0,1},{1,2},{2,3},{3,0},{4,5},{5,6},{6,7},{7,4},{8,9},{9,10},{10,1... | collective-permute-start | bytes 1179656 | tf_op jit(solution)/shard_map/ppermute | solution.py:366
  221.9 12.1 %collective-permute-start.11 = (bf16[96,2048]{1,0:T(8,128)(2,1)S(1)}, bf16[96,2048]{1,0:T(8,128)(2,1)S(1)}, u32[]{:S(2)}, u32[]{:S(2)}) collective-permute-start(bf16[96,2048]{1,0:T(8,128)(2,1)S(1)} %slice.25), channel_id=1, source_target_pairs={{0,3},{1,0},{2,1},{3,2},{4,7},{5,4},{6,5},{7,6},{8,11},{9,8},{10,9... | collective-permute-start | bytes 1179656 | tf_op jit(solution)/shard_map/ppermute | solution.py:366
  231.2 14.5 %collective-permute-start.7 = (bf16[192,768]{1,0:T(8,128)(2,1)S(1)}, bf16[192,768]{1,0:T(8,128)(2,1)S(1)}, u32[]{:S(2)}, u32[]{:S(2)}) collective-permute-start(bf16[192,768]{1,0:T(8,128)(2,1)S(1)} %multiply_convert_fusion.2), channel_id=1, source_target_pairs={{0,1},{1,2},{2,3},{3,0},{4,5},{5,6},{6,7},{7,4},{8,9},{9,10},{10,1... | collective-permute-start | bytes 884744 | tf_op jit(solution)/shard_map/ppermute | solution.py:429
  234.0 17.2 %collective-permute-start.9 = (bf16[192,768]{1,0:T(8,128)(2,1)S(1)}, bf16[192,768]{1,0:T(8,128)(2,1)S(1)}, u32[]{:S(2)}, u32[]{:S(2)}) collective-permute-start(bf16[192,768]{1,0:T(8,128)(2,1)S(1)} %multiply_convert_fusion.1), channel_id=1, source_target_pairs={{0,3},{1,0},{2,1},{3,2},{4,7},{5,4},{6,5},{7,6},{8,11},{9,8},{10,9... | collective-permute-start | bytes 884744 | tf_op jit(solution)/shard_map/ppermute | solution.py:430
  234.9 10.8 %copy-start.4 = (f32[192,2048]{1,0:T(8,128)S(1)}, f32[192,2048]{1,0:T(8,128)}, u32[]{:S(2)}) copy-start(f32[192,2048]{1,0:T(8,128)} %fusion.28) | copy-start | bytes 4718596
  235.7 12.8 %collective-permute-start.13 = (bf16[192,768]{1,0:T(8,128)(2,1)S(1)}, bf16[192,768]{1,0:T(8,128)(2,1)S(1)}, u32[]{:S(2)}, u32[]{:S(2)}) collective-permute-start(bf16[192,768]{1,0:T(8,128)(2,1)S(1)} %multiply_convert_fusion), channel_id=1, source_target_pairs={{0,2},{1,3},{2,0},{3,1},{4,6},{5,7},{6,4},{7,5},{8,10},{9,11},{10,... | collective-permute-start | bytes 884744 | tf_op jit(solution)/shard_map/ppermute | solution.py:432
  255.2 12.7 %copy-start.6 = (f32[64,2]{0,1:T(2,128)S(1)}, f32[64,2]{0,1:T(2,128)}, u32[]{:S(2)}) copy-start(f32[64,2]{0,1:T(2,128)} %param.18) | copy-start | bytes 1540
  258.1 32.9 %all-to-all-start.2 = ((bf16[64,48,128]{2,1,0:T(8,128)(2,1)}), bf16[64,48,128]{2,1,0:T(8,128)(2,1)}, u32[]{:S(2)}, u32[]{:S(2)}) async-start(bf16[64,48,128]{2,1,0:T(8,128)(2,1)} %spread.1), calls=%async_computation.2 | async-start | bytes 1572864 | tf_op jit(solution)/shard_map/all_to_all | solution.py:440
Sparse Core Ops, SparseCore 0:
  30.7 47.2 all-gather.3

commit v9 on v7

--- a/solution.py
+++ b/solution.py
@@ -380,15 +380,15 @@
     near = lax.all_gather(block, "sp_1")
     near, mirrored_queries = lax.optimization_barrier((near, mirrored_queries))
     own = lax.all_gather(near, "sp_0").reshape(-1, *block.shape)
-    own, swapped_residual, swapped_routes = lax.optimization_barrier((own, residual_in, routes))
+    held_routes = lax.ppermute(routes, SP_TP, whole)
+    own, held_routes, swapped_residual = lax.optimization_barrier((own, held_routes, residual_in))
     held_residual = lax.ppermute(swapped_residual, SP_TP, whole)
-    held_routes = lax.ppermute(swapped_routes, SP_TP, whole)
     other = lax.ppermute(own, "sp_2", [(0, 1), (1, 0)])
     attended = attend_rows(
         index.reshape(1), queries[:HALF], mirrored_queries, own, other
     )
-    down_before, down_after, attended, held_residual, held_routes = lax.optimization_barrier(
-        (down_before, down_after, attended, held_residual, held_routes)
+    down_before, down_after, attended, held_residual = lax.optimization_barrier(
+        (down_before, down_after, attended, held_residual)
     )
     half = down_own.shape[0] // 2
     across_low = lax.ppermute(down_before[:half], "tp", up)

time: 307 us -> 301 us (0.980)
  starting transfers between devices: 83.6 us -> 79.8 us
    all_gather x1, waiting for transfers between devices: 38.3 us -> 29 us  [layer(): own = lax.all_gather(near, 'sp_0').reshape(-1, *block.shape)]
    ppermute x1, waiting for transfers between devices: 0.01 us -> 6.92 us  [layer(): held_routes = lax.ppermute(routes, SP_TP, whole)]
  transfers between devices with their start and end apart: 20 -> 20, of which waited for: 7 -> 8; matrix products, arithmetic and copies ran while one was open for 12% -> 12% of each run, Pallas kernels for 9% -> 9%
where the time goes in v9:
time: 301 us; the launch traced here: 295 us
  waiting for transfers between devices  110 us (37%)
  starting transfers between devices  79.8 us (27%)
  Pallas kernels  35.7 us (12%)
  matrix products  30.4 us (10%)
  between operations  13.7 us (5%)
  blocking collectives  13.5 us (4%)
  local copies, waits for them, and re-layouts  11.9 us (4%)
    all_to_all x1, starting transfers between devices, layer(): lax.all_to_all(slots, SP_TP, 0, 0, axis_index_groups=ranks, tiled=True)  30.4 us
    all_gather x1, waiting for transfers between devices, layer(): own = lax.all_gather(near, 'sp_0').reshape(-1, *block.shape)  29 us
    all_to_all x1, waiting for transfers between devices, layer(): returned = lax.all_to_all(spread(summed, capacity), SP, 0, 0, tiled=True)  22.4 us
    pallas_call x1, Pallas kernels, attend_rows(): pl.pallas_call(functools.partial(attend_body, blocks=blocks, heads=heads)...  22.2 us
    ppermute x2, waiting for transfers between devices, neighbours(): return (lax.ppermute(array, 'tp', up), lax.ppermute(array, 'tp', down))  18.9 us
    all_gather x1, blocking collectives, layer(): near = lax.all_gather(block, 'sp_1')  13.5 us
    all_to_all x1, waiting for transfers between devices, layer(): lax.all_to_all(partial.reshape(head_devices, -1, partial.shape[1]), 'tp',...  12.7 us
    all_to_all x1, waiting for transfers between devices, layer(): lax.all_to_all(slots, SP_TP, 0, 0, axis_index_groups=ranks, tiled=True)  11.6 us
  transfers between devices with their start and end apart: 20, of which 8 were waited for; matrix products, arithmetic and copies ran while one was open for 12% of the time, Pallas kernels for 9%

profile of v9, /device:TPU:6, one launch (start us, length us, event | category | flops | bytes accessed | tf_op | source)
XLA Modules:
  0.0 295.4 jit_solution(14781344704975255761)
XLA Ops:
  6.5 1.1 fusion.39
  7.7 7.8 %collective-permute-start.2 = (bf16[128,512]{1,0:T(8,128)(2,1)S(1)}, bf16[128,512]{1,0:T(8,128)(2,1)S(1)}, u32[]{:S(2)}, u32[]{:S(2)}) collective-permute-start(bf16[128,512]{1,0:T(8,128)(2,1)S(1)} %get-tuple-element.35), channel_id=1, source_target_pairs={{0,252},{4,248},{8,244},{12,240},{16,236},{20,232},{24,228},{28,22... | collective-permute-start | bytes 393224 | tf_op jit(solution)/shard_map/ppermute | solution.py:376
  15.5 1.6 prepare_keys.1
  17.1 13.5 %all-gather = bf16[640,256]{1,0:T(8,128)(2,1)} all-gather(bf16[160,256]{1,0:T(8,128)(2,1)} %prepare_keys.1), channel_id=2, replica_groups=mesh['sp_0'=8,'sp_1'=4,'sp_2'=2,'tp'=4] {'sp_1'}, dimensions={0}, use_global_device_ids=true | all-gather | bytes 409600 | tf_op jit(solution)/shard_map/all_gather | solution.py:380
  31.1 1.5 collective-permute-start.1
  32.7 0.8 copy.15.routes_ref
  33.5 1.9 collective-permute-start.3
  35.4 6.9 %collective-permute-done.3 = s32[64,2]{1,0:T(8,128)S(1)} collective-permute-done((s32[64,2]{1,0:T(8,128)S(1)}, s32[64,2]{1,0:T(8,128)S(1)}, u32[]{:S(2)}, u32[]{:S(2)}) %collective-permute-start.3) | collective-permute-done | bytes 544 | tf_op jit(solution)/shard_map/ppermute | solution.py:383
  42.3 29.0 %all-gather.4.cloned.1.call-done.own_ref = bf16[32,160,256]{2,1,0:T(8,128)(2,1)} async-done(((bf16[4,160,256]{2,1,0:T(8,128)(2,1)}), bf16[32,160,256]{2,1,0:T(8,128)(2,1)}) %all-gather.4.cloned.1.call-update) | async-done | bytes 2621456 | tf_op jit(solution)/shard_map/all_gather | solution.py:382
  71.4 6.0 %collective-permute-start.5 = (bf16[64,2048]{1,0:T(8,128)(2,1)}, bf16[64,2048]{1,0:T(8,128)(2,1)}, u32[]{:S(2)}, u32[]{:S(2)}) collective-permute-start(bf16[64,2048]{1,0:T(8,128)(2,1)} %param.14), channel_id=1, source_target_pairs={{0,0},{1,1},{2,254},{3,255},{4,4},{5,5},{6,250},{7,251},{8,8},{9,9... | collective-permute-start | bytes 786440 | tf_op jit(solution)/shard_map/ppermute | solution.py:385
  77.4 1.7 copy-done.1
  79.1 22.2 %attend_rows.1 = bf16[2,128,512]{2,1,0:T(8,128)(2,1)S(1)} custom-call(s32[1]{0:T(128)} %bitcast.1.index_ref, bf16[128,512]{1,0:T(8,128)(2,1)S(1)} %get-tuple-element.36.qa_ref, bf16[128,512]{1,0:T(8,128)(2,1)S(1)} %collective-permute-done.2.qb_ref, bf16[32,160,256]{2,1,0:T(8,128)(2,1)S(1)} %copy-done.1, bf16[32,160,256]{2,1,0:T(8,128)(2,1)} %collective-permute-done.4.other_ref), custom_call_target="tpu_custom_call" | custom-call | tf_op jit(solution)/shard_map/attend_rows/pallas_call | solution.py:196
  101.3 1.8 convolution_convert_fusion
  103.2 4.8 %all-to-all-start = ((bf16[4,64,2048]{2,1,0:T(8,128)(2,1)}), bf16[4,64,2048]{2,1,0:T(8,128)(2,1)}, u32[]{:S(2)}, u32[]{:S(2)}) async-start(bf16[4,64,2048]{2,1,0:T(8,128)(2,1)} %bitcast.55), calls=%async_computation | async-start | bytes 2097152 | tf_op jit(solution)/shard_map/all_to_all | solution.py:399
  108.6 12.7 %all-to-all-done.parts_ref = bf16[4,64,2048]{2,1,0:T(8,128)(2,1)} async-done(((bf16[4,64,2048]{2,1,0:T(8,128)(2,1)}), bf16[4,64,2048]{2,1,0:T(8,128)(2,1)}, u32[]{:S(2)}, u32[]{:S(2)}) %all-to-all-start) | async-done | bytes 1048608 | tf_op jit(solution)/shard_map/all_to_all | solution.py:399
  121.2 3.3 %dispatch.1 = (f32[64,2048]{1,0:T(8,128)}, bf16[64,48,128]{2,1,0:T(8,128)(2,1)}) custom-call(bf16[4,64,2048]{2,1,0:T(8,128)(2,1)} %all-to-all-done.parts_ref, bf16[64,2048]{1,0:T(8,128)(2,1)} %collective-permute-done.5.residual_ref, f32[1,2048]{1,0:T(1,128)} %bitcast.57, s32[64,2]{1,0:T(8,128)} %subtract_select_fusion.routes_ref), custom_call_target="tpu_custom_call" | custom-call | tf_op jit(solution)/shard_map/dispatch/pallas_call | solution.py:266
  124.5 30.4 %all-to-all-start.1 = ((bf16[64,48,128]{2,1,0:T(8,128)(2,1)}), bf16[64,48,128]{2,1,0:T(8,128)(2,1)}, u32[]{:S(2)}, u32[]{:S(2)}) async-start(bf16[64,48,128]{2,1,0:T(8,128)(2,1)} %get-tuple-element.27), calls=%async_computation.1 | async-start | bytes 1572864 | tf_op jit(solution)/shard_map/all_to_all | solution.py:413
  154.9 2.7 slice.22
  157.6 2.8 slice.23
  160.4 2.0 collective-permute-start.15
  162.4 11.6 %all-to-all-done.1.arrived_ref = bf16[64,48,128]{2,1,0:T(8,128)(2,1)} async-done(((bf16[64,48,128]{2,1,0:T(8,128)(2,1)}), bf16[64,48,128]{2,1,0:T(8,128)(2,1)}, u32[]{:S(2)}, u32[]{:S(2)}) %all-to-all-start.1) | async-done | bytes 786464 | tf_op jit(solution)/shard_map/all_to_all | solution.py:413
  174.0 2.6 arrange.1
  176.6 3.9 %collective-permute-start.8 = (bf16[192,2048]{1,0:T(8,128)(2,1)}, bf16[192,2048]{1,0:T(8,128)(2,1)}, u32[]{:S(2)}, u32[]{:S(2)}) collective-permute-start(bf16[192,2048]{1,0:T(8,128)(2,1)} %arrange.1), channel_id=1, source_target_pairs={{0,1},{1,2},{2,3},{3,0},{4,5},{5,6},{6,7},{7,4},{8,9},{9,10},{10,1... | collective-permute-start | bytes 2359304 | tf_op jit(solution)/shard_map/ppermute | solution.py:361
  180.5 4.3 %collective-permute-start.12 = (f32[64,2048]{1,0:T(8,128)}, f32[64,2048]{1,0:T(8,128)}, u32[]{:S(2)}, u32[]{:S(2)}) collective-permute-start(f32[64,2048]{1,0:T(8,128)} %get-tuple-element.32), channel_id=1, source_target_pairs={{0,0},{1,1},{2,254},{3,255},{4,4},{5,5},{6,250},{7,251},{8,8},{9,9... | collective-permute-start | bytes 1572872 | tf_op jit(solution)/shard_map/ppermute | solution.py:417
  184.8 3.8 %fusion.18 = f32[192,768]{1,0:T(8,128)} fusion(bf16[192,2048]{1,0:T(8,128)(2,1)} %arrange.1, bf16[1,2048,768]{2,1,0:T(8,128)(2,1)} %param.19), kind=kOutput, calls=%fused_computation.18 | convolution fusion | flops 603979776 | bytes 4521984 | tf_op jit(solution)/shard_map/dot_general | solution.py:421
  188.6 5.1 %fusion.28 = f32[192,2048]{1,0:T(8,128)} fusion(bf16[192,2048]{1,0:T(8,128)(2,1)} %arrange.1, bf16[1,2048,768]{2,1,0:T(8,128)(2,1)S(1)} %copy-done, f32[192,768]{1,0:T(8,128)} %fusion.18, bf16[1,768,2048]{2,1,0:T(8,128)(2,1)} %param.21), kind=kOutput, calls=%fused_computation.26 | convolution fusion | flops 1208844288 | bytes 9240576 | tf_op jit(solution)/shard_map/dot_general | solution.py:433
  193.7 17.5 %collective-permute-done.8 = bf16[192,2048]{1,0:T(8,128)(2,1)} collective-permute-done((bf16[192,2048]{1,0:T(8,128)(2,1)}, bf16[192,2048]{1,0:T(8,128)(2,1)}, u32[]{:S(2)}, u32[]{:S(2)}) %collective-permute-start.8) | collective-permute-done | bytes 786464 | tf_op jit(solution)/shard_map/ppermute | solution.py:361
  211.2 1.0 slice.24
  212.2 1.6 collective-permute-start.10
  213.8 1.4 collective-permute-done.6
  215.2 1.0 slice.25
  216.8 2.9 fusion.16
  219.8 1.9 fusion.14
  221.7 1.9 multiply_convert_fusion.2
  223.6 1.9 multiply_convert_fusion.1
  225.6 2.8 collective-permute-start.7
  228.4 0.8 fusion.12
  229.2 0.8 multiply_convert_fusion
  230.1 1.9 collective-permute-start.13
  231.9 8.2 %collective-permute-done.7 = bf16[192,768]{1,0:T(8,128)(2,1)S(1)} collective-permute-done((bf16[192,768]{1,0:T(8,128)(2,1)S(1)}, bf16[192,768]{1,0:T(8,128)(2,1)S(1)}, u32[]{:S(2)}, u32[]{:S(2)}) %collective-permute-start.7) | collective-permute-done | bytes 294944 | tf_op jit(solution)/shard_map/ppermute | solution.py:429
  240.1 2.7 convolution_add_fusion.1
  242.8 2.7 fusion
  245.6 4.0 %fusion.20.rows_ref = f32[192,2048]{1,0:T(8,128)} fusion(f32[192,2048]{1,0:T(8,128)S(1)} %fusion, f32[192,2048]{1,0:T(8,128)S(1)} %convolution_add_fusion.1, bf16[192,768]{1,0:T(8,128)(2,1)S(1)} %collective-permute-done.9, bf16[768,2048]{1,0:T(8,128)(2,1)} %collective-permute-done.1), kind=kOutput, calls=%fused_computation.21 | convolution fusion | flops 604766208 | bytes 8159232 | tf_op jit(solution)/shard_map/dot_general | solution.py:439
  249.5 2.9 spread.1
  252.4 9.8 %all-to-all-start.2 = ((bf16[64,48,128]{2,1,0:T(8,128)(2,1)}), bf16[64,48,128]{2,1,0:T(8,128)(2,1)}, u32[]{:S(2)}, u32[]{:S(2)}) async-start(bf16[64,48,128]{2,1,0:T(8,128)(2,1)} %spread.1), calls=%async_computation.2 | async-start | bytes 1572864 | tf_op jit(solution)/shard_map/all_to_all | solution.py:440
  262.2 0.7 copy.17.weight_ref
  262.9 22.4 %all-to-all-done.2.returned_ref = bf16[64,48,128]{2,1,0:T(8,128)(2,1)} async-done(((bf16[64,48,128]{2,1,0:T(8,128)(2,1)}), bf16[64,48,128]{2,1,0:T(8,128)(2,1)}, u32[]{:S(2)}, u32[]{:S(2)}) %all-to-all-start.2) | async-done | bytes 786464 | tf_op jit(solution)/shard_map/all_to_all | solution.py:440
  285.4 3.2 %combine.1 = bf16[64,2048]{1,0:T(8,128)(2,1)} custom-call(bf16[64,48,128]{2,1,0:T(8,128)(2,1)} %all-to-all-done.2.returned_ref, f32[64,2048]{1,0:T(8,128)} %collective-permute-done.12.hidden_ref, s32[64,2]{1,0:T(8,128)} %copy-done.5, f32[64,2]{1,0:T(8,128)} %copy.17.weight_ref), custom_call_target="tpu_custom_call" | custom-call | tf_op jit(solution)/shard_map/combine/pallas_call | solution.py:332
  (35 shorter events, 1.9 us)
Async XLA Ops:
  6.5 182.0 %copy-start = (bf16[1,2048,768]{2,1,0:T(8,128)(2,1)S(1)}, bf16[1,2048,768]{2,1,0:T(8,128)(2,1)}, u32[]{:S(2)}) copy-start(bf16[1,2048,768]{2,1,0:T(8,128)(2,1)} %param.20) | copy-start | bytes 9437188
  6.5 64.8 %all-gather.4.cloned.1.call-start = ((), (), s32[]{:S(2)}) async-start(), calls=%async_computation.3 | async-start | bytes 2949120 | tf_op jit(solution)/shard_map/all_gather | solution.py:382
  7.7 22.9 %collective-permute-start.2 = (bf16[128,512]{1,0:T(8,128)(2,1)S(1)}, bf16[128,512]{1,0:T(8,128)(2,1)S(1)}, u32[]{:S(2)}, u32[]{:S(2)}) collective-permute-start(bf16[128,512]{1,0:T(8,128)(2,1)S(1)} %get-tuple-element.35), channel_id=1, source_target_pairs={{0,252},{4,248},{8,244},{12,240},{16,236},{20,232},{24,228},{28,22... | collective-permute-start | bytes 393224 | tf_op jit(solution)/shard_map/ppermute | solution.py:376
  30.6 70.7 %collective-permute-start = (bf16[768,2048]{1,0:T(8,128)(2,1)}, bf16[768,2048]{1,0:T(8,128)(2,1)}, u32[]{:S(2)}, u32[]{:S(2)}) collective-permute-start(bf16[768,2048]{1,0:T(8,128)(2,1)} %bitcast.59), channel_id=1, source_target_pairs={{0,1},{1,2},{2,3},{3,0},{4,5},{5,6},{6,7},{7,4},{8,9},{9,10},{10,1... | collective-permute-start | bytes 9437192 | tf_op jit(solution)/shard_map/ppermute | solution.py:378
  31.1 70.1 %collective-permute-start.1 = (bf16[768,2048]{1,0:T(8,128)(2,1)}, bf16[768,2048]{1,0:T(8,128)(2,1)}, u32[]{:S(2)}, u32[]{:S(2)}) collective-permute-start(bf16[768,2048]{1,0:T(8,128)(2,1)} %bitcast.60), channel_id=1, source_target_pairs={{0,3},{1,0},{2,1},{3,2},{4,7},{5,4},{6,5},{7,6},{8,11},{9,8},{10,9... | collective-permute-start | bytes 9437192 | tf_op jit(solution)/shard_map/ppermute | solution.py:379
  33.5 69.7 %copy-start.5 = (s32[64,2]{1,0:T(8,128)}, s32[64,2]{1,0:T(8,128)S(1)}, u32[]{:S(2)}) copy-start(s32[64,2]{1,0:T(8,128)S(1)} %copy.15.routes_ref) | copy-start | bytes 1540
  33.5 8.8 %collective-permute-start.3 = (s32[64,2]{1,0:T(8,128)S(1)}, s32[64,2]{1,0:T(8,128)S(1)}, u32[]{:S(2)}, u32[]{:S(2)}) collective-permute-start(s32[64,2]{1,0:T(8,128)S(1)} %copy.15.routes_ref), channel_id=1, source_target_pairs={{0,0},{1,1},{2,254},{3,255},{4,4},{5,5},{6,250},{7,251},{8,8},{9,9... | collective-permute-start | bytes 1544 | tf_op jit(solution)/shard_map/ppermute | solution.py:383
  71.4 6.0 %collective-permute-start.4 = (bf16[32,160,256]{2,1,0:T(8,128)(2,1)}, bf16[32,160,256]{2,1,0:T(8,128)(2,1)}, u32[]{:S(2)}, u32[]{:S(2)}) collective-permute-start(bf16[32,160,256]{2,1,0:T(8,128)(2,1)} %all-gather.4.cloned.1.call-done.own_ref), channel_id=1, source_target_pairs={{0,4},{4,0},{1,5},{5,1},{2,6},{6,2},{3,7},{7,3},{8,12},{12,8},{9,1... | collective-permute-start | bytes 7864328 | tf_op jit(solution)/shard_map/ppermute | solution.py:386
  71.4 29.9 %collective-permute-start.5 = (bf16[64,2048]{1,0:T(8,128)(2,1)}, bf16[64,2048]{1,0:T(8,128)(2,1)}, u32[]{:S(2)}, u32[]{:S(2)}) collective-permute-start(bf16[64,2048]{1,0:T(8,128)(2,1)} %param.14), channel_id=1, source_target_pairs={{0,0},{1,1},{2,254},{3,255},{4,4},{5,5},{6,250},{7,251},{8,8},{9,9... | collective-permute-start | bytes 786440 | tf_op jit(solution)/shard_map/ppermute | solution.py:385
  77.4 1.7 copy-start.1
  79.1 22.2 %copy-start.3 = (bf16[512,2048]{1,0:T(8,128)(2,1)S(1)}, bf16[512,2048]{1,0:T(8,128)(2,1)}, u32[]{:S(2)}) copy-start(bf16[512,2048]{1,0:T(8,128)(2,1)} %param.15) | copy-start | bytes 6291460
  103.2 18.1 %all-to-all-start = ((bf16[4,64,2048]{2,1,0:T(8,128)(2,1)}), bf16[4,64,2048]{2,1,0:T(8,128)(2,1)}, u32[]{:S(2)}, u32[]{:S(2)}) async-start(bf16[4,64,2048]{2,1,0:T(8,128)(2,1)} %bitcast.55), calls=%async_computation | async-start | bytes 2097152 | tf_op jit(solution)/shard_map/all_to_all | solution.py:399
  124.5 49.5 %all-to-all-start.1 = ((bf16[64,48,128]{2,1,0:T(8,128)(2,1)}), bf16[64,48,128]{2,1,0:T(8,128)(2,1)}, u32[]{:S(2)}, u32[]{:S(2)}) async-start(bf16[64,48,128]{2,1,0:T(8,128)(2,1)} %get-tuple-element.27), calls=%async_computation.1 | async-start | bytes 1572864 | tf_op jit(solution)/shard_map/all_to_all | solution.py:413
  157.6 85.2 %collective-permute-start.14 = (bf16[384,2048]{1,0:T(8,128)(2,1)}, bf16[384,2048]{1,0:T(8,128)(2,1)}, u32[]{:S(2)}, u32[]{:S(2)}) collective-permute-start(bf16[384,2048]{1,0:T(8,128)(2,1)} %slice.22), channel_id=1, source_target_pairs={{0,1},{1,2},{2,3},{3,0},{4,5},{5,6},{6,7},{7,4},{8,9},{9,10},{10,1... | collective-permute-start | bytes 4718600 | tf_op jit(solution)/shard_map/ppermute | solution.py:394
  160.4 82.4 %collective-permute-start.15 = (bf16[384,2048]{1,0:T(8,128)(2,1)}, bf16[384,2048]{1,0:T(8,128)(2,1)}, u32[]{:S(2)}, u32[]{:S(2)}) collective-permute-start(bf16[384,2048]{1,0:T(8,128)(2,1)} %slice.23), channel_id=1, source_target_pairs={{0,3},{1,0},{2,1},{3,2},{4,7},{5,4},{6,5},{7,6},{8,11},{9,8},{10,9... | collective-permute-start | bytes 4718600 | tf_op jit(solution)/shard_map/ppermute | solution.py:395
  176.6 38.6 %collective-permute-start.6 = (bf16[192,2048]{1,0:T(8,128)(2,1)}, bf16[192,2048]{1,0:T(8,128)(2,1)}, u32[]{:S(2)}, u32[]{:S(2)}) collective-permute-start(bf16[192,2048]{1,0:T(8,128)(2,1)} %arrange.1), channel_id=1, source_target_pairs={{0,3},{1,0},{2,1},{3,2},{4,7},{5,4},{6,5},{7,6},{8,11},{9,8},{10,9... | collective-permute-start | bytes 2359304 | tf_op jit(solution)/shard_map/ppermute | solution.py:361
  176.6 34.6 %collective-permute-start.8 = (bf16[192,2048]{1,0:T(8,128)(2,1)}, bf16[192,2048]{1,0:T(8,128)(2,1)}, u32[]{:S(2)}, u32[]{:S(2)}) collective-permute-start(bf16[192,2048]{1,0:T(8,128)(2,1)} %arrange.1), channel_id=1, source_target_pairs={{0,1},{1,2},{2,3},{3,0},{4,5},{5,6},{6,7},{7,4},{8,9},{9,10},{10,1... | collective-permute-start | bytes 2359304 | tf_op jit(solution)/shard_map/ppermute | solution.py:361
  180.5 48.0 %collective-permute-start.12 = (f32[64,2048]{1,0:T(8,128)}, f32[64,2048]{1,0:T(8,128)}, u32[]{:S(2)}, u32[]{:S(2)}) collective-permute-start(f32[64,2048]{1,0:T(8,128)} %get-tuple-element.32), channel_id=1, source_target_pairs={{0,0},{1,1},{2,254},{3,255},{4,4},{5,5},{6,250},{7,251},{8,8},{9,9... | collective-permute-start | bytes 1572872 | tf_op jit(solution)/shard_map/ppermute | solution.py:417
  193.7 26.1 %copy-start.2 = (bf16[1,2048,768]{2,1,0:T(8,128)(2,1)S(1)}, bf16[1,2048,768]{2,1,0:T(8,128)(2,1)}, u32[]{:S(2)}) copy-start(bf16[1,2048,768]{2,1,0:T(8,128)(2,1)} %param.19) | copy-start | bytes 9437188
  212.2 13.3 %collective-permute-start.10 = (bf16[96,2048]{1,0:T(8,128)(2,1)S(1)}, bf16[96,2048]{1,0:T(8,128)(2,1)S(1)}, u32[]{:S(2)}, u32[]{:S(2)}) collective-permute-start(bf16[96,2048]{1,0:T(8,128)(2,1)S(1)} %slice.24), channel_id=1, source_target_pairs={{0,1},{1,2},{2,3},{3,0},{4,5},{5,6},{6,7},{7,4},{8,9},{9,10},{10,1... | collective-permute-start | bytes 1179656 | tf_op jit(solution)/shard_map/ppermute | solution.py:366
  216.2 12.1 %collective-permute-start.11 = (bf16[96,2048]{1,0:T(8,128)(2,1)S(1)}, bf16[96,2048]{1,0:T(8,128)(2,1)S(1)}, u32[]{:S(2)}, u32[]{:S(2)}) collective-permute-start(bf16[96,2048]{1,0:T(8,128)(2,1)S(1)} %slice.25), channel_id=1, source_target_pairs={{0,3},{1,0},{2,1},{3,2},{4,7},{5,4},{6,5},{7,6},{8,11},{9,8},{10,9... | collective-permute-start | bytes 1179656 | tf_op jit(solution)/shard_map/ppermute | solution.py:366
  225.6 14.5 %collective-permute-start.7 = (bf16[192,768]{1,0:T(8,128)(2,1)S(1)}, bf16[192,768]{1,0:T(8,128)(2,1)S(1)}, u32[]{:S(2)}, u32[]{:S(2)}) collective-permute-start(bf16[192,768]{1,0:T(8,128)(2,1)S(1)} %multiply_convert_fusion.2), channel_id=1, source_target_pairs={{0,1},{1,2},{2,3},{3,0},{4,5},{5,6},{6,7},{7,4},{8,9},{9,10},{10,1... | collective-permute-start | bytes 884744 | tf_op jit(solution)/shard_map/ppermute | solution.py:429
  228.4 17.2 %collective-permute-start.9 = (bf16[192,768]{1,0:T(8,128)(2,1)S(1)}, bf16[192,768]{1,0:T(8,128)(2,1)S(1)}, u32[]{:S(2)}, u32[]{:S(2)}) collective-permute-start(bf16[192,768]{1,0:T(8,128)(2,1)S(1)} %multiply_convert_fusion.1), channel_id=1, source_target_pairs={{0,3},{1,0},{2,1},{3,2},{4,7},{5,4},{6,5},{7,6},{8,11},{9,8},{10,9... | collective-permute-start | bytes 884744 | tf_op jit(solution)/shard_map/ppermute | solution.py:430
  229.2 10.8 %copy-start.4 = (f32[192,2048]{1,0:T(8,128)S(1)}, f32[192,2048]{1,0:T(8,128)}, u32[]{:S(2)}) copy-start(f32[192,2048]{1,0:T(8,128)} %fusion.28) | copy-start | bytes 4718596
  230.1 12.8 %collective-permute-start.13 = (bf16[192,768]{1,0:T(8,128)(2,1)S(1)}, bf16[192,768]{1,0:T(8,128)(2,1)S(1)}, u32[]{:S(2)}, u32[]{:S(2)}) collective-permute-start(bf16[192,768]{1,0:T(8,128)(2,1)S(1)} %multiply_convert_fusion), channel_id=1, source_target_pairs={{0,2},{1,3},{2,0},{3,1},{4,6},{5,7},{6,4},{7,5},{8,10},{9,11},{10,... | collective-permute-start | bytes 884744 | tf_op jit(solution)/shard_map/ppermute | solution.py:432
  249.5 12.7 %copy-start.6 = (f32[64,2]{0,1:T(2,128)S(1)}, f32[64,2]{0,1:T(2,128)}, u32[]{:S(2)}) copy-start(f32[64,2]{0,1:T(2,128)} %param.18) | copy-start | bytes 1540
  252.4 32.9 %all-to-all-start.2 = ((bf16[64,48,128]{2,1,0:T(8,128)(2,1)}), bf16[64,48,128]{2,1,0:T(8,128)(2,1)}, u32[]{:S(2)}, u32[]{:S(2)}) async-start(bf16[64,48,128]{2,1,0:T(8,128)(2,1)} %spread.1), calls=%async_computation.2 | async-start | bytes 1572864 | tf_op jit(solution)/shard_map/all_to_all | solution.py:440
Sparse Core Ops, SparseCore 0:
  30.7 40.5 all-gather.3

commit v10 on v9

--- a/solution.py
+++ b/solution.py
@@ -22,7 +22,7 @@
 
 
 SAFE_SCORE = 60.0
-STEP = 512
+STEP = 1024
 PAIRS = 2
 
 
@@ -296,7 +296,8 @@
 def spread_body(rows_ref, leaving_ref, tiles_ref, *, capacity):
     count = leaving_ref.shape[0]
     for slot in range(capacity):
-        spread_rows(tiles_ref, rows_ref[slot * count : (slot + 1) * count, :], slot, capacity)
+        rows = rows_ref[slot * count : (slot + 1) * count, :].astype(jnp.float32)
+        spread_rows(tiles_ref, rows, slot, capacity)
     leaving_ref[...] = tiles_ref[...].reshape(leaving_ref.shape).astype(jnp.bfloat16)
 
 
@@ -437,7 +438,7 @@
         (units_from_across, down_across),
     ):
         summed = summed + jnp.dot(got, weight, preferred_element_type=jnp.float32)
-    returned = lax.all_to_all(spread(summed, capacity), SP, 0, 0, tiled=True)
+    returned = lax.all_to_all(spread(summed.astype(jnp.bfloat16), capacity), SP, 0, 0, tiled=True)
     return combine(returned, hidden_state, routes, route_weight, capacity)
 
 

time: 301 us -> 289 us (0.960)
  starting transfers between devices: 79.8 us -> 69.4 us
    all_to_all x1, starting transfers between devices: 30.4 us -> 19.9 us  [layer(): lax.all_to_all(slots, SP_TP, 0, 0, axis_index_groups=ranks, tiled=True)]
where the time goes in v10:
time: 289 us; the launch traced here: 284 us
  waiting for transfers between devices  110 us (38%)
  starting transfers between devices  69.4 us (24%)
  Pallas kernels  34.6 us (12%)
  matrix products  30.1 us (10%)
  between operations  13.7 us (5%)
  blocking collectives  13.5 us (5%)
  local copies, waits for them, and re-layouts  11.9 us (4%)
    all_gather x1, waiting for transfers between devices, layer(): own = lax.all_gather(near, 'sp_0').reshape(-1, *block.shape)  29 us
    all_to_all x1, waiting for transfers between devices, layer(): lax.all_to_all(spread(summed.astype(jnp.bfloat16), capacity), SP, 0, 0, t...  22.4 us
    pallas_call x1, Pallas kernels, attend_rows(): pl.pallas_call(functools.partial(attend_body, blocks=blocks, heads=heads)...  21.4 us
    all_to_all x1, starting transfers between devices, layer(): lax.all_to_all(slots, SP_TP, 0, 0, axis_index_groups=ranks, tiled=True)  19.9 us
    ppermute x2, waiting for transfers between devices, neighbours(): return (lax.ppermute(array, 'tp', up), lax.ppermute(array, 'tp', down))  18.9 us
    all_gather x1, blocking collectives, layer(): near = lax.all_gather(block, 'sp_1')  13.5 us
    all_to_all x1, waiting for transfers between devices, layer(): lax.all_to_all(partial.reshape(head_devices, -1, partial.shape[1]), 'tp',...  12.7 us
    all_to_all x1, waiting for transfers between devices, layer(): lax.all_to_all(slots, SP_TP, 0, 0, axis_index_groups=ranks, tiled=True)  11.6 us
  transfers between devices with their start and end apart: 20, of which 8 were waited for; matrix products, arithmetic and copies ran while one was open for 12% of the time, Pallas kernels for 9%

profile of v10, /device:TPU:6, one launch (start us, length us, event | category | flops | bytes accessed | tf_op | source)
XLA Modules:
  0.0 283.7 jit_solution(13953002772953811452)
XLA Ops:
  6.5 1.1 fusion.40
  7.7 7.8 %collective-permute-start.2 = (bf16[128,512]{1,0:T(8,128)(2,1)S(1)}, bf16[128,512]{1,0:T(8,128)(2,1)S(1)}, u32[]{:S(2)}, u32[]{:S(2)}) collective-permute-start(bf16[128,512]{1,0:T(8,128)(2,1)S(1)} %get-tuple-element.35), channel_id=1, source_target_pairs={{0,252},{4,248},{8,244},{12,240},{16,236},{20,232},{24,228},{28,22... | collective-permute-start | bytes 393224 | tf_op jit(solution)/shard_map/ppermute | solution.py:377
  15.5 1.6 prepare_keys.1
  17.1 13.5 %all-gather = bf16[640,256]{1,0:T(8,128)(2,1)} all-gather(bf16[160,256]{1,0:T(8,128)(2,1)} %prepare_keys.1), channel_id=2, replica_groups=mesh['sp_0'=8,'sp_1'=4,'sp_2'=2,'tp'=4] {'sp_1'}, dimensions={0}, use_global_device_ids=true | all-gather | bytes 409600 | tf_op jit(solution)/shard_map/all_gather | solution.py:381
  31.1 1.5 collective-permute-start.1
  32.7 0.8 copy.15.routes_ref
  33.5 1.9 collective-permute-start.3
  35.4 6.9 %collective-permute-done.3 = s32[64,2]{1,0:T(8,128)S(1)} collective-permute-done((s32[64,2]{1,0:T(8,128)S(1)}, s32[64,2]{1,0:T(8,128)S(1)}, u32[]{:S(2)}, u32[]{:S(2)}) %collective-permute-start.3) | collective-permute-done | bytes 544 | tf_op jit(solution)/shard_map/ppermute | solution.py:384
  42.3 29.0 %all-gather.4.cloned.1.call-done.own_ref = bf16[32,160,256]{2,1,0:T(8,128)(2,1)} async-done(((bf16[4,160,256]{2,1,0:T(8,128)(2,1)}), bf16[32,160,256]{2,1,0:T(8,128)(2,1)}) %all-gather.4.cloned.1.call-update) | async-done | bytes 2621456 | tf_op jit(solution)/shard_map/all_gather | solution.py:383
  71.4 6.0 %collective-permute-start.5 = (bf16[64,2048]{1,0:T(8,128)(2,1)}, bf16[64,2048]{1,0:T(8,128)(2,1)}, u32[]{:S(2)}, u32[]{:S(2)}) collective-permute-start(bf16[64,2048]{1,0:T(8,128)(2,1)} %param.14), channel_id=1, source_target_pairs={{0,0},{1,1},{2,254},{3,255},{4,4},{5,5},{6,250},{7,251},{8,8},{9,9... | collective-permute-start | bytes 786440 | tf_op jit(solution)/shard_map/ppermute | solution.py:386
  77.4 1.7 copy-done.1
  79.1 21.4 %attend_rows.1 = bf16[2,128,512]{2,1,0:T(8,128)(2,1)S(1)} custom-call(s32[1]{0:T(128)} %bitcast.1.index_ref, bf16[128,512]{1,0:T(8,128)(2,1)S(1)} %get-tuple-element.36.qa_ref, bf16[128,512]{1,0:T(8,128)(2,1)S(1)} %collective-permute-done.2.qb_ref, bf16[32,160,256]{2,1,0:T(8,128)(2,1)S(1)} %copy-done.1, bf16[32,160,256]{2,1,0:T(8,128)(2,1)} %collective-permute-done.4.other_ref), custom_call_target="tpu_custom_call" | custom-call | tf_op jit(solution)/shard_map/attend_rows/pallas_call | solution.py:196
  100.6 1.8 convolution_convert_fusion
  102.4 4.8 %all-to-all-start = ((bf16[4,64,2048]{2,1,0:T(8,128)(2,1)}), bf16[4,64,2048]{2,1,0:T(8,128)(2,1)}, u32[]{:S(2)}, u32[]{:S(2)}) async-start(bf16[4,64,2048]{2,1,0:T(8,128)(2,1)} %bitcast.55), calls=%async_computation | async-start | bytes 2097152 | tf_op jit(solution)/shard_map/all_to_all | solution.py:400
  107.8 12.7 %all-to-all-done.parts_ref = bf16[4,64,2048]{2,1,0:T(8,128)(2,1)} async-done(((bf16[4,64,2048]{2,1,0:T(8,128)(2,1)}), bf16[4,64,2048]{2,1,0:T(8,128)(2,1)}, u32[]{:S(2)}, u32[]{:S(2)}) %all-to-all-start) | async-done | bytes 1048608 | tf_op jit(solution)/shard_map/all_to_all | solution.py:400
  120.5 3.3 %dispatch.1 = (f32[64,2048]{1,0:T(8,128)}, bf16[64,48,128]{2,1,0:T(8,128)(2,1)}) custom-call(bf16[4,64,2048]{2,1,0:T(8,128)(2,1)} %all-to-all-done.parts_ref, bf16[64,2048]{1,0:T(8,128)(2,1)} %collective-permute-done.5.residual_ref, f32[1,2048]{1,0:T(1,128)} %bitcast.57, s32[64,2]{1,0:T(8,128)} %subtract_select_fusion.routes_ref), custom_call_target="tpu_custom_call" | custom-call | tf_op jit(solution)/shard_map/dispatch/pallas_call | solution.py:266
  123.8 19.9 %all-to-all-start.1 = ((bf16[64,48,128]{2,1,0:T(8,128)(2,1)}), bf16[64,48,128]{2,1,0:T(8,128)(2,1)}, u32[]{:S(2)}, u32[]{:S(2)}) async-start(bf16[64,48,128]{2,1,0:T(8,128)(2,1)} %get-tuple-element.27), calls=%async_computation.1 | async-start | bytes 1572864 | tf_op jit(solution)/shard_map/all_to_all | solution.py:414
  143.7 2.7 slice.22
  146.5 2.8 slice.23
  149.2 2.0 collective-permute-start.15
  151.3 11.6 %all-to-all-done.1.arrived_ref = bf16[64,48,128]{2,1,0:T(8,128)(2,1)} async-done(((bf16[64,48,128]{2,1,0:T(8,128)(2,1)}), bf16[64,48,128]{2,1,0:T(8,128)(2,1)}, u32[]{:S(2)}, u32[]{:S(2)}) %all-to-all-start.1) | async-done | bytes 786464 | tf_op jit(solution)/shard_map/all_to_all | solution.py:414
  162.8 2.6 arrange.1
  165.4 3.9 %collective-permute-start.8 = (bf16[192,2048]{1,0:T(8,128)(2,1)}, bf16[192,2048]{1,0:T(8,128)(2,1)}, u32[]{:S(2)}, u32[]{:S(2)}) collective-permute-start(bf16[192,2048]{1,0:T(8,128)(2,1)} %arrange.1), channel_id=1, source_target_pairs={{0,1},{1,2},{2,3},{3,0},{4,5},{5,6},{6,7},{7,4},{8,9},{9,10},{10,1... | collective-permute-start | bytes 2359304 | tf_op jit(solution)/shard_map/ppermute | solution.py:362
  169.3 4.3 %collective-permute-start.12 = (f32[64,2048]{1,0:T(8,128)}, f32[64,2048]{1,0:T(8,128)}, u32[]{:S(2)}, u32[]{:S(2)}) collective-permute-start(f32[64,2048]{1,0:T(8,128)} %get-tuple-element.32), channel_id=1, source_target_pairs={{0,0},{1,1},{2,254},{3,255},{4,4},{5,5},{6,250},{7,251},{8,8},{9,9... | collective-permute-start | bytes 1572872 | tf_op jit(solution)/shard_map/ppermute | solution.py:418
  173.6 3.8 %fusion.18 = f32[192,768]{1,0:T(8,128)} fusion(bf16[192,2048]{1,0:T(8,128)(2,1)} %arrange.1, bf16[1,2048,768]{2,1,0:T(8,128)(2,1)} %param.19), kind=kOutput, calls=%fused_computation.18 | convolution fusion | flops 603979776 | bytes 4521984 | tf_op jit(solution)/shard_map/dot_general | solution.py:422
  177.4 5.1 %fusion.29 = f32[192,2048]{1,0:T(8,128)} fusion(bf16[192,2048]{1,0:T(8,128)(2,1)} %arrange.1, bf16[1,2048,768]{2,1,0:T(8,128)(2,1)S(1)} %copy-done, f32[192,768]{1,0:T(8,128)} %fusion.18, bf16[1,768,2048]{2,1,0:T(8,128)(2,1)} %param.21), kind=kOutput, calls=%fused_computation.27 | convolution fusion | flops 1208844288 | bytes 9240576 | tf_op jit(solution)/shard_map/dot_general | solution.py:434
  182.5 17.5 %collective-permute-done.8 = bf16[192,2048]{1,0:T(8,128)(2,1)} collective-permute-done((bf16[192,2048]{1,0:T(8,128)(2,1)}, bf16[192,2048]{1,0:T(8,128)(2,1)}, u32[]{:S(2)}, u32[]{:S(2)}) %collective-permute-start.8) | collective-permute-done | bytes 786464 | tf_op jit(solution)/shard_map/ppermute | solution.py:362
  200.0 1.0 slice.24
  201.1 1.6 collective-permute-start.10
  202.6 1.4 collective-permute-done.6
  204.0 1.0 slice.25
  205.7 2.9 %fusion.16 = f32[192,768]{1,0:T(8,128)S(1)} fusion(bf16[192,2048]{1,0:T(8,128)(2,1)} %collective-permute-done.6, bf16[1,2048,768]{2,1,0:T(8,128)(2,1)} %param.19), kind=kOutput, calls=%fused_computation.16 | convolution fusion | flops 603979776 | bytes 4521984 | tf_op jit(solution)/shard_map/dot_general | solution.py:422
  208.6 1.9 fusion.14
  210.6 1.9 multiply_convert_fusion.2
  212.5 1.9 multiply_convert_fusion.1
  214.4 2.8 collective-permute-start.7
  217.3 0.8 fusion.12
  218.1 0.8 multiply_convert_fusion
  218.9 1.9 collective-permute-start.13
  220.8 8.2 %collective-permute-done.7 = bf16[192,768]{1,0:T(8,128)(2,1)S(1)} collective-permute-done((bf16[192,768]{1,0:T(8,128)(2,1)S(1)}, bf16[192,768]{1,0:T(8,128)(2,1)S(1)}, u32[]{:S(2)}, u32[]{:S(2)}) %collective-permute-start.7) | collective-permute-done | bytes 294944 | tf_op jit(solution)/shard_map/ppermute | solution.py:430
  228.9 2.7 convolution_add_fusion.1
  231.7 2.7 fusion
  234.4 3.7 %fusion.21.rows_ref = bf16[192,2048]{1,0:T(8,128)(2,1)} fusion(f32[192,2048]{1,0:T(8,128)S(1)} %fusion, f32[192,2048]{1,0:T(8,128)S(1)} %convolution_add_fusion.1, bf16[192,768]{1,0:T(8,128)(2,1)S(1)} %collective-permute-done.9, bf16[768,2048]{1,0:T(8,128)(2,1)} %collective-permute-done.1), kind=kOutput, calls=%fused_computation.24 | convolution fusion | flops 605159424 | bytes 7372800 | tf_op jit(solution)/shard_map/dot_general | solution.py:440
  238.1 2.6 spread.1
  240.7 9.8 %all-to-all-start.2 = ((bf16[64,48,128]{2,1,0:T(8,128)(2,1)}), bf16[64,48,128]{2,1,0:T(8,128)(2,1)}, u32[]{:S(2)}, u32[]{:S(2)}) async-start(bf16[64,48,128]{2,1,0:T(8,128)(2,1)} %spread.1), calls=%async_computation.2 | async-start | bytes 1572864 | tf_op jit(solution)/shard_map/all_to_all | solution.py:441
  250.5 0.7 copy.17.weight_ref
  251.2 22.4 %all-to-all-done.2.returned_ref = bf16[64,48,128]{2,1,0:T(8,128)(2,1)} async-done(((bf16[64,48,128]{2,1,0:T(8,128)(2,1)}), bf16[64,48,128]{2,1,0:T(8,128)(2,1)}, u32[]{:S(2)}, u32[]{:S(2)}) %all-to-all-start.2) | async-done | bytes 786464 | tf_op jit(solution)/shard_map/all_to_all | solution.py:441
  273.6 3.2 %combine.1 = bf16[64,2048]{1,0:T(8,128)(2,1)} custom-call(bf16[64,48,128]{2,1,0:T(8,128)(2,1)} %all-to-all-done.2.returned_ref, f32[64,2048]{1,0:T(8,128)} %collective-permute-done.12.hidden_ref, s32[64,2]{1,0:T(8,128)} %copy-done.5, f32[64,2]{1,0:T(8,128)} %copy.17.weight_ref), custom_call_target="tpu_custom_call" | custom-call | tf_op jit(solution)/shard_map/combine/pallas_call | solution.py:333
  (35 shorter events, 1.9 us)
Async XLA Ops:
  6.5 170.9 %copy-start = (bf16[1,2048,768]{2,1,0:T(8,128)(2,1)S(1)}, bf16[1,2048,768]{2,1,0:T(8,128)(2,1)}, u32[]{:S(2)}) copy-start(bf16[1,2048,768]{2,1,0:T(8,128)(2,1)} %param.20) | copy-start | bytes 9437188
  6.5 64.8 %all-gather.4.cloned.1.call-start = ((), (), s32[]{:S(2)}) async-start(), calls=%async_computation.3 | async-start | bytes 2949120 | tf_op jit(solution)/shard_map/all_gather | solution.py:383
  7.7 22.9 %collective-permute-start.2 = (bf16[128,512]{1,0:T(8,128)(2,1)S(1)}, bf16[128,512]{1,0:T(8,128)(2,1)S(1)}, u32[]{:S(2)}, u32[]{:S(2)}) collective-permute-start(bf16[128,512]{1,0:T(8,128)(2,1)S(1)} %get-tuple-element.35), channel_id=1, source_target_pairs={{0,252},{4,248},{8,244},{12,240},{16,236},{20,232},{24,228},{28,22... | collective-permute-start | bytes 393224 | tf_op jit(solution)/shard_map/ppermute | solution.py:377
  30.6 69.9 %collective-permute-start = (bf16[768,2048]{1,0:T(8,128)(2,1)}, bf16[768,2048]{1,0:T(8,128)(2,1)}, u32[]{:S(2)}, u32[]{:S(2)}) collective-permute-start(bf16[768,2048]{1,0:T(8,128)(2,1)} %bitcast.59), channel_id=1, source_target_pairs={{0,1},{1,2},{2,3},{3,0},{4,5},{5,6},{6,7},{7,4},{8,9},{9,10},{10,1... | collective-permute-start | bytes 9437192 | tf_op jit(solution)/shard_map/ppermute | solution.py:379
  31.1 69.4 %collective-permute-start.1 = (bf16[768,2048]{1,0:T(8,128)(2,1)}, bf16[768,2048]{1,0:T(8,128)(2,1)}, u32[]{:S(2)}, u32[]{:S(2)}) collective-permute-start(bf16[768,2048]{1,0:T(8,128)(2,1)} %bitcast.60), channel_id=1, source_target_pairs={{0,3},{1,0},{2,1},{3,2},{4,7},{5,4},{6,5},{7,6},{8,11},{9,8},{10,9... | collective-permute-start | bytes 9437192 | tf_op jit(solution)/shard_map/ppermute | solution.py:380
  33.5 68.9 %copy-start.5 = (s32[64,2]{1,0:T(8,128)}, s32[64,2]{1,0:T(8,128)S(1)}, u32[]{:S(2)}) copy-start(s32[64,2]{1,0:T(8,128)S(1)} %copy.15.routes_ref) | copy-start | bytes 1540
  33.5 8.8 %collective-permute-start.3 = (s32[64,2]{1,0:T(8,128)S(1)}, s32[64,2]{1,0:T(8,128)S(1)}, u32[]{:S(2)}, u32[]{:S(2)}) collective-permute-start(s32[64,2]{1,0:T(8,128)S(1)} %copy.15.routes_ref), channel_id=1, source_target_pairs={{0,0},{1,1},{2,254},{3,255},{4,4},{5,5},{6,250},{7,251},{8,8},{9,9... | collective-permute-start | bytes 1544 | tf_op jit(solution)/shard_map/ppermute | solution.py:384
  71.4 6.0 %collective-permute-start.4 = (bf16[32,160,256]{2,1,0:T(8,128)(2,1)}, bf16[32,160,256]{2,1,0:T(8,128)(2,1)}, u32[]{:S(2)}, u32[]{:S(2)}) collective-permute-start(bf16[32,160,256]{2,1,0:T(8,128)(2,1)} %all-gather.4.cloned.1.call-done.own_ref), channel_id=1, source_target_pairs={{0,4},{4,0},{1,5},{5,1},{2,6},{6,2},{3,7},{7,3},{8,12},{12,8},{9,1... | collective-permute-start | bytes 7864328 | tf_op jit(solution)/shard_map/ppermute | solution.py:387
  71.4 29.2 %collective-permute-start.5 = (bf16[64,2048]{1,0:T(8,128)(2,1)}, bf16[64,2048]{1,0:T(8,128)(2,1)}, u32[]{:S(2)}, u32[]{:S(2)}) collective-permute-start(bf16[64,2048]{1,0:T(8,128)(2,1)} %param.14), channel_id=1, source_target_pairs={{0,0},{1,1},{2,254},{3,255},{4,4},{5,5},{6,250},{7,251},{8,8},{9,9... | collective-permute-start | bytes 786440 | tf_op jit(solution)/shard_map/ppermute | solution.py:386
  77.4 1.7 copy-start.1
  79.1 21.5 %copy-start.3 = (bf16[512,2048]{1,0:T(8,128)(2,1)S(1)}, bf16[512,2048]{1,0:T(8,128)(2,1)}, u32[]{:S(2)}) copy-start(bf16[512,2048]{1,0:T(8,128)(2,1)} %param.15) | copy-start | bytes 6291460
  102.4 18.1 %all-to-all-start = ((bf16[4,64,2048]{2,1,0:T(8,128)(2,1)}), bf16[4,64,2048]{2,1,0:T(8,128)(2,1)}, u32[]{:S(2)}, u32[]{:S(2)}) async-start(bf16[4,64,2048]{2,1,0:T(8,128)(2,1)} %bitcast.55), calls=%async_computation | async-start | bytes 2097152 | tf_op jit(solution)/shard_map/all_to_all | solution.py:400
  123.8 39.1 %all-to-all-start.1 = ((bf16[64,48,128]{2,1,0:T(8,128)(2,1)}), bf16[64,48,128]{2,1,0:T(8,128)(2,1)}, u32[]{:S(2)}, u32[]{:S(2)}) async-start(bf16[64,48,128]{2,1,0:T(8,128)(2,1)} %get-tuple-element.27), calls=%async_computation.1 | async-start | bytes 1572864 | tf_op jit(solution)/shard_map/all_to_all | solution.py:414
  146.5 85.2 %collective-permute-start.14 = (bf16[384,2048]{1,0:T(8,128)(2,1)}, bf16[384,2048]{1,0:T(8,128)(2,1)}, u32[]{:S(2)}, u32[]{:S(2)}) collective-permute-start(bf16[384,2048]{1,0:T(8,128)(2,1)} %slice.22), channel_id=1, source_target_pairs={{0,1},{1,2},{2,3},{3,0},{4,5},{5,6},{6,7},{7,4},{8,9},{9,10},{10,1... | collective-permute-start | bytes 4718600 | tf_op jit(solution)/shard_map/ppermute | solution.py:395
  149.2 82.4 %collective-permute-start.15 = (bf16[384,2048]{1,0:T(8,128)(2,1)}, bf16[384,2048]{1,0:T(8,128)(2,1)}, u32[]{:S(2)}, u32[]{:S(2)}) collective-permute-start(bf16[384,2048]{1,0:T(8,128)(2,1)} %slice.23), channel_id=1, source_target_pairs={{0,3},{1,0},{2,1},{3,2},{4,7},{5,4},{6,5},{7,6},{8,11},{9,8},{10,9... | collective-permute-start | bytes 4718600 | tf_op jit(solution)/shard_map/ppermute | solution.py:396
  165.4 38.6 %collective-permute-start.6 = (bf16[192,2048]{1,0:T(8,128)(2,1)}, bf16[192,2048]{1,0:T(8,128)(2,1)}, u32[]{:S(2)}, u32[]{:S(2)}) collective-permute-start(bf16[192,2048]{1,0:T(8,128)(2,1)} %arrange.1), channel_id=1, source_target_pairs={{0,3},{1,0},{2,1},{3,2},{4,7},{5,4},{6,5},{7,6},{8,11},{9,8},{10,9... | collective-permute-start | bytes 2359304 | tf_op jit(solution)/shard_map/ppermute | solution.py:362
  165.4 34.6 %collective-permute-start.8 = (bf16[192,2048]{1,0:T(8,128)(2,1)}, bf16[192,2048]{1,0:T(8,128)(2,1)}, u32[]{:S(2)}, u32[]{:S(2)}) collective-permute-start(bf16[192,2048]{1,0:T(8,128)(2,1)} %arrange.1), channel_id=1, source_target_pairs={{0,1},{1,2},{2,3},{3,0},{4,5},{5,6},{6,7},{7,4},{8,9},{9,10},{10,1... | collective-permute-start | bytes 2359304 | tf_op jit(solution)/shard_map/ppermute | solution.py:362
  169.3 48.0 %collective-permute-start.12 = (f32[64,2048]{1,0:T(8,128)}, f32[64,2048]{1,0:T(8,128)}, u32[]{:S(2)}, u32[]{:S(2)}) collective-permute-start(f32[64,2048]{1,0:T(8,128)} %get-tuple-element.32), channel_id=1, source_target_pairs={{0,0},{1,1},{2,254},{3,255},{4,4},{5,5},{6,250},{7,251},{8,8},{9,9... | collective-permute-start | bytes 1572872 | tf_op jit(solution)/shard_map/ppermute | solution.py:418
  182.5 26.1 %copy-start.2 = (bf16[1,2048,768]{2,1,0:T(8,128)(2,1)S(1)}, bf16[1,2048,768]{2,1,0:T(8,128)(2,1)}, u32[]{:S(2)}) copy-start(bf16[1,2048,768]{2,1,0:T(8,128)(2,1)} %param.19) | copy-start | bytes 9437188
  201.1 13.3 %collective-permute-start.10 = (bf16[96,2048]{1,0:T(8,128)(2,1)S(1)}, bf16[96,2048]{1,0:T(8,128)(2,1)S(1)}, u32[]{:S(2)}, u32[]{:S(2)}) collective-permute-start(bf16[96,2048]{1,0:T(8,128)(2,1)S(1)} %slice.24), channel_id=1, source_target_pairs={{0,1},{1,2},{2,3},{3,0},{4,5},{5,6},{6,7},{7,4},{8,9},{9,10},{10,1... | collective-permute-start | bytes 1179656 | tf_op jit(solution)/shard_map/ppermute | solution.py:367
  205.1 12.1 %collective-permute-start.11 = (bf16[96,2048]{1,0:T(8,128)(2,1)S(1)}, bf16[96,2048]{1,0:T(8,128)(2,1)S(1)}, u32[]{:S(2)}, u32[]{:S(2)}) collective-permute-start(bf16[96,2048]{1,0:T(8,128)(2,1)S(1)} %slice.25), channel_id=1, source_target_pairs={{0,3},{1,0},{2,1},{3,2},{4,7},{5,4},{6,5},{7,6},{8,11},{9,8},{10,9... | collective-permute-start | bytes 1179656 | tf_op jit(solution)/shard_map/ppermute | solution.py:367
  214.4 14.5 %collective-permute-start.7 = (bf16[192,768]{1,0:T(8,128)(2,1)S(1)}, bf16[192,768]{1,0:T(8,128)(2,1)S(1)}, u32[]{:S(2)}, u32[]{:S(2)}) collective-permute-start(bf16[192,768]{1,0:T(8,128)(2,1)S(1)} %multiply_convert_fusion.2), channel_id=1, source_target_pairs={{0,1},{1,2},{2,3},{3,0},{4,5},{5,6},{6,7},{7,4},{8,9},{9,10},{10,1... | collective-permute-start | bytes 884744 | tf_op jit(solution)/shard_map/ppermute | solution.py:430
  217.2 17.2 %collective-permute-start.9 = (bf16[192,768]{1,0:T(8,128)(2,1)S(1)}, bf16[192,768]{1,0:T(8,128)(2,1)S(1)}, u32[]{:S(2)}, u32[]{:S(2)}) collective-permute-start(bf16[192,768]{1,0:T(8,128)(2,1)S(1)} %multiply_convert_fusion.1), channel_id=1, source_target_pairs={{0,3},{1,0},{2,1},{3,2},{4,7},{5,4},{6,5},{7,6},{8,11},{9,8},{10,9... | collective-permute-start | bytes 884744 | tf_op jit(solution)/shard_map/ppermute | solution.py:431
  218.1 10.8 %copy-start.4 = (f32[192,2048]{1,0:T(8,128)S(1)}, f32[192,2048]{1,0:T(8,128)}, u32[]{:S(2)}) copy-start(f32[192,2048]{1,0:T(8,128)} %fusion.29) | copy-start | bytes 4718596
  218.9 12.8 %collective-permute-start.13 = (bf16[192,768]{1,0:T(8,128)(2,1)S(1)}, bf16[192,768]{1,0:T(8,128)(2,1)S(1)}, u32[]{:S(2)}, u32[]{:S(2)}) collective-permute-start(bf16[192,768]{1,0:T(8,128)(2,1)S(1)} %multiply_convert_fusion), channel_id=1, source_target_pairs={{0,2},{1,3},{2,0},{3,1},{4,6},{5,7},{6,4},{7,5},{8,10},{9,11},{10,... | collective-permute-start | bytes 884744 | tf_op jit(solution)/shard_map/ppermute | solution.py:433
  238.1 12.4 %copy-start.6 = (f32[64,2]{0,1:T(2,128)S(1)}, f32[64,2]{0,1:T(2,128)}, u32[]{:S(2)}) copy-start(f32[64,2]{0,1:T(2,128)} %param.18) | copy-start | bytes 1540
  240.7 32.9 %all-to-all-start.2 = ((bf16[64,48,128]{2,1,0:T(8,128)(2,1)}), bf16[64,48,128]{2,1,0:T(8,128)(2,1)}, u32[]{:S(2)}, u32[]{:S(2)}) async-start(bf16[64,48,128]{2,1,0:T(8,128)(2,1)} %spread.1), calls=%async_computation.2 | async-start | bytes 1572864 | tf_op jit(solution)/shard_map/all_to_all | solution.py:441
Sparse Core Ops, SparseCore 0:
  30.7 40.5 all-gather.3
